TPU v7x, 32 devices: a whole 2x2x4 slice. The times are simulated.
32 devices in a mesh: sp: 16 (over z, y, x), tp: 2 (over core).
Axes of the slice: x: 2, y: 2, z: 4, core: 2. Of those that a mesh axis runs over, the one named last changes fastest.
Arguments:
- conv_out: bfloat16 [2048, 2048], P('sp', 'tp'), may hold values from -1500 to 1500
- ln_gain: float32 [2048], P('tp'), may hold values from 0.1 to 1.9
- taps: bfloat16 [31, 2048], P(None, 'tp'), may hold values from -1 to 1
- proj_weight: bfloat16 [2048, 2048], P('sp', 'tp'), may hold values from -0.125 to 0.125
- stream_mid: bfloat16 [2048, 2048], P('sp', 'tp'), may hold values from -6 to 6
- out_grad: bfloat16 [2048, 2048], P('sp', 'tp'), may hold values from -6 to 6
- routes: int32 [2048, 2], P('sp'), may hold values from 0 to 7, all different within a row; in each aligned block of 128 rows (0 to 127, 128 to 255, ...) at most 48 rows name the same one
- route_probs: float32 [2048, 2], P('sp'), may hold values from 0.2 to 1
- gate_slabs: bfloat16 [16, 2048, 1792], P('sp', None, 'tp'), may hold values from -0.125 to 0.125
- up_slabs: bfloat16 [16, 2048, 1792], P('sp', None, 'tp'), may hold values from -0.125 to 0.125
- down_slabs: bfloat16 [16, 1792, 2048], P('sp', 'tp'), may hold values from -0.09375 to 0.09375
Outputs:
- grad_input: bfloat16 [2048, 2048], P('sp', 'tp')
- grad_proj: float32 [2048, 2048], P('sp', 'tp')
- grad_gate: bfloat16 [16, 2048, 1792], P('sp', None, 'tp')
- grad_up: bfloat16 [16, 2048, 1792], P('sp', None, 'tp')
- grad_down: bfloat16 [16, 1792, 2048], P('sp', 'tp')
Inputs may be any that keep to these rules, and one draw needn't show every extreme that they name: `routes`: each row names two different experts. Among the rows of one device no expert is named more than 48 times, and in every draw some device's rows name some expert exactly 48 times.
All inputs are finite; a program needn't handle non-finite values.
Results may differ from a plain program's by a relative error of at most 0.015.
Values may be sent and summed in bfloat16 or wider, within the bound.
No kernel may reach another device: no remote copies, remote signals or barrier semaphores. Data moves between devices by JAX's collectives and lax.ppermute only.
A program may use at most 128 MiB of HBM per device.

v0:
```python
import jax
import jax.numpy as jnp
from jax import lax
from jax.sharding import PartitionSpec as P

D = 2048


def passed_along(value, axis, steps):
    count = lax.axis_size(axis)
    first, last = (max(0, -steps), min(count, count - steps))
    return lax.ppermute(value, axis, [(source, source + steps) for source in range(first, last)])


def dispatch_table(route_block, experts, capacity):
    tok_rows = route_block.shape[0]
    labels = jnp.arange(experts, dtype=jnp.int32)
    onehot = (route_block[:, :, None] == labels[None, None, :]).astype(jnp.float32)
    per_token = jnp.sum(onehot, axis=1)
    earlier = (jnp.arange(tok_rows)[:, None] > jnp.arange(tok_rows)[None, :]).astype(jnp.float32)
    before = jnp.dot(earlier, per_token, precision=lax.Precision.HIGHEST)
    slot_index = jnp.sum(onehot * before[:, None, :], axis=2).astype(jnp.int32)
    position = route_block * capacity + slot_index
    columns = jnp.arange(experts * capacity, dtype=jnp.int32)
    first_pick = position[:, 0:1] == columns[None, :]
    second_pick = position[:, 1:2] == columns[None, :]
    return (first_pick, second_pick)


def contract_rows(left, right):
    return lax.dot_general(
        left, right, (((0,), (0,)), ((), ())), preferred_element_type=jnp.float32
    )


def contract_cols(left, right):
    return lax.dot_general(
        left, right, (((1,), (1,)), ((), ())), preferred_element_type=jnp.float32
    )


def on_device(
    conv_out,
    ln_gain,
    taps,
    proj_weight,
    stream_mid,
    out_grad,
    routes,
    route_probs,
    gate_slabs,
    up_slabs,
    down_slabs,
):
    tok_rows = conv_out.shape[0]
    experts = lax.axis_size("sp") // 2
    capacity = 3 * tok_rows // experts
    first_pick, second_pick = dispatch_table(routes, experts, capacity)
    route_table = (first_pick | second_pick).astype(jnp.bfloat16)
    slot_probs = jnp.sum(
        first_pick.astype(jnp.float32) * route_probs[:, 0:1]
        + second_pick.astype(jnp.float32) * route_probs[:, 1:2],
        axis=0,
    )
    probs_out = jnp.repeat(slot_probs.reshape(experts, capacity), 2, axis=0)

    def packed(source):
        filled = contract_rows(route_table, source).astype(jnp.bfloat16)
        return jnp.repeat(filled.reshape(experts, capacity, source.shape[1]), 2, axis=0)

    whole_mid, whole_grad = (
        lax.all_gather(stream_mid, "tp", axis=1, tiled=True),
        lax.all_gather(out_grad, "tp", axis=1, tiled=True),
    )
    arrived_mid, arrived_grad, arrived_probs = (
        lax.all_to_all(packed(whole_mid), "sp", split_axis=0, concat_axis=0, tiled=True),
        lax.all_to_all(packed(whole_grad), "sp", split_axis=0, concat_axis=0, tiled=True),
        lax.all_to_all(
            probs_out.astype(jnp.bfloat16), "sp", split_axis=0, concat_axis=0, tiled=True
        ).astype(probs_out.dtype),
    )
    slot_rows = arrived_mid.shape[0] * arrived_mid.shape[1]
    expert_in = arrived_mid.reshape(slot_rows, arrived_mid.shape[2])
    expert_grad = arrived_grad.reshape(slot_rows, arrived_grad.shape[2])
    weight = arrived_probs.reshape(slot_rows, 1)
    w_gate = gate_slabs[0]
    w_up = up_slabs[0]
    w_down = down_slabs[0]
    gate_value = jnp.dot(expert_in, w_gate, preferred_element_type=jnp.float32)
    up_value = jnp.dot(expert_in, w_up, preferred_element_type=jnp.float32)
    gate_sig = jax.nn.sigmoid(gate_value)
    hidden_act = gate_value * gate_sig * up_value
    scaled = (weight * hidden_act).astype(jnp.bfloat16)
    grad_down = contract_rows(scaled, expert_grad).astype(jnp.bfloat16)
    grad_hidden = weight * contract_cols(expert_grad, w_down)
    grad_gate_pre = (
        grad_hidden * up_value * gate_sig * (1.0 + gate_value * (1.0 - gate_sig))
    ).astype(jnp.bfloat16)
    grad_up_pre = (grad_hidden * gate_value * gate_sig).astype(jnp.bfloat16)
    grad_gate = contract_rows(expert_in, grad_gate_pre).astype(jnp.bfloat16)
    grad_up = contract_rows(expert_in, grad_up_pre).astype(jnp.bfloat16)
    partial_value = contract_cols(grad_gate_pre, w_gate) + contract_cols(grad_up_pre, w_up)
    summed = lax.psum_scatter(
        partial_value.astype(jnp.bfloat16), "tp", scatter_dimension=1, tiled=True
    )
    returned = lax.all_to_all(
        summed.reshape(arrived_mid.shape[0], capacity, summed.shape[1]),
        "sp",
        split_axis=0,
        concat_axis=0,
        tiled=True,
    )
    pair_rows = returned.reshape(experts, 2, capacity, returned.shape[2])
    contrib = jnp.dot(
        route_table,
        pair_rows[:, 0].reshape(experts * capacity, returned.shape[2]),
        preferred_element_type=jnp.float32,
    )
    contrib = contrib + jnp.dot(
        route_table,
        pair_rows[:, 1].reshape(experts * capacity, returned.shape[2]),
        preferred_element_type=jnp.float32,
    )
    grad_stream = (out_grad.astype(jnp.float32) + contrib).astype(jnp.bfloat16)
    values = conv_out.astype(jnp.float32)
    row_total, row_squares = lax.psum(
        (jnp.sum(values, axis=1), jnp.sum(values * values, axis=1)), "tp"
    )
    row_mean = row_total[:, None] / D
    row_var = row_squares[:, None] / D - row_mean * row_mean
    inv_std = lax.rsqrt(row_var + 1e-06)
    normed = (values - row_mean) * inv_std
    scaled_z = normed * ln_gain[None, :]
    z_sig = jax.nn.sigmoid(scaled_z)
    activated = (scaled_z * z_sig).astype(jnp.bfloat16)
    whole_stream = lax.all_gather(grad_stream, "tp", axis=1, tiled=True)
    grad_act = jnp.dot(
        whole_stream,
        lax.all_gather(proj_weight, "sp", axis=0, tiled=True),
        preferred_element_type=jnp.float32,
    )
    grad_normed = grad_act * z_sig * (1.0 + scaled_z * (1.0 - z_sig)) * ln_gain[None, :]
    first_sum, second_sum = lax.psum(
        (jnp.sum(grad_normed, axis=1), jnp.sum(grad_normed * normed, axis=1)), "tp"
    )
    grad_conv = (
        inv_std * (grad_normed - first_sum[:, None] / D - normed * second_sum[:, None] / D)
    ).astype(jnp.bfloat16)
    reach_rows = taps.shape[0] - 1
    following = passed_along(grad_conv[:reach_rows], "sp", -1)
    extended = jnp.concatenate([grad_conv, following], axis=0).astype(jnp.float32)
    tap_values = taps.astype(jnp.float32)
    grad_input = jnp.zeros((tok_rows, grad_conv.shape[1]), jnp.float32)
    for offset in range(taps.shape[0]):
        grad_input = grad_input + tap_values[offset][None, :] * extended[offset : offset + tok_rows]
    own_columns = lax.all_to_all(whole_stream, "sp", split_axis=1, concat_axis=0, tiled=True)
    grad_proj = contract_rows(own_columns, lax.all_gather(activated, "sp", axis=0, tiled=True))
    return (
        grad_input.astype(jnp.bfloat16),
        grad_proj,
        grad_gate[None],
        grad_up[None],
        grad_down[None],
    )


def solution(mesh):
    return jax.shard_map(
        on_device,
        mesh=mesh,
        in_specs=(
            P("sp", "tp"),
            P("tp"),
            P(None, "tp"),
            P("sp", "tp"),
            P("sp", "tp"),
            P("sp", "tp"),
            P("sp", None),
            P("sp", None),
            P("sp", None, "tp"),
            P("sp", None, "tp"),
            P("sp", "tp", None),
        ),
        out_specs=(
            P("sp", "tp"),
            P("sp", "tp"),
            P("sp", None, "tp"),
            P("sp", None, "tp"),
            P("sp", "tp", None),
        ),
        check_vma=False,
    )
```

profile of v0, /device:TPU:0, one launch (start us, length us, event | category | flops | bytes accessed | tf_op | source)
XLA Modules:
  0.0 395.2 jit_solution(838631886129890489)
XLA Ops:
  8.0 0.7 convert_reduce_fusion.2
  8.7 0.1 fusion.73
  8.8 0.8 select_reduce_fusion
  9.6 0.7 convert_add_fusion
  10.3 0.8 slice_bitcast_fusion.1
  11.0 0.1 add_reduce_fusion
  11.2 0.1 convert_element_type.94
  11.3 0.6 copy.28
  11.9 8.3 %all-to-all-start = ((bf16[16,1,48]{2,1,0:T(2,128)(2,1)}), bf16[16,1,48]{2,1,0:T(2,128)(2,1)S(1)}, u32[]{:S(2)}, u32[]{:S(2)}) async-start(bf16[16,1,48]{2,1,0:T(2,128)(2,1)} %copy.28), calls=%async_computation | async-start | bytes 16384 | tf_op jit(solution)/shard_map/all_to_all | solution.py:78
  20.2 2.4 all_gather.16
  22.6 0.7 convolution_convert_fusion
  23.3 4.1 %all-to-all-done = bf16[16,1,48]{2,1,0:T(2,128)(2,1)S(1)} async-done(((bf16[16,1,48]{2,1,0:T(2,128)(2,1)}), bf16[16,1,48]{2,1,0:T(2,128)(2,1)S(1)}, u32[]{:S(2)}, u32[]{:S(2)}) %all-to-all-start) | async-done | bytes 1568 | tf_op jit(solution)/shard_map/all_to_all | solution.py:78
  27.5 2.1 broadcast_in_dim.14
  29.5 4.6 %all-to-all-start.2 = ((bf16[16,48,2048]{2,1,0:T(8,128)(2,1)}), bf16[16,48,2048]{2,1,0:T(8,128)(2,1)}, u32[]{:S(2)}, u32[]{:S(2)}) async-start(bf16[16,48,2048]{2,1,0:T(8,128)(2,1)} %bitcast.11), calls=%async_computation.2 | async-start | bytes 6291456 | tf_op jit(solution)/shard_map/all_to_all | solution.py:76
  34.2 0.0 copy-done.2
  34.2 2.2 all_gather.15
  36.4 0.7 convolution_convert_fusion.1
  37.0 57.4 %all-to-all-done.2 = bf16[16,48,2048]{2,1,0:T(8,128)(2,1)} async-done(((bf16[16,48,2048]{2,1,0:T(8,128)(2,1)}), bf16[16,48,2048]{2,1,0:T(8,128)(2,1)}, u32[]{:S(2)}, u32[]{:S(2)}) %all-to-all-start.2) | async-done | bytes 3145760 | tf_op jit(solution)/shard_map/all_to_all | solution.py:76
  94.4 2.1 broadcast_in_dim.13
  96.5 14.0 %all-to-all-start.1 = ((bf16[16,48,2048]{2,1,0:T(8,128)(2,1)}), bf16[16,48,2048]{2,1,0:T(8,128)(2,1)S(1)}, u32[]{:S(2)}, u32[]{:S(2)}) async-start(bf16[16,48,2048]{2,1,0:T(8,128)(2,1)} %bitcast.7), calls=%async_computation.1 | async-start | bytes 6291456 | tf_op jit(solution)/shard_map/all_to_all | solution.py:77
  110.5 0.2 reduce-scatter.2.cloned.1.call-start
  110.8 0.1 reshape.83
  110.9 8.0 %fusion.6 = f32[768,896]{1,0:T(8,128)} fusion(bf16[768,2048]{1,0:T(8,128)(2,1)} %bitcast.12, bf16[1,2048,896]{2,1,0:T(8,128)(2,1)} %param.20), kind=kOutput, calls=%fused_computation.7 | convolution fusion | flops 2818572288 | bytes 9568256 | tf_op jit(solution)/shard_map/dot_general | solution.py:90
  118.8 52.3 %all-to-all-done.1 = bf16[16,48,2048]{2,1,0:T(8,128)(2,1)S(1)} async-done(((bf16[16,48,2048]{2,1,0:T(8,128)(2,1)}), bf16[16,48,2048]{2,1,0:T(8,128)(2,1)S(1)}, u32[]{:S(2)}, u32[]{:S(2)}) %all-to-all-start.1) | async-done | bytes 3145760 | tf_op jit(solution)/shard_map/all_to_all | solution.py:77
  171.2 6.7 %fusion.8 = f32[768,896]{1,0:T(8,128)S(1)} fusion(bf16[768,2048]{1,0:T(8,128)(2,1)S(1)} %bitcast.103, bf16[1,896,2048]{2,1,0:T(8,128)(2,1)} %param.21), kind=kOutput, calls=%fused_computation.9 | convolution fusion | flops 2818572288 | bytes 9568256 | tf_op jit(solution)/shard_map/dot_general | solution.py:37
  177.8 0.0 copy-done
  177.9 7.7 %multiply_convert_fusion.1 = (bf16[768,896]{1,0:T(8,128)(2,1)S(1)}, bf16[768,896]{1,0:T(8,128)(2,1)S(1)}, f32[768,896]{1,0:T(8,128)}) fusion(f32[768,896]{1,0:T(8,128)S(1)} %fusion.8, f32[768]{0:T(1024)S(1)} %reshape.83, f32[768,896]{1,0:T(8,128)S(1)} %copy-done.10, bf16[768,2048]{1,0:T(8,128)(2,1)} %bitcast.12, bf16[1,2048,896]{2,1,0:T(8,128)(2,1)S(1)} %copy-done.5), kind=kOutput, calls=%fused_computation.17 | convolution fusion | flops 2828206080 | bytes 17828864 | tf_op jit(solution)/shard_map/dot_general | solution.py:89
  185.6 3.4 fusion
  189.0 4.8 %add_convert_fusion = bf16[768,2048]{1,0:T(8,128)(2,1)} fusion(f32[768,2048]{1,0:T(8,128)S(1)} %fusion, bf16[768,896]{1,0:T(8,128)(2,1)S(1)} %get-tuple-element.13, bf16[1,2048,896]{2,1,0:T(8,128)(2,1)S(1)} %copy-done.6), kind=kOutput, calls=%fused_computation | convolution fusion | flops 2821718016 | bytes 14483456 | tf_op jit(solution)/shard_map/dot_general | solution.py:37
  193.9 0.0 reduce-scatter.2.cloned.1.call-update
  193.9 0.0 all-gather.3.cloned.1.call-start
  193.9 0.5 all-gather.3.cloned.1.call-update
  194.5 19.0 %reduce-scatter.2.cloned.1.call-done = bf16[768,1024]{1,0:T(8,128)(2,1)} async-done(((bf16[768,2048]{1,0:T(8,128)(2,1)}), bf16[768,1024]{1,0:T(8,128)(2,1)}) %reduce-scatter.2.cloned.1.call-update) | async-done | bytes 1572880 | tf_op jit(solution)/shard_map/reduce_scatter | solution.py:103
  213.5 6.9 %all-to-all-start.3 = ((bf16[16,48,1024]{2,1,0:T(8,128)(2,1)}), bf16[16,48,1024]{2,1,0:T(8,128)(2,1)S(1)}, u32[]{:S(2)}, u32[]{:S(2)}) async-start(bf16[16,48,1024]{2,1,0:T(8,128)(2,1)} %bitcast.108), calls=%async_computation.4 | async-start | bytes 3145728 | tf_op jit(solution)/shard_map/all_to_all | solution.py:106
  220.3 0.0 all-gather.5.cloned.1.call-start
  220.4 0.1 fusion.18
  220.6 2.7 all-reduce.1
  223.3 40.7 %all-to-all-done.3 = bf16[16,48,1024]{2,1,0:T(8,128)(2,1)S(1)} async-done(((bf16[16,48,1024]{2,1,0:T(8,128)(2,1)}), bf16[16,48,1024]{2,1,0:T(8,128)(2,1)S(1)}, u32[]{:S(2)}, u32[]{:S(2)}) %all-to-all-start.3) | async-done | bytes 1572896 | tf_op jit(solution)/shard_map/all_to_all | solution.py:106
  264.0 0.1 fusion.76
  264.1 0.3 fusion.69
  264.5 0.4 fusion.17
  264.8 2.2 all_gather.17
  267.0 35.9 %all-gather.3.cloned.1.call-done = bf16[2048,1024]{1,0:T(8,128)(2,1)} async-done(((bf16[128,1024]{1,0:T(8,128)(2,1)}), bf16[2048,1024]{1,0:T(8,128)(2,1)}) %all-gather.3.cloned.1.call-update) | async-done | bytes 4194320 | tf_op jit(solution)/shard_map/all_gather | solution.py:139
  302.9 4.0 %fusion.75 = (f32[128]{0:T(128)S(1)}, f32[128]{0:T(128)S(1)}, bf16[128,1024]{1,0:T(8,128)(2,1)}, f32[128,1024]{1,0:T(8,128)S(1)}) fusion(f32[128]{0:T(128)S(1)} %get-tuple-element.53, f32[128]{0:T(128)S(1)} %get-tuple-element.54, bf16[128,1024]{1,0:T(8,128)(2,1)S(1)} %copy-done.3, f32[1024]{0:T(1024)S(1)} %copy-done.7, ...), kind=kOutput, calls=%fused_computation.133 | convolution fusion | flops 539229952 | bytes 5773312 | tf_op jit(solution)/shard_map/dot_general | solution.py:137
  306.9 0.0 all-gather.5.cloned.1.call-update
  307.0 0.0 copy-done.4
  307.0 0.1 fusion.77
  307.1 0.0 copy-done.13
  307.1 0.0 copy-start.1
  307.1 7.4 %convert_bitcast_fusion.1 = bf16[1,2048,896]{2,1,0:T(8,128)(2,1)} fusion(bf16[768,2048]{1,0:T(8,128)(2,1)} %bitcast.12, bf16[768,896]{1,0:T(8,128)(2,1)S(1)} %copy-done.13), kind=kOutput, calls=%fused_computation.12 | convolution fusion | flops 2820407296 | bytes 8192000 | tf_op jit(solution)/shard_map/dot_general | solution.py:31
  314.5 0.0 copy-done.11
  314.5 5.2 %convert_bitcast_fusion = bf16[1,896,2048]{2,1,0:T(8,128)(2,1)} fusion(bf16[768,2048]{1,0:T(8,128)(2,1)S(1)} %bitcast.104, f32[768,896]{1,0:T(8,128)S(1)} %copy-done.11, f32[768,896]{1,0:T(8,128)S(1)} %copy-done.14, f32[768]{0:T(1024)S(1)} %reshape.83), kind=kOutput, calls=%fused_computation.11 | convolution fusion | flops 2825224192 | bytes 12323840 | tf_op jit(solution)/shard_map/dot_general | solution.py:31
  319.7 0.9 copy_bitcast_fusion
  320.6 4.2 %all-to-all-start.4 = ((bf16[128,16,128]{2,0,1:T(8,128)(2,1)}), bf16[128,16,128]{2,0,1:T(8,128)(2,1)S(1)}, u32[]{:S(2)}, u32[]{:S(2)}) async-start(bf16[128,16,128]{2,0,1:T(8,128)(2,1)} %copy_bitcast_fusion), calls=%async_computation.5 | async-start | bytes 1048576 | tf_op jit(solution)/shard_map/all_to_all | solution.py:156
  324.8 2.5 all-reduce
  327.3 0.3 fusion.35
  327.6 1.6 collective-permute-start
  329.1 7.2 %convert_bitcast_fusion.2 = bf16[1,2048,896]{2,1,0:T(8,128)(2,1)} fusion(bf16[768,2048]{1,0:T(8,128)(2,1)} %bitcast.12, bf16[768,896]{1,0:T(8,128)(2,1)S(1)} %copy-done.9), kind=kOutput, calls=%fused_computation.13 | convolution fusion | flops 2820407296 | bytes 8192000 | tf_op jit(solution)/shard_map/dot_general | solution.py:31
  336.4 0.5 collective-permute-done
  336.8 0.1 maximum_convert_fusion
  336.9 2.7 fusion.37
  339.6 3.4 all-to-all-done.4
  343.1 40.9 %all-gather.5.cloned.1.call-done = bf16[2048,1024]{1,0:T(8,128)(2,1)} async-done(((bf16[128,1024]{1,0:T(8,128)(2,1)}), bf16[2048,1024]{1,0:T(8,128)(2,1)}) %all-gather.5.cloned.1.call-update) | async-done | bytes 4194320 | tf_op jit(solution)/shard_map/all_gather | solution.py:157
  384.0 3.7 fusion.79
  (31 shorter events, 0.1 us)
Async XLA Ops:
  11.9 15.6 %all-to-all-start = ((bf16[16,1,48]{2,1,0:T(2,128)(2,1)}), bf16[16,1,48]{2,1,0:T(2,128)(2,1)S(1)}, u32[]{:S(2)}, u32[]{:S(2)}) async-start(bf16[16,1,48]{2,1,0:T(2,128)(2,1)} %copy.28), calls=%async_computation | async-start | bytes 16384 | tf_op jit(solution)/shard_map/all_to_all | solution.py:78
  29.5 4.6 %copy-start.2 = (bf16[128,1024]{1,0:T(8,128)(2,1)S(1)}, bf16[128,1024]{1,0:T(8,128)(2,1)}, u32[]{:S(2)}) copy-start(bf16[128,1024]{1,0:T(8,128)(2,1)} %param.16) | copy-start | bytes 786436
  29.5 64.9 %all-to-all-start.2 = ((bf16[16,48,2048]{2,1,0:T(8,128)(2,1)}), bf16[16,48,2048]{2,1,0:T(8,128)(2,1)}, u32[]{:S(2)}, u32[]{:S(2)}) async-start(bf16[16,48,2048]{2,1,0:T(8,128)(2,1)} %bitcast.11), calls=%async_computation.2 | async-start | bytes 6291456 | tf_op jit(solution)/shard_map/all_to_all | solution.py:76
  96.5 74.7 %all-to-all-start.1 = ((bf16[16,48,2048]{2,1,0:T(8,128)(2,1)}), bf16[16,48,2048]{2,1,0:T(8,128)(2,1)S(1)}, u32[]{:S(2)}, u32[]{:S(2)}) async-start(bf16[16,48,2048]{2,1,0:T(8,128)(2,1)} %bitcast.7), calls=%async_computation.1 | async-start | bytes 6291456 | tf_op jit(solution)/shard_map/all_to_all | solution.py:77
  110.5 102.9 %reduce-scatter.2.cloned.1.call-start = ((), (), s32[]{:S(2)}) async-start(), calls=%async_computation.6 | async-start | bytes 4718592 | tf_op jit(solution)/shard_map/reduce_scatter | solution.py:103
  171.2 6.7 %copy-start = (bf16[16,48,2048]{2,1,0:T(8,128)(2,1)}, bf16[16,48,2048]{2,1,0:T(8,128)(2,1)S(1)}, u32[]{:S(2)}) copy-start(bf16[16,48,2048]{2,1,0:T(8,128)(2,1)S(1)} %all-to-all-done.1) | copy-start | bytes 9437188
  171.2 6.7 %copy-start.5 = (bf16[1,2048,896]{2,1,0:T(8,128)(2,1)S(1)}, bf16[1,2048,896]{2,1,0:T(8,128)(2,1)}, u32[]{:S(2)}) copy-start(bf16[1,2048,896]{2,1,0:T(8,128)(2,1)} %param.19) | copy-start | bytes 11010052
  171.2 6.7 %copy-start.10 = (f32[768,896]{1,0:T(8,128)S(1)}, f32[768,896]{1,0:T(8,128)}, u32[]{:S(2)}) copy-start(f32[768,896]{1,0:T(8,128)} %fusion.6) | copy-start | bytes 8257540
  185.6 3.5 copy-start.8
  185.6 3.5 copy-start.12
  185.6 3.5 copy-start.6
  193.9 26.5 %copy-start.3 = (bf16[128,1024]{1,0:T(8,128)(2,1)S(1)}, bf16[128,1024]{1,0:T(8,128)(2,1)}, u32[]{:S(2)}) copy-start(bf16[128,1024]{1,0:T(8,128)(2,1)} %param.11) | copy-start | bytes 786436
  193.9 109.0 %all-gather.3.cloned.1.call-start = ((), (), s32[]{:S(2)}) async-start(), calls=%async_computation.7 | async-start | bytes 4456448 | tf_op jit(solution)/shard_map/all_gather | solution.py:139
  213.5 50.5 %all-to-all-start.3 = ((bf16[16,48,1024]{2,1,0:T(8,128)(2,1)}), bf16[16,48,1024]{2,1,0:T(8,128)(2,1)S(1)}, u32[]{:S(2)}, u32[]{:S(2)}) async-start(bf16[16,48,1024]{2,1,0:T(8,128)(2,1)} %bitcast.108), calls=%async_computation.4 | async-start | bytes 3145728 | tf_op jit(solution)/shard_map/all_to_all | solution.py:106
  220.3 163.6 %all-gather.5.cloned.1.call-start = ((), (), s32[]{:S(2)}) async-start(), calls=%async_computation.8 | async-start | bytes 4456448 | tf_op jit(solution)/shard_map/all_gather | solution.py:157
  264.0 38.9 %copy-start.7 = (f32[1024]{0:T(1024)S(1)}, f32[1024]{0:T(1024)}, u32[]{:S(2)}) copy-start(f32[1024]{0:T(1024)} %param.12) | copy-start | bytes 12292
  302.9 4.0 %copy-start.4 = (bf16[31,1024]{1,0:T(8,128)(2,1)S(1)}, bf16[31,1024]{1,0:T(8,128)(2,1)}, u32[]{:S(2)}) copy-start(bf16[31,1024]{1,0:T(8,128)(2,1)} %param.13) | copy-start | bytes 190468
  302.9 4.2 %copy-start.13 = (bf16[768,896]{1,0:T(8,128)(2,1)S(1)}, bf16[768,896]{1,0:T(8,128)(2,1)}, u32[]{:S(2)}) copy-start(bf16[768,896]{1,0:T(8,128)(2,1)} %copy-done.12) | copy-start | bytes 4128772
  307.1 7.4 %copy-start.1 = (bf16[16,48,2048]{2,1,0:T(8,128)(2,1)S(1)}, bf16[16,48,2048]{2,1,0:T(8,128)(2,1)}, u32[]{:S(2)}) copy-start(bf16[16,48,2048]{2,1,0:T(8,128)(2,1)} %copy-done) | copy-start | bytes 9437188
  307.1 7.4 %copy-start.11 = (f32[768,896]{1,0:T(8,128)S(1)}, f32[768,896]{1,0:T(8,128)}, u32[]{:S(2)}) copy-start(f32[768,896]{1,0:T(8,128)} %fusion.6) | copy-start | bytes 8257540
  307.1 7.4 %copy-start.14 = (f32[768,896]{1,0:T(8,128)S(1)}, f32[768,896]{1,0:T(8,128)}, u32[]{:S(2)}) copy-start(f32[768,896]{1,0:T(8,128)} %get-tuple-element.55) | copy-start | bytes 8257540
  319.7 9.5 %copy-start.9 = (bf16[768,896]{1,0:T(8,128)(2,1)S(1)}, bf16[768,896]{1,0:T(8,128)(2,1)}, u32[]{:S(2)}) copy-start(bf16[768,896]{1,0:T(8,128)(2,1)} %copy-done.8) | copy-start | bytes 4128772
  320.6 22.5 %all-to-all-start.4 = ((bf16[128,16,128]{2,0,1:T(8,128)(2,1)}), bf16[128,16,128]{2,0,1:T(8,128)(2,1)S(1)}, u32[]{:S(2)}, u32[]{:S(2)}) async-start(bf16[128,16,128]{2,0,1:T(8,128)(2,1)} %copy_bitcast_fusion), calls=%async_computation.5 | async-start | bytes 1048576 | tf_op jit(solution)/shard_map/all_to_all | solution.py:156
  327.6 9.3 %collective-permute-start = (bf16[30,1024]{1,0:T(8,128)(2,1)S(1)}, bf16[30,1024]{1,0:T(8,128)(2,1)S(1)}, u32[]{:S(2)}, u32[]{:S(2)}) collective-permute-start(bf16[30,1024]{1,0:T(8,128)(2,1)S(1)} %slice.279), channel_id=1, source_target_pairs={{2,0},{4,2},{6,4},{8,6},{10,8},{12,10},{14,12},{16,14},{18,16},{20... | collective-permute-start | bytes 184328 | tf_op jit(solution)/shard_map/ppermute | solution.py:12
Sparse Core Ops, SparseCore 0:
  194.0 19.4 reduce-scatter.1
Sparse Core Ops, SparseCore 1:
  197.1 105.7 all-gather.2
  307.0 76.9 all-gather.4
where the time goes:
time: 396 us; the launch traced here: 395 us
  waiting for transfers between devices  255 us (64%)
  matrix products  60.3 us (15%)
  starting transfers between devices  39.9 us (10%)
  between operations  15.8 us (4%)
  blocking collectives  11.9 us (3%)
  local copies, waits for them, and re-layouts  6.88 us (2%)
  other arithmetic  5.52 us (1%)
    all_to_all x1, waiting for transfers between devices, on_device(): lax.all_to_all(packed(whole_mid), 'sp', split_axis=0, concat_axis=0, tile...  57.4 us
    all_to_all x1, waiting for transfers between devices, on_device(): lax.all_to_all(packed(whole_grad), 'sp', split_axis=0, concat_axis=0, til...  52.3 us
    all_gather x1, waiting for transfers between devices, on_device(): lax.all_gather(activated, 'sp', axis=0, tiled=True)  40.9 us
    all_to_all x1, waiting for transfers between devices, on_device(): lax.all_to_all(summed.reshape(arrived_mid.shape[0], capacity, summed.shap...  40.7 us
    all_gather x1, waiting for transfers between devices, on_device(): lax.all_gather(proj_weight, 'sp', axis=0, tiled=True)  35.9 us
    dot_general x6, matrix products, contract_rows(): lax.dot_general(left, right, (((0,), (0,)), ((), ())), preferred_element_...  24.9 us
    reduce_scatter x1, waiting for transfers between devices, on_device(): lax.psum_scatter(partial_value.astype(jnp.bfloat16), 'tp', scatter_dimens...  19 us
    dot_general x3, matrix products, contract_cols(): lax.dot_general(left, right, (((1,), (1,)), ((), ())), preferred_element_...  14.9 us
  transfers between devices with their start and end apart: 9, of which 9 were waited for; matrix products, arithmetic and copies ran while one was open for 9% of the time, Pallas kernels for 0%

commit v1 on v0

v1 whole, which is shorter than its diff:
```python
import jax
import jax.numpy as jnp
from jax import lax
from jax.sharding import Mesh
from jax.sharding import PartitionSpec as P


SP = ("far", "side", "pair")
fence = lax.optimization_barrier


def swapped(value, axis):
    return lax.ppermute(value, axis, [(0, 1), (1, 0)])


def shifted(value, steps):
    count = lax.axis_size("far")
    return lax.ppermute(value, "far", [(s, (s + steps) % count) for s in range(count)])


def passed_along(value, steps):
    count = lax.axis_size(SP)
    first, last = (max(0, -steps), min(count, count - steps))
    return lax.ppermute(value, SP, [(source, source + steps) for source in range(first, last)])


def chosen(bit, low, high):
    return jnp.where(bit == 0, low, high)


def slot_columns(info, targets, capacity):
    rows = info.shape[1]
    routes = info[0:2]
    probs = info[2:4]
    wide = targets.shape[0] * capacity
    earlier = (jnp.arange(rows)[:, None] > jnp.arange(rows)[None, :]).astype(jnp.bfloat16)
    target_of = jnp.repeat(targets, capacity).astype(jnp.float32)
    slot_of = (jnp.arange(wide) % capacity).astype(jnp.float32)
    first = routes[0][:, None] == target_of[None, :]
    second = routes[1][:, None] == target_of[None, :]
    named = (first | second).astype(jnp.bfloat16)
    before = jnp.dot(earlier, named, preferred_element_type=jnp.float32)
    here = before == slot_of[None, :]
    first, second = (first & here, second & here)
    weights = jnp.sum(
        jnp.where(first, probs[0][:, None], 0.0) + jnp.where(second, probs[1][:, None], 0.0),
        axis=0,
    )
    return ((first | second).astype(jnp.bfloat16), weights)


def contract_rows(left, right):
    return lax.dot_general(
        left, right, (((0,), (0,)), ((), ())), preferred_element_type=jnp.float32
    )


def contract_cols(left, right):
    return lax.dot_general(
        left, right, (((1,), (1,)), ((), ())), preferred_element_type=jnp.float32
    )


def on_device(
    conv_out,
    ln_gain,
    taps,
    proj_weight,
    stream_mid,
    out_grad,
    routes,
    route_probs,
    gate_slabs,
    up_slabs,
    down_slabs,
):
    tok_rows, half = conv_out.shape
    width = half * lax.axis_size("tp")
    planes = lax.axis_size("far")
    experts = 2 * planes
    capacity = 3 * tok_rows // experts
    out_rows = proj_weight.shape[0]
    core = lax.axis_index("tp")
    plane = lax.axis_index("far")
    side = lax.axis_index("side")
    pair = lax.axis_index("pair")
    wide = planes * capacity
    hops = range(1, planes)

    info = jnp.concatenate([routes.astype(jnp.float32).T, route_probs.T], axis=0)
    beside_info = swapped(info, "side")
    beside_mid = swapped(stream_mid, "side")
    beside_grad = swapped(out_grad, "side")

    values = conv_out.astype(jnp.float32)
    row_total, row_squares = lax.psum(
        (jnp.sum(values, axis=1), jnp.sum(values * values, axis=1)), "tp"
    )
    row_mean = row_total[:, None] / width
    row_var = row_squares[:, None] / width - row_mean * row_mean
    inv_std = lax.rsqrt(row_var + 1e-06)
    normed = (values - row_mean) * inv_std
    scaled_z = normed * ln_gain[None, :]
    z_sig = jax.nn.sigmoid(scaled_z)
    activated = (scaled_z * z_sig).astype(jnp.bfloat16)

    targets = 2 * ((plane + jnp.arange(planes)) % planes) + side
    own_table, own_weights = slot_columns(info, targets, capacity)
    beside_table, beside_weights = slot_columns(beside_info, targets, capacity)

    def by_target(near, far):
        near, far = (
            block.astype(jnp.bfloat16).reshape(planes, capacity, half) for block in (near, far)
        )
        return [jnp.stack([near[k], far[k]]) for k in range(planes)]

    mid_slots = by_target(
        contract_rows(own_table, stream_mid), contract_rows(beside_table, beside_mid)
    )
    grad_slots = by_target(
        contract_rows(own_table, out_grad) * own_weights[:, None],
        contract_rows(beside_table, beside_grad) * beside_weights[:, None],
    )
    mid_far = [shifted(mid_slots[k], k) for k in hops]
    mid_far, grad_slots, activated = fence((mid_far, grad_slots, activated))
    mid_mine = jnp.stack([mid_slots[0], *mid_far]).reshape(2 * wide, half)
    mid_pair = swapped(mid_mine, "pair")
    grad_far = [shifted(grad_slots[k], k) for k in hops]
    mid_pair, grad_far, proj_held, act_held = fence(
        (mid_pair, grad_far, proj_weight, activated)
    )
    grad_mine = jnp.stack([grad_slots[0], *grad_far]).reshape(2 * wide, half)
    grad_pair = swapped(grad_mine, "pair")
    proj_far = [shifted(proj_held, k) for k in hops]
    act_far = [shifted(act_held, k) for k in hops]

    def assembled(mine, paired):
        rows = jnp.concatenate([mine, paired], axis=0)
        other = swapped(rows, "tp")
        return chosen(
            core,
            jnp.concatenate([rows, other], axis=1),
            jnp.concatenate([other, rows], axis=1),
        )

    def in_order(own, pieces):
        held = jnp.zeros((planes, *own.shape), own.dtype)
        for k, piece in enumerate([own, *pieces]):
            held = lax.dynamic_update_slice(
                held, piece[None], ((plane - k) % planes,) + (0,) * own.ndim
            )
        return held.reshape(planes * own.shape[0], own.shape[1])

    expert_in = fence(assembled(mid_mine, mid_pair))
    expert_grad = fence(assembled(grad_mine, grad_pair))
    w_gate = gate_slabs[0]
    w_up = up_slabs[0]
    w_down = down_slabs[0]
    gate_value = jnp.dot(expert_in, w_gate, preferred_element_type=jnp.float32)
    up_value = jnp.dot(expert_in, w_up, preferred_element_type=jnp.float32)
    gate_sig = jax.nn.sigmoid(gate_value)
    hidden_act = (gate_value * gate_sig * up_value).astype(jnp.bfloat16)
    grad_hidden = contract_cols(expert_grad, w_down)
    grad_gate_pre = (
        grad_hidden * up_value * gate_sig * (1.0 + gate_value * (1.0 - gate_sig))
    ).astype(jnp.bfloat16)
    grad_up_pre = (grad_hidden * gate_value * gate_sig).astype(jnp.bfloat16)
    partial_value = (
        contract_cols(grad_gate_pre, w_gate) + contract_cols(grad_up_pre, w_up)
    ).astype(jnp.bfloat16)
    low, high = (partial_value[:, :half], partial_value[:, half:])
    given = swapped(chosen(core, high, low), "tp")
    summed = (chosen(core, low, high).astype(jnp.float32) + given.astype(jnp.float32)).astype(
        jnp.bfloat16
    )
    proj_mine = in_order(proj_weight, proj_far)
    proj_side = swapped(proj_mine, "side")
    act_mine = in_order(activated, act_far)
    act_side = swapped(act_mine, "side")
    across = swapped(summed[2 * wide :], "pair")
    both = (summed[: 2 * wide].astype(jnp.float32) + across.astype(jnp.float32)).astype(
        jnp.bfloat16
    )
    both = both.reshape(planes, 2, capacity, half)
    back = jnp.stack([both[0]] + [shifted(both[k], -k) for k in hops])
    for_beside = jnp.dot(
        beside_table, back[:, 1].reshape(wide, half), preferred_element_type=jnp.float32
    ).astype(jnp.bfloat16)
    for_own = jnp.dot(
        own_table, back[:, 0].reshape(wide, half), preferred_element_type=jnp.float32
    )
    from_beside = swapped(for_beside, "side")
    grad_stream = (
        out_grad.astype(jnp.float32) + for_own + from_beside.astype(jnp.float32)
    ).astype(jnp.bfloat16)

    grad_down = contract_rows(hidden_act, expert_grad).astype(jnp.bfloat16)
    grad_gate = contract_rows(expert_in, grad_gate_pre).astype(jnp.bfloat16)
    grad_up = contract_rows(expert_in, grad_up_pre).astype(jnp.bfloat16)

    by_pair = grad_stream.reshape(tok_rows, half // (2 * out_rows), 2, out_rows)
    even, odd = (by_pair[:, :, 0].reshape(tok_rows, -1), by_pair[:, :, 1].reshape(tok_rows, -1))
    stream_kept = chosen(pair, even, odd)
    stream_met = swapped(chosen(pair, odd, even), "pair")
    shared = lax.all_gather(
        jnp.concatenate([stream_kept, stream_met], axis=0), "tp", axis=1, tiled=True
    )
    shared = shared.reshape(2 * tok_rows, planes, 2, out_rows)
    side_cols = [shared[:, :, s].reshape(2 * tok_rows, planes * out_rows) for s in range(2)]
    near_cols = chosen(side, side_cols[0], side_cols[1])
    far_cols = chosen(side, side_cols[1], side_cols[0])
    act_partial = jnp.dot(near_cols, proj_mine, preferred_element_type=jnp.float32) + jnp.dot(
        far_cols, proj_side, preferred_element_type=jnp.float32
    )
    act_met = swapped(act_partial[tok_rows:].astype(jnp.bfloat16), "pair")
    grad_act = act_partial[:tok_rows] + act_met.astype(jnp.float32)

    whole_stream = lax.all_gather(grad_stream, "tp", axis=1, tiled=True)
    own_columns = lax.all_to_all(
        whole_stream, ("far", "side"), split_axis=1, concat_axis=0, tiled=True
    )
    grad_normed = grad_act * z_sig * (1.0 + scaled_z * (1.0 - z_sig)) * ln_gain[None, :]
    first_sum, second_sum = lax.psum(
        (jnp.sum(grad_normed, axis=1), jnp.sum(grad_normed * normed, axis=1)), "tp"
    )
    grad_conv = (
        inv_std * (grad_normed - first_sum[:, None] / width - normed * second_sum[:, None] / width)
    ).astype(jnp.bfloat16)
    reach_rows = taps.shape[0] - 1
    following = passed_along(grad_conv[:reach_rows], -1)
    extended = jnp.concatenate([grad_conv, following], axis=0).astype(jnp.float32)
    tap_values = taps.astype(jnp.float32)
    grad_input = jnp.zeros((tok_rows, grad_conv.shape[1]), jnp.float32)
    for offset in range(taps.shape[0]):
        grad_input = grad_input + tap_values[offset][None, :] * extended[offset : offset + tok_rows]

    columns = own_columns.reshape(planes, 2, tok_rows, 2 * out_rows)
    near_rows = chosen(side, columns[:, 0], columns[:, 1]).reshape(planes * tok_rows, 2 * out_rows)
    far_rows = chosen(side, columns[:, 1], columns[:, 0]).reshape(planes * tok_rows, 2 * out_rows)
    proj_partial = contract_rows(near_rows, act_mine) + contract_rows(far_rows, act_side)
    first_rows, second_rows = (proj_partial[:out_rows], proj_partial[out_rows:])
    proj_met = swapped(chosen(pair, second_rows, first_rows).astype(jnp.bfloat16), "pair")
    grad_proj = chosen(pair, first_rows, second_rows) + proj_met.astype(jnp.float32)
    return (
        grad_input.astype(jnp.bfloat16),
        grad_proj,
        grad_gate[None],
        grad_up[None],
        grad_down[None],
    )


def solution(mesh):
    places, cores = mesh.devices.shape
    split = Mesh(mesh.devices.reshape(places // 4, 2, 2, cores), (*SP, "tp"))
    return jax.shard_map(
        on_device,
        mesh=split,
        in_specs=(
            P(SP, "tp"),
            P("tp"),
            P(None, "tp"),
            P(SP, "tp"),
            P(SP, "tp"),
            P(SP, "tp"),
            P(SP, None),
            P(SP, None),
            P(SP, None, "tp"),
            P(SP, None, "tp"),
            P(SP, "tp", None),
        ),
        out_specs=(
            P(SP, "tp"),
            P(SP, "tp"),
            P(SP, None, "tp"),
            P(SP, None, "tp"),
            P(SP, "tp", None),
        ),
        check_vma=False,
    )
```

time: 396 us -> 295 us (0.74); the launches traced: 395 us -> 290 us
  waiting for transfers between devices: 255 us -> 96.5 us
  other arithmetic: 5.52 us -> 46 us
  starting transfers between devices: 39.9 us -> 78.5 us
  between operations: 15.8 us -> 2.05 us
  matrix products: 60.3 us -> 48.1 us
    all_to_all x5 -> x1, waiting for transfers between devices: 158 us -> 0.3 us  [on_device(): lax.all_to_all(whole_stream, ('far', 'side'), split_axis=1, concat_axis=0...]
    ppermute x1 -> x31, waiting for transfers between devices: 0.47 us -> 96.2 us  [the longest x15 52.8 us: shifted(): lax.ppermute(value, 'far', [(s, (s + steps) % count) for s in range(count)])]
    all_gather x2 -> x0, waiting for transfers between devices: 76.8 us -> none  [the longest x1 40.9 us: on_device(): lax.all_gather(activated, 'sp', axis=0, tiled=True)]
    ppermute x1 -> x31, starting transfers between devices: 1.55 us -> 62.8 us  [the longest x15 45.6 us: shifted(): lax.ppermute(value, 'far', [(s, (s + steps) % count) for s in range(count)])]
    select_n x0 -> x6, other arithmetic: none -> 30.5 us  [chosen(): return jnp.where(bit == 0, low, high)]
    all_to_all x5 -> x1, starting transfers between devices: 38.1 us -> 15.7 us  [on_device(): lax.all_to_all(whole_stream, ('far', 'side'), split_axis=1, concat_axis=0...]
    reduce_scatter x1 -> x0, waiting for transfers between devices: 19 us -> none  [on_device(): lax.psum_scatter(partial_value.astype(jnp.bfloat16), 'tp', scatter_dimens...]
    convert_element_type x2 -> x7, other arithmetic: 0.29 us -> 5.33 us  [the longest x1 2.45 us: on_device(): (chosen(core, low, high).astype(jnp.float32) + given.astype(jnp.float32))...]
  transfers between devices with their start and end apart: 9 -> 32, of which waited for: 9 -> 13; matrix products, arithmetic and copies ran while one was open for 9% -> 24% of each run, Pallas kernels for 0% -> 0%
where the time goes in v1:
time: 295 us; the launch traced here: 290 us
  waiting for transfers between devices  96.5 us (33%)
  starting transfers between devices  78.5 us (27%)
  matrix products  48.1 us (16%)
  other arithmetic  46 us (16%)
  local copies, waits for them, and re-layouts  9.62 us (3%)
  blocking collectives  9.26 us (3%)
    ppermute x15, waiting for transfers between devices, shifted(): lax.ppermute(value, 'far', [(s, (s + steps) % count) for s in range(count)])  52.8 us
    ppermute x15, starting transfers between devices, shifted(): lax.ppermute(value, 'far', [(s, (s + steps) % count) for s in range(count)])  45.6 us
    ppermute x15, waiting for transfers between devices, swapped(): return lax.ppermute(value, axis, [(0, 1), (1, 0)])  43.4 us
    select_n x6, other arithmetic, chosen(): return jnp.where(bit == 0, low, high)  30.5 us
    dot_general x9, matrix products, contract_rows(): lax.dot_general(left, right, (((0,), (0,)), ((), ())), preferred_element_...  26.3 us
    all_to_all x1, starting transfers between devices, on_device(): lax.all_to_all(whole_stream, ('far', 'side'), split_axis=1, concat_axis=0...  15.7 us
    ppermute x15, starting transfers between devices, swapped(): return lax.ppermute(value, axis, [(0, 1), (1, 0)])  15.6 us
    dot_general x3, matrix products, contract_cols(): lax.dot_general(left, right, (((1,), (1,)), ((), ())), preferred_element_...  11.3 us
  transfers between devices with their start and end apart: 32, of which 13 were waited for; matrix products, arithmetic and copies ran while one was open for 24% of the time, Pallas kernels for 0%

profile of v1, /device:TPU:0, one launch (start us, length us, event | category | flops | bytes accessed | tf_op | source)
XLA Modules:
  0.0 290.1 jit_solution(17253613973534126923)
XLA Ops:
  2.0 3.0 %collective-permute-start = (f32[4,128]{1,0:T(4,128)S(1)}, f32[4,128]{1,0:T(4,128)S(1)}, u32[]{:S(2)}, u32[]{:S(2)}) collective-permute-start(f32[4,128]{1,0:T(4,128)S(1)} %pad_maximum_fusion.13), channel_id=1, source_target_pairs={{0,4},{4,0},{1,5},{5,1},{2,6},{6,2},{3,7},{7,3},{8,12},{12,8},{9,1... | collective-permute-start | bytes 6152 | tf_op jit(solution)/shard_map/ppermute | solution.py:13
  5.1 2.0 collective-permute-start.1
  7.0 0.8 slice_bitcast_fusion.21
  7.8 1.1 fusion.16
  8.9 2.5 all-reduce.1
  11.4 1.2 fusion.27
  13.4 1.3 convolution_convert_fusion.1
  14.6 1.3 fusion.14
  16.3 2.3 collective-permute-done.1
  19.0 2.7 collective-permute-start.3
  21.7 1.4 collective-permute-start.4
  23.1 0.7 collective-permute-start.2
  24.0 11.0 %collective-permute-done.3 = bf16[2,48,1024]{2,1,0:T(8,128)(2,1)S(1)} collective-permute-done((bf16[2,48,1024]{2,1,0:T(8,128)(2,1)S(1)}, bf16[2,48,1024]{2,1,0:T(8,128)(2,1)S(1)}, u32[]{:S(2)}, u32[]{:S(2)}) %collective-permute-start.3) | collective-permute-done | bytes 196640 | tf_op jit(solution)/shard_map/ppermute | solution.py:18
  35.1 1.6 collective-permute-start.6
  36.7 3.8 %collective-permute-start.7 = (bf16[2,48,1024]{2,1,0:T(8,128)(2,1)S(1)}, bf16[2,48,1024]{2,1,0:T(8,128)(2,1)S(1)}, u32[]{:S(2)}, u32[]{:S(2)}) collective-permute-start(bf16[2,48,1024]{2,1,0:T(8,128)(2,1)S(1)} %pad_maximum_fusion.10), channel_id=1, source_target_pairs={{0,8},{8,16},{16,24},{24,0},{1,9},{9,17},{17,25},{25,1},{2,10},{10... | collective-permute-start | bytes 589832 | tf_op jit(solution)/shard_map/ppermute | solution.py:18
  40.4 1.9 collective-permute-start.8
  42.4 3.4 %collective-permute-start.9 = (bf16[2,48,1024]{2,1,0:T(8,128)(2,1)S(1)}, bf16[2,48,1024]{2,1,0:T(8,128)(2,1)S(1)}, u32[]{:S(2)}, u32[]{:S(2)}) collective-permute-start(bf16[2,48,1024]{2,1,0:T(8,128)(2,1)S(1)} %pad_maximum_fusion.12), channel_id=1, source_target_pairs={{0,24},{8,0},{16,8},{24,16},{1,25},{9,1},{17,9},{25,17},{2,26},{10... | collective-permute-start | bytes 589832 | tf_op jit(solution)/shard_map/ppermute | solution.py:18
  45.8 7.5 %collective-permute-done.8 = bf16[2,48,1024]{2,1,0:T(8,128)(2,1)S(1)} collective-permute-done((bf16[2,48,1024]{2,1,0:T(8,128)(2,1)S(1)}, bf16[2,48,1024]{2,1,0:T(8,128)(2,1)S(1)}, u32[]{:S(2)}, u32[]{:S(2)}) %collective-permute-start.8) | collective-permute-done | bytes 196640 | tf_op jit(solution)/shard_map/ppermute | solution.py:18
  53.3 1.3 pad_maximum_fusion.1
  55.3 19.4 %collective-permute-done.10 = bf16[384,1024]{1,0:T(8,128)(2,1)S(1)} collective-permute-done((bf16[384,1024]{1,0:T(8,128)(2,1)S(1)}, bf16[384,1024]{1,0:T(8,128)(2,1)S(1)}, u32[]{:S(2)}, u32[]{:S(2)}) %collective-permute-start.10) | collective-permute-done | bytes 786464 | tf_op jit(solution)/shard_map/ppermute | solution.py:13
  74.9 15.3 %maximum_select_fusion.1 = bf16[768,2048]{1,0:T(8,128)(2,1)S(1)} fusion(bf16[768,1024]{1,0:T(8,128)(2,1)} %collective-permute-done.12, bf16[384,1024]{1,0:T(8,128)(2,1)S(1)} %collective-permute-done.6, bf16[384,1024]{1,0:T(8,128)(2,1)S(1)} %bitcast.200, pred[]{:T(512)S(6)} %eq.113), kind=kLoop, calls=%fused_computation.15 | loop fusion | flops 20447232 | bytes 6291457 | tf_op jit(solution)/shard_map/jit(_where)/select_n | solution.py:28
  90.2 3.4 %fusion.2 = f32[768,896]{1,0:T(8,128)S(1)} fusion(bf16[768,2048]{1,0:T(8,128)(2,1)S(1)} %maximum_select_fusion.1, bf16[1,2048,896]{2,1,0:T(8,128)(2,1)S(1)} %copy-done.41), kind=kOutput, calls=%fused_computation.3 | convolution fusion | flops 2818572288 | bytes 9568256 | tf_op jit(solution)/shard_map/dot_general | solution.py:159
  93.7 3.4 %fusion.6 = f32[768,896]{1,0:T(8,128)S(1)} fusion(bf16[768,2048]{1,0:T(8,128)(2,1)S(1)} %maximum_select_fusion.1, bf16[1,2048,896]{2,1,0:T(8,128)(2,1)S(1)} %copy-done.42), kind=kOutput, calls=%fused_computation.7 | convolution fusion | flops 2818572288 | bytes 9568256 | tf_op jit(solution)/shard_map/dot_general | solution.py:160
  97.2 13.8 %maximum_select_fusion = bf16[768,2048]{1,0:T(8,128)(2,1)S(1)} fusion(bf16[768,1024]{1,0:T(8,128)(2,1)S(1)} %collective-permute-done.11, bf16[384,1024]{1,0:T(8,128)(2,1)S(1)} %collective-permute-done.10, bf16[384,1024]{1,0:T(8,128)(2,1)S(1)} %bitcast.203, pred[]{:T(512)S(6)} %eq.113), kind=kLoop, calls=%fused_computation.14 | loop fusion | flops 20447232 | bytes 6291457 | tf_op jit(solution)/shard_map/jit(_where)/select_n | solution.py:28
  111.0 4.2 %multiply_convert_fusion.1 = (bf16[768,896]{1,0:T(8,128)(2,1)S(1)}, bf16[768,896]{1,0:T(8,128)(2,1)S(1)}) fusion(f32[768,896]{1,0:T(8,128)S(1)} %fusion.2, f32[768,896]{1,0:T(8,128)S(1)} %fusion.6, bf16[768,2048]{1,0:T(8,128)(2,1)S(1)} %maximum_select_fusion, bf16[1,896,2048]{2,1,0:T(8,128)(2,1)S(1)} %copy-done.40), kind=kOutput, calls=%fused_computation.18 | convolution fusion | flops 2827517952 | bytes 15073280 | tf_op jit(solution)/shard_map/dot_general | solution.py:59
  115.2 3.4 %fusion = f32[768,2048]{1,0:T(8,128)S(1)} fusion(bf16[768,896]{1,0:T(8,128)(2,1)S(1)} %get-tuple-element.45, bf16[1,2048,896]{2,1,0:T(8,128)(2,1)S(1)} %copy-done.41), kind=kOutput, calls=%fused_computation.1 | convolution fusion | flops 2818572288 | bytes 11337728 | tf_op jit(solution)/shard_map/dot_general | solution.py:59
  118.7 3.7 %add_convert_fusion = bf16[768,2048]{1,0:T(8,128)(2,1)S(1)} fusion(f32[768,2048]{1,0:T(8,128)S(1)} %fusion, bf16[768,896]{1,0:T(8,128)(2,1)S(1)} %get-tuple-element.44, bf16[1,2048,896]{2,1,0:T(8,128)(2,1)S(1)} %copy-done.42), kind=kOutput, calls=%fused_computation | convolution fusion | flops 2821718016 | bytes 14483456 | tf_op jit(solution)/shard_map/dot_general | solution.py:59
  122.4 1.3 broadcast_select_fusion
  125.5 1.1 broadcast.76.clone
  126.6 1.7 bitcast_dynamic-update-slice_fusion.7
  128.3 6.3 %collective-permute-start.26 = (bf16[128,1024]{1,0:T(8,128)(2,1)S(1)}, bf16[128,1024]{1,0:T(8,128)(2,1)S(1)}, u32[]{:S(2)}, u32[]{:S(2)}) collective-permute-start(bf16[128,1024]{1,0:T(8,128)(2,1)S(1)} %fusion.27), channel_id=1, source_target_pairs={{0,8},{8,16},{16,24},{24,0},{1,9},{9,17},{17,25},{25,1},{2,10},{10... | collective-permute-start | bytes 786440 | tf_op jit(solution)/shard_map/ppermute | solution.py:18
  134.6 1.3 collective-permute-start.20
  135.9 2.5 add_convert_fusion.1
  138.4 1.6 collective-permute-start.14
  140.1 1.3 collective-permute-start.27
  141.4 2.9 collective-permute-start.28
  144.8 5.5 %collective-permute-done.20 = bf16[128,1024]{1,0:T(8,128)(2,1)S(1)} collective-permute-done((bf16[128,1024]{1,0:T(8,128)(2,1)}, bf16[128,1024]{1,0:T(8,128)(2,1)S(1)}, u32[]{:S(2)}, u32[]{:S(2)}) %collective-permute-start.20) | collective-permute-done | bytes 262176 | tf_op jit(solution)/shard_map/ppermute | solution.py:18
  150.3 1.6 collective-permute-start.22
  152.6 9.0 %collective-permute-done.27 = bf16[128,1024]{1,0:T(8,128)(2,1)S(1)} collective-permute-done((bf16[128,1024]{1,0:T(8,128)(2,1)S(1)}, bf16[128,1024]{1,0:T(8,128)(2,1)S(1)}, u32[]{:S(2)}, u32[]{:S(2)}) %collective-permute-start.27) | collective-permute-done | bytes 262176 | tf_op jit(solution)/shard_map/ppermute | solution.py:18
  162.0 17.5 %collective-permute-start.15 = (bf16[2,48,1024]{2,1,0:T(8,128)(2,1)S(1)}, bf16[2,48,1024]{2,1,0:T(8,128)(2,1)S(1)}, u32[]{:S(2)}, u32[]{:S(2)}) collective-permute-start(bf16[2,48,1024]{2,1,0:T(8,128)(2,1)S(1)} %bitcast.228), channel_id=1, source_target_pairs={{0,24},{8,0},{16,8},{24,16},{1,25},{9,1},{17,9},{25,17},{2,26},{10... | collective-permute-start | bytes 589832 | tf_op jit(solution)/shard_map/ppermute | solution.py:18
  179.6 0.9 collective-permute-start.17
  180.5 4.4 %collective-permute-done.15 = bf16[2,48,1024]{2,1,0:T(8,128)(2,1)S(1)} collective-permute-done((bf16[2,48,1024]{2,1,0:T(8,128)(2,1)S(1)}, bf16[2,48,1024]{2,1,0:T(8,128)(2,1)S(1)}, u32[]{:S(2)}, u32[]{:S(2)}) %collective-permute-start.15) | collective-permute-done | bytes 196640 | tf_op jit(solution)/shard_map/ppermute | solution.py:18
  185.4 14.8 %collective-permute-done.16 = bf16[2,48,1024]{2,1,0:T(8,128)(2,1)S(1)} collective-permute-done((bf16[2,48,1024]{2,1,0:T(8,128)(2,1)S(1)}, bf16[2,48,1024]{2,1,0:T(8,128)(2,1)S(1)}, u32[]{:S(2)}, u32[]{:S(2)}) %collective-permute-start.16) | collective-permute-done | bytes 196640 | tf_op jit(solution)/shard_map/ppermute | solution.py:18
  201.4 0.7 bitcast_dynamic-update-slice_fusion.5
  202.8 1.5 collective-permute-start.23
  204.3 12.2 %collective-permute-done.18 = bf16[128,1024]{1,0:T(8,128)(2,1)S(1)} collective-permute-done((bf16[128,1024]{1,0:T(8,128)(2,1)S(1)}, bf16[128,1024]{1,0:T(8,128)(2,1)S(1)}, u32[]{:S(2)}, u32[]{:S(2)}) %collective-permute-start.18) | collective-permute-done | bytes 262176 | tf_op jit(solution)/shard_map/ppermute | solution.py:13
  218.5 8.5 %convert_bitcast_fusion = bf16[1,896,2048]{2,1,0:T(8,128)(2,1)} fusion(bf16[768,2048]{1,0:T(8,128)(2,1)} %copy-done.3, f32[768,896]{1,0:T(8,128)} %copy-done.45, f32[768,896]{1,0:T(8,128)} %copy-done.44), kind=kOutput, calls=%fused_computation.11 | convolution fusion | flops 2824536064 | bytes 12320768 | tf_op jit(solution)/shard_map/dot_general | solution.py:53
  227.0 2.2 all_gather.6
  229.2 6.1 %collective-permute-done.23 = bf16[512,1024]{1,0:T(8,128)(2,1)S(1)} collective-permute-done((bf16[512,1024]{1,0:T(8,128)(2,1)}, bf16[512,1024]{1,0:T(8,128)(2,1)S(1)}, u32[]{:S(2)}, u32[]{:S(2)}) %collective-permute-start.23) | collective-permute-done | bytes 1048608 | tf_op jit(solution)/shard_map/ppermute | solution.py:13
  235.8 1.9 convolution_add_fusion
  238.4 4.9 %convert_bitcast_fusion.1 = bf16[1,2048,896]{2,1,0:T(8,128)(2,1)} fusion(bf16[768,2048]{1,0:T(8,128)(2,1)S(1)} %copy-done.2, bf16[768,896]{1,0:T(8,128)(2,1)S(1)} %copy-done.47), kind=kOutput, calls=%fused_computation.12 | convolution fusion | flops 2820407296 | bytes 8192000 | tf_op jit(solution)/shard_map/dot_general | solution.py:53
  243.3 2.2 all_gather.7
  245.4 0.9 copy.29
  246.3 15.7 %all-to-all-start = ((bf16[128,8,256]{2,0,1:T(8,128)(2,1)}), bf16[128,8,256]{2,0,1:T(8,128)(2,1)S(1)}, u32[]{:S(2)}, u32[]{:S(2)}) async-start(bf16[128,8,256]{2,0,1:T(8,128)(2,1)} %bitcast.207), calls=%async_computation | async-start | bytes 1048576 | tf_op jit(solution)/shard_map/all_to_all | solution.py:219
  262.1 2.2 fusion.93
  264.2 2.4 all-reduce
  266.7 1.3 fusion.35
  268.0 1.6 collective-permute-start.25
  269.6 7.6 %convert_bitcast_fusion.2 = bf16[1,2048,896]{2,1,0:T(8,128)(2,1)} fusion(bf16[768,2048]{1,0:T(8,128)(2,1)} %copy-done.1, bf16[768,896]{1,0:T(8,128)(2,1)} %copy-done.43), kind=kOutput, calls=%fused_computation.13 | convolution fusion | flops 2820407296 | bytes 8192000 | tf_op jit(solution)/shard_map/dot_general | solution.py:53
  277.9 1.7 fusion.101
  280.1 2.4 collective-permute-start.30
  282.8 2.7 fusion.37
  285.5 3.4 %collective-permute-done.30 = bf16[128,1024]{1,0:T(8,128)(2,1)S(1)} collective-permute-done((bf16[128,1024]{1,0:T(8,128)(2,1)S(1)}, bf16[128,1024]{1,0:T(8,128)(2,1)S(1)}, u32[]{:S(2)}, u32[]{:S(2)}) %collective-permute-start.30) | collective-permute-done | bytes 262176 | tf_op jit(solution)/shard_map/ppermute | solution.py:13
  288.9 0.9 convert_add_fusion
  (186 shorter events, 14.3 us)
Async XLA Ops:
  2.0 10.8 %collective-permute-start = (f32[4,128]{1,0:T(4,128)S(1)}, f32[4,128]{1,0:T(4,128)S(1)}, u32[]{:S(2)}, u32[]{:S(2)}) collective-permute-start(f32[4,128]{1,0:T(4,128)S(1)} %pad_maximum_fusion.13), channel_id=1, source_target_pairs={{0,4},{4,0},{1,5},{5,1},{2,6},{6,2},{3,7},{7,3},{8,12},{12,8},{9,1... | collective-permute-start | bytes 6152 | tf_op jit(solution)/shard_map/ppermute | solution.py:13
  5.0 11.0 %collective-permute-start.5 = (bf16[128,1024]{1,0:T(8,128)(2,1)}, bf16[128,1024]{1,0:T(8,128)(2,1)S(1)}, u32[]{:S(2)}, u32[]{:S(2)}) collective-permute-start(bf16[128,1024]{1,0:T(8,128)(2,1)} %param.16), channel_id=1, source_target_pairs={{0,4},{4,0},{1,5},{5,1},{2,6},{6,2},{3,7},{7,3},{8,12},{12,8},{9,1... | collective-permute-start | bytes 786440 | tf_op jit(solution)/shard_map/ppermute | solution.py:13
  5.1 13.5 %collective-permute-start.1 = (bf16[128,1024]{1,0:T(8,128)(2,1)}, bf16[128,1024]{1,0:T(8,128)(2,1)S(1)}, u32[]{:S(2)}, u32[]{:S(2)}) collective-permute-start(bf16[128,1024]{1,0:T(8,128)(2,1)} %param.15), channel_id=1, source_target_pairs={{0,4},{4,0},{1,5},{5,1},{2,6},{6,2},{3,7},{7,3},{8,12},{12,8},{9,1... | collective-permute-start | bytes 786440 | tf_op jit(solution)/shard_map/ppermute | solution.py:13
  11.4 7.5 %copy-start.36 = (f32[128]{0:T(128)}, f32[128]{0:T(128)S(1)}, u32[]{:S(2)}) copy-start(f32[128]{0:T(128)S(1)} %get-tuple-element.113) | copy-start | bytes 1540
  11.4 7.5 %copy-start.38 = (f32[128]{0:T(128)}, f32[128]{0:T(128)S(1)}, u32[]{:S(2)}) copy-start(f32[128]{0:T(128)S(1)} %get-tuple-element.114) | copy-start | bytes 1540
  19.0 16.0 %collective-permute-start.3 = (bf16[2,48,1024]{2,1,0:T(8,128)(2,1)S(1)}, bf16[2,48,1024]{2,1,0:T(8,128)(2,1)S(1)}, u32[]{:S(2)}, u32[]{:S(2)}) collective-permute-start(bf16[2,48,1024]{2,1,0:T(8,128)(2,1)S(1)} %pad_maximum_fusion.7), channel_id=1, source_target_pairs={{0,16},{8,24},{16,0},{24,8},{1,17},{9,25},{17,1},{25,9},{2,18},{10... | collective-permute-start | bytes 589832 | tf_op jit(solution)/shard_map/ppermute | solution.py:18
  21.7 13.3 %collective-permute-start.4 = (bf16[2,48,1024]{2,1,0:T(8,128)(2,1)S(1)}, bf16[2,48,1024]{2,1,0:T(8,128)(2,1)S(1)}, u32[]{:S(2)}, u32[]{:S(2)}) collective-permute-start(bf16[2,48,1024]{2,1,0:T(8,128)(2,1)S(1)} %pad_maximum_fusion.8), channel_id=1, source_target_pairs={{0,24},{8,0},{16,8},{24,16},{1,25},{9,1},{17,9},{25,17},{2,26},{10... | collective-permute-start | bytes 589832 | tf_op jit(solution)/shard_map/ppermute | solution.py:18
  23.1 11.9 %collective-permute-start.2 = (bf16[2,48,1024]{2,1,0:T(8,128)(2,1)S(1)}, bf16[2,48,1024]{2,1,0:T(8,128)(2,1)S(1)}, u32[]{:S(2)}, u32[]{:S(2)}) collective-permute-start(bf16[2,48,1024]{2,1,0:T(8,128)(2,1)S(1)} %pad_maximum_fusion.6), channel_id=1, source_target_pairs={{0,8},{8,16},{16,24},{24,0},{1,9},{9,17},{17,25},{25,1},{2,10},{10... | collective-permute-start | bytes 589832 | tf_op jit(solution)/shard_map/ppermute | solution.py:18
  35.1 18.2 %collective-permute-start.6 = (bf16[384,1024]{1,0:T(8,128)(2,1)S(1)}, bf16[384,1024]{1,0:T(8,128)(2,1)S(1)}, u32[]{:S(2)}, u32[]{:S(2)}) collective-permute-start(bf16[384,1024]{1,0:T(8,128)(2,1)S(1)} %bitcast.198), channel_id=1, source_target_pairs={{0,2},{2,0},{1,3},{3,1},{4,6},{6,4},{5,7},{7,5},{8,10},{10,8},{9,1... | collective-permute-start | bytes 2359304 | tf_op jit(solution)/shard_map/ppermute | solution.py:13
  36.7 9.1 %collective-permute-start.7 = (bf16[2,48,1024]{2,1,0:T(8,128)(2,1)S(1)}, bf16[2,48,1024]{2,1,0:T(8,128)(2,1)S(1)}, u32[]{:S(2)}, u32[]{:S(2)}) collective-permute-start(bf16[2,48,1024]{2,1,0:T(8,128)(2,1)S(1)} %pad_maximum_fusion.10), channel_id=1, source_target_pairs={{0,8},{8,16},{16,24},{24,0},{1,9},{9,17},{17,25},{25,1},{2,10},{10... | collective-permute-start | bytes 589832 | tf_op jit(solution)/shard_map/ppermute | solution.py:18
  40.4 12.9 %collective-permute-start.8 = (bf16[2,48,1024]{2,1,0:T(8,128)(2,1)S(1)}, bf16[2,48,1024]{2,1,0:T(8,128)(2,1)S(1)}, u32[]{:S(2)}, u32[]{:S(2)}) collective-permute-start(bf16[2,48,1024]{2,1,0:T(8,128)(2,1)S(1)} %pad_maximum_fusion.11), channel_id=1, source_target_pairs={{0,16},{8,24},{16,0},{24,8},{1,17},{9,25},{17,1},{25,9},{2,18},{10... | collective-permute-start | bytes 589832 | tf_op jit(solution)/shard_map/ppermute | solution.py:18
  42.4 11.0 %collective-permute-start.9 = (bf16[2,48,1024]{2,1,0:T(8,128)(2,1)S(1)}, bf16[2,48,1024]{2,1,0:T(8,128)(2,1)S(1)}, u32[]{:S(2)}, u32[]{:S(2)}) collective-permute-start(bf16[2,48,1024]{2,1,0:T(8,128)(2,1)S(1)} %pad_maximum_fusion.12), channel_id=1, source_target_pairs={{0,24},{8,0},{16,8},{24,16},{1,25},{9,1},{17,9},{25,17},{2,26},{10... | collective-permute-start | bytes 589832 | tf_op jit(solution)/shard_map/ppermute | solution.py:18
  54.6 20.3 %collective-permute-start.12 = (bf16[768,1024]{1,0:T(8,128)(2,1)}, bf16[768,1024]{1,0:T(8,128)(2,1)}, u32[]{:S(2)}, u32[]{:S(2)}) collective-permute-start(bf16[768,1024]{1,0:T(8,128)(2,1)} %pad_maximum_fusion.1), channel_id=1, source_target_pairs={{0,1},{1,0},{2,3},{3,2},{4,5},{5,4},{6,7},{7,6},{8,9},{9,8},{10,11... | collective-permute-start | bytes 4718600 | tf_op jit(solution)/shard_map/ppermute | solution.py:13
  54.7 20.0 %collective-permute-start.10 = (bf16[384,1024]{1,0:T(8,128)(2,1)S(1)}, bf16[384,1024]{1,0:T(8,128)(2,1)S(1)}, u32[]{:S(2)}, u32[]{:S(2)}) collective-permute-start(bf16[384,1024]{1,0:T(8,128)(2,1)S(1)} %bitcast.201), channel_id=1, source_target_pairs={{0,2},{2,0},{1,3},{3,1},{4,6},{6,4},{5,7},{7,5},{8,10},{10,8},{9,1... | collective-permute-start | bytes 2359304 | tf_op jit(solution)/shard_map/ppermute | solution.py:13
  74.8 15.4 %copy-start.41 = (bf16[1,2048,896]{2,1,0:T(8,128)(2,1)S(1)}, bf16[1,2048,896]{2,1,0:T(8,128)(2,1)}, u32[]{:S(2)}) copy-start(bf16[1,2048,896]{2,1,0:T(8,128)(2,1)} %param.19) | copy-start | bytes 11010052
  74.8 22.3 %collective-permute-start.11 = (bf16[768,1024]{1,0:T(8,128)(2,1)S(1)}, bf16[768,1024]{1,0:T(8,128)(2,1)S(1)}, u32[]{:S(2)}, u32[]{:S(2)}) collective-permute-start(bf16[768,1024]{1,0:T(8,128)(2,1)S(1)} %pad_maximum_fusion), channel_id=1, source_target_pairs={{0,1},{1,0},{2,3},{3,2},{4,5},{5,4},{6,7},{7,6},{8,9},{9,8},{10,11... | collective-permute-start | bytes 4718600 | tf_op jit(solution)/shard_map/ppermute | solution.py:13
  93.7 17.3 %copy-start.44 = (f32[768,896]{1,0:T(8,128)}, f32[768,896]{1,0:T(8,128)S(1)}, u32[]{:S(2)}) copy-start(f32[768,896]{1,0:T(8,128)S(1)} %fusion.2) | copy-start | bytes 8257540
  97.1 13.9 %copy-start.45 = (f32[768,896]{1,0:T(8,128)}, f32[768,896]{1,0:T(8,128)S(1)}, u32[]{:S(2)}) copy-start(f32[768,896]{1,0:T(8,128)S(1)} %fusion.6) | copy-start | bytes 8257540
  97.2 13.9 %copy-start.40 = (bf16[1,896,2048]{2,1,0:T(8,128)(2,1)S(1)}, bf16[1,896,2048]{2,1,0:T(8,128)(2,1)}, u32[]{:S(2)}) copy-start(bf16[1,896,2048]{2,1,0:T(8,128)(2,1)} %param.21) | copy-start | bytes 11010052
  123.7 12.2 %collective-permute-start.13 = (bf16[768,1024]{1,0:T(8,128)(2,1)}, bf16[768,1024]{1,0:T(8,128)(2,1)}, u32[]{:S(2)}, u32[]{:S(2)}) collective-permute-start(bf16[768,1024]{1,0:T(8,128)(2,1)} %broadcast_select_fusion), channel_id=1, source_target_pairs={{0,1},{1,0},{2,3},{3,2},{4,5},{5,4},{6,7},{7,6},{8,9},{9,8},{10,11... | collective-permute-start | bytes 4718600 | tf_op jit(solution)/shard_map/ppermute | solution.py:13
  128.3 16.5 %collective-permute-start.26 = (bf16[128,1024]{1,0:T(8,128)(2,1)S(1)}, bf16[128,1024]{1,0:T(8,128)(2,1)S(1)}, u32[]{:S(2)}, u32[]{:S(2)}) collective-permute-start(bf16[128,1024]{1,0:T(8,128)(2,1)S(1)} %fusion.27), channel_id=1, source_target_pairs={{0,8},{8,16},{16,24},{24,0},{1,9},{9,17},{17,25},{25,1},{2,10},{10... | collective-permute-start | bytes 786440 | tf_op jit(solution)/shard_map/ppermute | solution.py:18
  134.6 15.8 %collective-permute-start.20 = (bf16[128,1024]{1,0:T(8,128)(2,1)}, bf16[128,1024]{1,0:T(8,128)(2,1)S(1)}, u32[]{:S(2)}, u32[]{:S(2)}) collective-permute-start(bf16[128,1024]{1,0:T(8,128)(2,1)} %param.14), channel_id=1, source_target_pairs={{0,8},{8,16},{16,24},{24,0},{1,9},{9,17},{17,25},{25,1},{2,10},{10... | collective-permute-start | bytes 786440 | tf_op jit(solution)/shard_map/ppermute | solution.py:18
  138.3 6.4 %copy-start.5 = (bf16[128,1024]{1,0:T(8,128)(2,1)S(1)}, bf16[128,1024]{1,0:T(8,128)(2,1)}, u32[]{:S(2)}) copy-start(bf16[128,1024]{1,0:T(8,128)(2,1)} %param.14) | copy-start | bytes 786436
  138.4 23.2 %collective-permute-start.14 = (bf16[384,1024]{1,0:T(8,128)(2,1)S(1)}, bf16[384,1024]{1,0:T(8,128)(2,1)S(1)}, u32[]{:S(2)}, u32[]{:S(2)}) collective-permute-start(bf16[384,1024]{1,0:T(8,128)(2,1)S(1)} %slice.528), channel_id=1, source_target_pairs={{0,2},{2,0},{1,3},{3,1},{4,6},{6,4},{5,7},{7,5},{8,10},{10,8},{9,1... | collective-permute-start | bytes 2359304 | tf_op jit(solution)/shard_map/ppermute | solution.py:13
  140.1 21.5 %collective-permute-start.27 = (bf16[128,1024]{1,0:T(8,128)(2,1)S(1)}, bf16[128,1024]{1,0:T(8,128)(2,1)S(1)}, u32[]{:S(2)}, u32[]{:S(2)}) collective-permute-start(bf16[128,1024]{1,0:T(8,128)(2,1)S(1)} %fusion.27), channel_id=1, source_target_pairs={{0,16},{8,24},{16,0},{24,8},{1,17},{9,25},{17,1},{25,9},{2,18},{10... | collective-permute-start | bytes 786440 | tf_op jit(solution)/shard_map/ppermute | solution.py:18
  141.4 38.2 %collective-permute-start.28 = (bf16[128,1024]{1,0:T(8,128)(2,1)S(1)}, bf16[128,1024]{1,0:T(8,128)(2,1)S(1)}, u32[]{:S(2)}, u32[]{:S(2)}) collective-permute-start(bf16[128,1024]{1,0:T(8,128)(2,1)S(1)} %fusion.27), channel_id=1, source_target_pairs={{0,24},{8,0},{16,8},{24,16},{1,25},{9,1},{17,9},{25,17},{2,26},{10... | collective-permute-start | bytes 786440 | tf_op jit(solution)/shard_map/ppermute | solution.py:18
  144.8 56.6 %collective-permute-start.21 = (bf16[128,1024]{1,0:T(8,128)(2,1)S(1)}, bf16[128,1024]{1,0:T(8,128)(2,1)S(1)}, u32[]{:S(2)}, u32[]{:S(2)}) collective-permute-start(bf16[128,1024]{1,0:T(8,128)(2,1)S(1)} %copy-done.5), channel_id=1, source_target_pairs={{0,16},{8,24},{16,0},{24,8},{1,17},{9,25},{17,1},{25,9},{2,18},{10... | collective-permute-start | bytes 786440 | tf_op jit(solution)/shard_map/ppermute | solution.py:18
  150.3 51.8 %collective-permute-start.22 = (bf16[128,1024]{1,0:T(8,128)(2,1)S(1)}, bf16[128,1024]{1,0:T(8,128)(2,1)S(1)}, u32[]{:S(2)}, u32[]{:S(2)}) collective-permute-start(bf16[128,1024]{1,0:T(8,128)(2,1)S(1)} %copy-done.5), channel_id=1, source_target_pairs={{0,24},{8,0},{16,8},{24,16},{1,25},{9,1},{17,9},{25,17},{2,26},{10... | collective-permute-start | bytes 786440 | tf_op jit(solution)/shard_map/ppermute | solution.py:18
  162.0 54.6 %copy-start.4 = (bf16[128,1024]{1,0:T(8,128)(2,1)S(1)}, bf16[128,1024]{1,0:T(8,128)(2,1)}, u32[]{:S(2)}) copy-start(bf16[128,1024]{1,0:T(8,128)(2,1)} %param.16) | copy-start | bytes 786436
  162.0 22.8 %collective-permute-start.15 = (bf16[2,48,1024]{2,1,0:T(8,128)(2,1)S(1)}, bf16[2,48,1024]{2,1,0:T(8,128)(2,1)S(1)}, u32[]{:S(2)}, u32[]{:S(2)}) collective-permute-start(bf16[2,48,1024]{2,1,0:T(8,128)(2,1)S(1)} %bitcast.228), channel_id=1, source_target_pairs={{0,24},{8,0},{16,8},{24,16},{1,25},{9,1},{17,9},{25,17},{2,26},{10... | collective-permute-start | bytes 589832 | tf_op jit(solution)/shard_map/ppermute | solution.py:18
  179.6 20.7 %collective-permute-start.16 = (bf16[2,48,1024]{2,1,0:T(8,128)(2,1)S(1)}, bf16[2,48,1024]{2,1,0:T(8,128)(2,1)S(1)}, u32[]{:S(2)}, u32[]{:S(2)}) collective-permute-start(bf16[2,48,1024]{2,1,0:T(8,128)(2,1)S(1)} %bitcast.223), channel_id=1, source_target_pairs={{0,16},{8,24},{16,0},{24,8},{1,17},{9,25},{17,1},{25,9},{2,18},{10... | collective-permute-start | bytes 589832 | tf_op jit(solution)/shard_map/ppermute | solution.py:18
  179.6 20.7 %collective-permute-start.17 = (bf16[2,48,1024]{2,1,0:T(8,128)(2,1)S(1)}, bf16[2,48,1024]{2,1,0:T(8,128)(2,1)S(1)}, u32[]{:S(2)}, u32[]{:S(2)}) collective-permute-start(bf16[2,48,1024]{2,1,0:T(8,128)(2,1)S(1)} %bitcast.221), channel_id=1, source_target_pairs={{0,8},{8,16},{16,24},{24,0},{1,9},{9,17},{17,25},{25,1},{2,10},{10... | collective-permute-start | bytes 589832 | tf_op jit(solution)/shard_map/ppermute | solution.py:18
  184.9 92.7 %collective-permute-start.29 = (bf16[512,1024]{1,0:T(8,128)(2,1)S(1)}, bf16[512,1024]{1,0:T(8,128)(2,1)}, u32[]{:S(2)}, u32[]{:S(2)}) collective-permute-start(bf16[512,1024]{1,0:T(8,128)(2,1)S(1)} %bitcast.204), channel_id=1, source_target_pairs={{0,4},{4,0},{1,5},{5,1},{2,6},{6,2},{3,7},{7,3},{8,12},{12,8},{9,1... | collective-permute-start | bytes 3145736 | tf_op jit(solution)/shard_map/ppermute | solution.py:13
  200.8 15.8 %collective-permute-start.18 = (bf16[128,1024]{1,0:T(8,128)(2,1)S(1)}, bf16[128,1024]{1,0:T(8,128)(2,1)S(1)}, u32[]{:S(2)}, u32[]{:S(2)}) collective-permute-start(bf16[128,1024]{1,0:T(8,128)(2,1)S(1)} %convolution_convert_fusion.2), channel_id=1, source_target_pairs={{0,4},{4,0},{1,5},{5,1},{2,6},{6,2},{3,7},{7,3},{8,12},{12,8},{9,1... | collective-permute-start | bytes 786440 | tf_op jit(solution)/shard_map/ppermute | solution.py:13
  202.8 32.5 %collective-permute-start.23 = (bf16[512,1024]{1,0:T(8,128)(2,1)}, bf16[512,1024]{1,0:T(8,128)(2,1)S(1)}, u32[]{:S(2)}, u32[]{:S(2)}) collective-permute-start(bf16[512,1024]{1,0:T(8,128)(2,1)} %bitcast.57), channel_id=1, source_target_pairs={{0,4},{4,0},{1,5},{5,1},{2,6},{6,2},{3,7},{7,3},{8,12},{12,8},{9,1... | collective-permute-start | bytes 3145736 | tf_op jit(solution)/shard_map/ppermute | solution.py:13
  217.8 9.2 %collective-permute-start.19 = (bf16[128,512]{0,1:T(8,128)(2,1)S(1)}, bf16[128,512]{0,1:T(8,128)(2,1)S(1)}, u32[]{:S(2)}, u32[]{:S(2)}) collective-permute-start(bf16[128,512]{0,1:T(8,128)(2,1)S(1)} %bitcast.230), channel_id=1, source_target_pairs={{0,2},{2,0},{1,3},{3,1},{4,6},{6,4},{5,7},{7,5},{8,10},{10,8},{9,1... | collective-permute-start | bytes 393224 | tf_op jit(solution)/shard_map/ppermute | solution.py:13
  237.7 24.3 %copy-start = (bf16[128,1024]{1,0:T(8,128)(2,1)S(1)}, bf16[128,1024]{1,0:T(8,128)(2,1)}, u32[]{:S(2)}) copy-start(bf16[128,1024]{1,0:T(8,128)(2,1)} %param.11) | copy-start | bytes 786436
  237.7 24.3 %copy-start.7 = (f32[1024]{0:T(1024)S(1)}, f32[1024]{0:T(1024)}, u32[]{:S(2)}) copy-start(f32[1024]{0:T(1024)} %param.12) | copy-start | bytes 12292
  237.8 24.3 %collective-permute-start.24 = (bf16[128,1024]{1,0:T(8,128)(2,1)S(1)}, bf16[128,1024]{1,0:T(8,128)(2,1)}, u32[]{:S(2)}, u32[]{:S(2)}) collective-permute-start(bf16[128,1024]{1,0:T(8,128)(2,1)S(1)} %slice.819), channel_id=1, source_target_pairs={{0,2},{2,0},{1,3},{3,1},{4,6},{6,4},{5,7},{7,5},{8,10},{10,8},{9,1... | collective-permute-start | bytes 786440 | tf_op jit(solution)/shard_map/ppermute | solution.py:13
  245.4 21.2 %copy-start.37 = (f32[128]{0:T(128)S(1)}, f32[128]{0:T(128)}, u32[]{:S(2)}) copy-start(f32[128]{0:T(128)} %copy-done.36) | copy-start | bytes 1540
  245.4 21.2 %copy-start.39 = (f32[128]{0:T(128)S(1)}, f32[128]{0:T(128)}, u32[]{:S(2)}) copy-start(f32[128]{0:T(128)} %copy-done.38) | copy-start | bytes 1540
  246.3 31.2 %all-to-all-start = ((bf16[128,8,256]{2,0,1:T(8,128)(2,1)}), bf16[128,8,256]{2,0,1:T(8,128)(2,1)S(1)}, u32[]{:S(2)}, u32[]{:S(2)}) async-start(bf16[128,8,256]{2,0,1:T(8,128)(2,1)} %bitcast.207), calls=%async_computation | async-start | bytes 1048576 | tf_op jit(solution)/shard_map/all_to_all | solution.py:219
  268.0 9.2 %collective-permute-start.25 = (bf16[30,1024]{1,0:T(8,128)(2,1)S(1)}, bf16[30,1024]{1,0:T(8,128)(2,1)S(1)}, u32[]{:S(2)}, u32[]{:S(2)}) collective-permute-start(bf16[30,1024]{1,0:T(8,128)(2,1)S(1)} %slice.541), channel_id=1, source_target_pairs={{2,0},{4,2},{6,4},{8,6},{10,8},{12,10},{14,12},{16,14},{18,16},{20... | collective-permute-start | bytes 184328 | tf_op jit(solution)/shard_map/ppermute | solution.py:24
  277.6 4.9 %copy-start.8 = (f32[1,1024]{1,0:T(1,128)S(1)}, f32[1,1024]{1,0:T(1,128)}, u32[]{:S(2)}) copy-start(f32[1,1024]{1,0:T(1,128)} %get-tuple-element.96) | copy-start | bytes 12292
  277.6 4.9 %copy-start.9 = (f32[1,1024]{1,0:T(1,128)S(1)}, f32[1,1024]{1,0:T(1,128)}, u32[]{:S(2)}) copy-start(f32[1,1024]{1,0:T(1,128)} %get-tuple-element.97) | copy-start | bytes 12292
  277.6 4.9 %copy-start.10 = (f32[1,1024]{1,0:T(1,128)S(1)}, f32[1,1024]{1,0:T(1,128)}, u32[]{:S(2)}) copy-start(f32[1,1024]{1,0:T(1,128)} %get-tuple-element.98) | copy-start | bytes 12292
  277.6 4.9 %copy-start.11 = (f32[1,1024]{1,0:T(1,128)S(1)}, f32[1,1024]{1,0:T(1,128)}, u32[]{:S(2)}) copy-start(f32[1,1024]{1,0:T(1,128)} %get-tuple-element.99) | copy-start | bytes 12292
  277.6 4.9 %copy-start.12 = (f32[1,1024]{1,0:T(1,128)S(1)}, f32[1,1024]{1,0:T(1,128)}, u32[]{:S(2)}) copy-start(f32[1,1024]{1,0:T(1,128)} %get-tuple-element.100) | copy-start | bytes 12292
  277.6 4.9 %copy-start.13 = (f32[1,1024]{1,0:T(1,128)S(1)}, f32[1,1024]{1,0:T(1,128)}, u32[]{:S(2)}) copy-start(f32[1,1024]{1,0:T(1,128)} %get-tuple-element.101) | copy-start | bytes 12292
  277.7 4.9 %copy-start.14 = (f32[1,1024]{1,0:T(1,128)S(1)}, f32[1,1024]{1,0:T(1,128)}, u32[]{:S(2)}) copy-start(f32[1,1024]{1,0:T(1,128)} %get-tuple-element.102) | copy-start | bytes 12292
  277.7 4.9 %copy-start.15 = (f32[1,1024]{1,0:T(1,128)S(1)}, f32[1,1024]{1,0:T(1,128)}, u32[]{:S(2)}) copy-start(f32[1,1024]{1,0:T(1,128)} %get-tuple-element.103) | copy-start | bytes 12292
  277.7 4.9 %copy-start.16 = (f32[1,1024]{1,0:T(1,128)S(1)}, f32[1,1024]{1,0:T(1,128)}, u32[]{:S(2)}) copy-start(f32[1,1024]{1,0:T(1,128)} %get-tuple-element.104) | copy-start | bytes 12292
  277.7 4.9 %copy-start.17 = (f32[1,1024]{1,0:T(1,128)S(1)}, f32[1,1024]{1,0:T(1,128)}, u32[]{:S(2)}) copy-start(f32[1,1024]{1,0:T(1,128)} %get-tuple-element.74) | copy-start | bytes 12292
  277.7 4.9 %copy-start.18 = (f32[1,1024]{1,0:T(1,128)S(1)}, f32[1,1024]{1,0:T(1,128)}, u32[]{:S(2)}) copy-start(f32[1,1024]{1,0:T(1,128)} %get-tuple-element.75) | copy-start | bytes 12292
  277.7 4.9 %copy-start.19 = (f32[1,1024]{1,0:T(1,128)S(1)}, f32[1,1024]{1,0:T(1,128)}, u32[]{:S(2)}) copy-start(f32[1,1024]{1,0:T(1,128)} %get-tuple-element.76) | copy-start | bytes 12292
  277.7 4.9 %copy-start.20 = (f32[1,1024]{1,0:T(1,128)S(1)}, f32[1,1024]{1,0:T(1,128)}, u32[]{:S(2)}) copy-start(f32[1,1024]{1,0:T(1,128)} %get-tuple-element.77) | copy-start | bytes 12292
  277.7 4.9 %copy-start.21 = (f32[1,1024]{1,0:T(1,128)S(1)}, f32[1,1024]{1,0:T(1,128)}, u32[]{:S(2)}) copy-start(f32[1,1024]{1,0:T(1,128)} %get-tuple-element.78) | copy-start | bytes 12292
  277.7 4.9 %copy-start.22 = (f32[1,1024]{1,0:T(1,128)S(1)}, f32[1,1024]{1,0:T(1,128)}, u32[]{:S(2)}) copy-start(f32[1,1024]{1,0:T(1,128)} %get-tuple-element.79) | copy-start | bytes 12292
  277.7 4.9 %copy-start.23 = (f32[1,1024]{1,0:T(1,128)S(1)}, f32[1,1024]{1,0:T(1,128)}, u32[]{:S(2)}) copy-start(f32[1,1024]{1,0:T(1,128)} %get-tuple-element.80) | copy-start | bytes 12292
  277.8 4.9 %copy-start.24 = (f32[1,1024]{1,0:T(1,128)S(1)}, f32[1,1024]{1,0:T(1,128)}, u32[]{:S(2)}) copy-start(f32[1,1024]{1,0:T(1,128)} %get-tuple-element.81) | copy-start | bytes 12292
  277.8 4.9 %copy-start.25 = (f32[1,1024]{1,0:T(1,128)S(1)}, f32[1,1024]{1,0:T(1,128)}, u32[]{:S(2)}) copy-start(f32[1,1024]{1,0:T(1,128)} %get-tuple-element.82) | copy-start | bytes 12292
  277.8 4.9 %copy-start.26 = (f32[1,1024]{1,0:T(1,128)S(1)}, f32[1,1024]{1,0:T(1,128)}, u32[]{:S(2)}) copy-start(f32[1,1024]{1,0:T(1,128)} %get-tuple-element.83) | copy-start | bytes 12292
  277.8 4.9 %copy-start.27 = (f32[1,1024]{1,0:T(1,128)S(1)}, f32[1,1024]{1,0:T(1,128)}, u32[]{:S(2)}) copy-start(f32[1,1024]{1,0:T(1,128)} %get-tuple-element.84) | copy-start | bytes 12292
  280.1 8.8 %collective-permute-start.30 = (bf16[128,1024]{1,0:T(8,128)(2,1)S(1)}, bf16[128,1024]{1,0:T(8,128)(2,1)S(1)}, u32[]{:S(2)}, u32[]{:S(2)}) collective-permute-start(bf16[128,1024]{1,0:T(8,128)(2,1)S(1)} %select_convert_fusion), channel_id=1, source_target_pairs={{0,2},{2,0},{1,3},{3,1},{4,6},{6,4},{5,7},{7,5},{8,10},{10,8},{9,1... | collective-permute-start | bytes 786440 | tf_op jit(solution)/shard_map/ppermute | solution.py:13
  (16 other events, 65.2 us)

commit v2 on v1

v2 whole, which is shorter than its diff:
```python
import functools

import jax
import jax.numpy as jnp
from jax import lax
from jax.experimental import pallas as pl
from jax.experimental.pallas import tpu as pltpu
from jax.sharding import Mesh
from jax.sharding import PartitionSpec as P


SP = ("far", "side", "pair")
fence = lax.optimization_barrier


def swapped(value, axis):
    return lax.ppermute(value, axis, [(0, 1), (1, 0)])


def shifted(value, steps):
    count = lax.axis_size("far")
    return lax.ppermute(value, "far", [(s, (s + steps) % count) for s in range(count)])


def passed_along(value, steps):
    count = lax.axis_size(SP)
    first, last = (max(0, -steps), min(count, count - steps))
    return lax.ppermute(value, SP, [(source, source + steps) for source in range(first, last)])


def chosen(bit, low, high):
    return jnp.where(bit == 0, low, high)


def slot_columns(info, targets, capacity):
    rows = info.shape[1]
    routes = info[0:2]
    probs = info[2:4]
    wide = targets.shape[0] * capacity
    earlier = (jnp.arange(rows)[:, None] > jnp.arange(rows)[None, :]).astype(jnp.bfloat16)
    target_of = jnp.repeat(targets, capacity).astype(jnp.float32)
    slot_of = (jnp.arange(wide) % capacity).astype(jnp.float32)
    first = routes[0][:, None] == target_of[None, :]
    second = routes[1][:, None] == target_of[None, :]
    named = (first | second).astype(jnp.bfloat16)
    before = jnp.dot(earlier, named, preferred_element_type=jnp.float32)
    here = before == slot_of[None, :]
    first, second = (first & here, second & here)
    weights = jnp.sum(
        jnp.where(first, probs[0][:, None], 0.0) + jnp.where(second, probs[1][:, None], 0.0),
        axis=0,
    )
    return ((first | second).astype(jnp.bfloat16), weights)


def contract_rows(left, right):
    return lax.dot_general(
        left, right, (((0,), (0,)), ((), ())), preferred_element_type=jnp.float32
    )


def contract_cols(left, right):
    return lax.dot_general(
        left, right, (((1,), (1,)), ((), ())), preferred_element_type=jnp.float32
    )


def own_and_other(half):
    core = lax.axis_index("tp")
    own = pl.ds(pl.multiple_of(core * half, half), half)
    other = pl.ds(pl.multiple_of((1 - core) * half, half), half)
    return (own, other)


def dotted(left, right):
    return jnp.dot(left, right, preferred_element_type=jnp.float32)


def in_vmem(kernel, shapes, flops, arrays, scratch=(), limit=24):
    return pl.pallas_call(
        kernel,
        out_shape=shapes,
        in_specs=[pl.BlockSpec(memory_space=pltpu.VMEM)] * len(arrays),
        out_specs=jax.tree.map(lambda _: pl.BlockSpec(memory_space=pltpu.VMEM), shapes),
        scratch_shapes=[pltpu.VMEM(shape, dtype) for shape, dtype in scratch],
        cost_estimate=pl.CostEstimate(
            flops=flops, bytes_accessed=sum(a.size * 2 for a in arrays), transcendentals=0
        ),
        compiler_params=pltpu.CompilerParams(vmem_limit_bytes=limit << 20),
    )(*arrays)


LANES = 128


def gathered(pieces, held):
    half = held.shape[1] // 2
    count = len(pieces) // 2
    for column, group in enumerate((pieces[:count], pieces[count:])):
        start = 0
        for piece in group:
            rows = piece.shape[0]
            held[start : start + rows, column * half : (column + 1) * half] = piece[...]
            start += rows


def hidden_kernel(*refs):
    pieces = refs[:8]
    gate_w, up_w, act_ref, gate_f, up_f, held = refs[8:]
    own, other = own_and_other(held.shape[1] // 2)
    gathered(pieces, held)

    def step(i, carry):
        cols = pl.ds(pl.multiple_of(i * LANES, LANES), LANES)
        own_w = jnp.concatenate([gate_w[0, own, cols], up_w[0, own, cols]], axis=1)
        oth_w = jnp.concatenate([gate_w[0, other, cols], up_w[0, other, cols]], axis=1)
        both = dotted(held[...], jnp.concatenate([own_w, oth_w], axis=0))
        gate, up = (both[:, :LANES], both[:, LANES:])
        sig = jax.nn.sigmoid(gate)
        silu = gate * sig
        act_ref[:, cols] = (silu * up).astype(act_ref.dtype)
        gate_f[:, cols] = (up * sig * (1.0 + gate * (1.0 - sig))).astype(gate_f.dtype)
        up_f[:, cols] = silu.astype(up_f.dtype)
        return carry

    lax.fori_loop(0, gate_w.shape[2] // LANES, step, 0)


def pre_kernel(*refs):
    pieces = refs[:8]
    down_w, gate_f, up_f, gate_pre, up_pre, held = refs[8:]
    own, other = own_and_other(held.shape[1] // 2)
    count = down_w.shape[1]
    gathered(pieces, held)

    def piece(start, size):
        at_w = pl.ds(start, size)
        weights = jnp.concatenate([down_w[0, at_w, own], down_w[0, at_w, other]], axis=1)
        hidden = contract_cols(held[...], weights)
        gate_pre[:, at_w] = (hidden * gate_f[:, at_w].astype(jnp.float32)).astype(gate_pre.dtype)
        up_pre[:, at_w] = (hidden * up_f[:, at_w].astype(jnp.float32)).astype(up_pre.dtype)

    def step(i, carry):
        piece(pl.multiple_of(i * 2 * LANES, 2 * LANES), 2 * LANES)
        return carry

    steps = count // (2 * LANES)
    lax.fori_loop(0, steps, step, 0)
    if count % (2 * LANES):
        piece(steps * 2 * LANES, count % (2 * LANES))


def held_block(k, refs, side_refs):
    if k == 0:
        return (refs[0][...], side_refs[0][...])
    rows = refs[0].shape[0]
    at = slice((k - 1) * rows, k * rows)
    return (refs[1][at, :], side_refs[1][at, :])


def act_kernel(columns, near_w, far_w, near_side_w, far_side_w, kept, given):
    blocks, rows, _ = columns.shape
    planes = blocks // 2
    plane = lax.axis_index("far")
    side = lax.axis_index("side")
    total = jnp.zeros((rows, near_w.shape[1]), jnp.float32)
    for k in range(planes):
        r = lax.rem(plane + planes - k, planes)
        here, beside = held_block(k, (near_w, far_w), (near_side_w, far_side_w))
        total = total + dotted(columns[2 * r + side], here)
        total = total + dotted(columns[2 * r + 1 - side], beside)
    kept[...] = total[: rows // 2]
    given[...] = total[rows // 2 :].astype(given.dtype)


def proj_kernel(columns, near, far, near_side, far_side, kept, given, total):
    planes = columns.shape[0] // 2
    plane = lax.axis_index("far")
    side = lax.axis_index("side")
    pair = lax.axis_index("pair")
    out = kept.shape[0]
    value = jnp.zeros(total.shape, jnp.float32)
    for k in range(planes):
        r = lax.rem(plane + planes - k, planes)
        here, beside = held_block(k, (near, far), (near_side, far_side))
        value = value + contract_rows(columns[2 * r + side], here)
        value = value + contract_rows(columns[2 * r + 1 - side], beside)
    total[...] = value
    kept[...] = total[pl.ds(pl.multiple_of(pair * out, out), out), :]
    given[...] = total[pl.ds(pl.multiple_of((1 - pair) * out, out), out), :].astype(given.dtype)


def back_kernel(part, gate_pre, up_pre, gate_w, up_w, kept, given):
    rows, half = kept.shape
    core = lax.axis_index("tp")
    at = pl.ds(part * rows, rows)
    block = 2 * LANES

    for out, place in ((given, 1 - core), (kept, core)):

        def step(i, carry, out=out, place=place):
            from_w = pl.ds(pl.multiple_of(place * half + i * block, block), block)
            value = contract_cols(gate_pre[at, :], gate_w[0, from_w, :]) + contract_cols(
                up_pre[at, :], up_w[0, from_w, :]
            )
            out[:, pl.ds(pl.multiple_of(i * block, block), block)] = value.astype(out.dtype)
            return carry

        lax.fori_loop(0, half // block, step, 0)


def grads_kernel(core_ref, *refs):
    mids, cots = (refs[:8], refs[8:16])
    act, gate_pre, up_pre, gate_ref, up_ref, down_ref = refs[16:]

    def fill(mids, cots):
        both = jnp.concatenate([piece[...] for piece in mids], axis=0)
        gate_ref[0] = contract_rows(both, gate_pre[...]).astype(gate_ref.dtype)
        up_ref[0] = contract_rows(both, up_pre[...]).astype(up_ref.dtype)
        both = jnp.concatenate([piece[...] for piece in cots], axis=0)
        down_ref[0] = contract_rows(act[...], both).astype(down_ref.dtype)

    @pl.when(pl.program_id(0) == 0)
    def _():
        fill(mids[:4], cots[:4])

    @pl.when(pl.program_id(0) != 0)
    def _():
        fill(mids[4:], cots[4:])


def weight_grads(core, mids, cots, act, gate_pre, up_pre):
    half = mids[0].shape[1]
    rows, hidden = act.shape
    block = 2 * LANES
    steps = half // block

    def piece(number, array):
        turn = number // 4

        def at(h, i, c):
            return (0, jnp.where(h == turn, i, (steps - 1) * (1 - turn)))

        return pl.BlockSpec((array.shape[0], block), at)

    def full(array):
        return pl.BlockSpec(array.shape, lambda h, i, c: (0, 0))

    spread = [piece(n, array) for n, array in enumerate(mids)]

    def out_rows(h, i, c):
        return (0, (h ^ c[0]) * steps + i, 0)

    def out_cols(h, i, c):
        return (0, 0, (h ^ c[0]) * steps + i)

    return pl.pallas_call(
        grads_kernel,
        grid_spec=pltpu.PrefetchScalarGridSpec(
            num_scalar_prefetch=1,
            grid=(2, steps),
            in_specs=[*spread, *spread, full(act), full(gate_pre), full(up_pre)],
            out_specs=[
                pl.BlockSpec((1, block, hidden), out_rows),
                pl.BlockSpec((1, block, hidden), out_rows),
                pl.BlockSpec((1, hidden, block), out_cols),
            ],
        ),
        out_shape=[
            jax.ShapeDtypeStruct((1, 2 * half, hidden), jnp.bfloat16),
            jax.ShapeDtypeStruct((1, 2 * half, hidden), jnp.bfloat16),
            jax.ShapeDtypeStruct((1, hidden, 2 * half), jnp.bfloat16),
        ],
        cost_estimate=pl.CostEstimate(
            flops=12 * rows * half * hidden, bytes_accessed=12 * half * hidden, transcendentals=0
        ),
        compiler_params=pltpu.CompilerParams(
            vmem_limit_bytes=40 << 20, dimension_semantics=("arbitrary", "arbitrary")
        ),
    )(core.reshape(1).astype(jnp.int32), *mids, *cots, act, gate_pre, up_pre)


def on_device(
    conv_out,
    ln_gain,
    taps,
    proj_weight,
    stream_mid,
    out_grad,
    routes,
    route_probs,
    gate_slabs,
    up_slabs,
    down_slabs,
):
    tok_rows, half = conv_out.shape
    width = half * lax.axis_size("tp")
    planes = lax.axis_size("far")
    experts = 2 * planes
    capacity = 3 * tok_rows // experts
    out_rows = proj_weight.shape[0]
    core = lax.axis_index("tp")
    plane = lax.axis_index("far")
    side = lax.axis_index("side")
    pair = lax.axis_index("pair")
    wide = planes * capacity
    hops = range(1, planes)

    info = jnp.concatenate([routes.astype(jnp.float32).T, route_probs.T], axis=0)
    beside_info = swapped(info, "side")
    beside_mid = swapped(stream_mid, "side")
    beside_grad = swapped(out_grad, "side")

    values = conv_out.astype(jnp.float32)
    sums = (jnp.sum(values, axis=1), jnp.sum(values * values, axis=1))
    row_total, row_squares = lax.psum(sums, "tp")
    row_mean = row_total[:, None] / width
    row_var = row_squares[:, None] / width - row_mean * row_mean
    inv_std = lax.rsqrt(row_var + 1e-06)
    normed = (values - row_mean) * inv_std
    scaled_z = normed * ln_gain[None, :]
    z_sig = jax.nn.sigmoid(scaled_z)
    activated = (scaled_z * z_sig).astype(jnp.bfloat16)

    targets = 2 * ((plane + jnp.arange(planes)) % planes) + side
    own_table, own_weights = slot_columns(info, targets, capacity)
    beside_table, beside_weights = slot_columns(beside_info, targets, capacity)

    def by_target(near, far):
        near, far = (
            block.astype(jnp.bfloat16).reshape(planes, capacity, half) for block in (near, far)
        )
        return [jnp.stack([near[k], far[k]]) for k in range(planes)]

    mid_slots = by_target(
        contract_rows(own_table, stream_mid), contract_rows(beside_table, beside_mid)
    )
    grad_slots = by_target(
        contract_rows(own_table, out_grad) * own_weights[:, None],
        contract_rows(beside_table, beside_grad) * beside_weights[:, None],
    )
    near_rows = 2 * capacity
    mid_far = [shifted(mid_slots[k], k) for k in hops]
    mid_near = mid_slots[0].reshape(near_rows, half)
    mid_near_pair = swapped(mid_near, "pair")
    mid_far, grad_slots, activated = fence((mid_far, grad_slots, activated))
    mid_mine = jnp.stack(mid_far).reshape(-1, half)
    mid_pair = swapped(mid_mine, "pair")
    grad_far = [shifted(grad_slots[k], k) for k in hops]
    grad_near = grad_slots[0].reshape(near_rows, half)
    grad_near_pair = swapped(grad_near, "pair")
    mid_pair, grad_far, grad_near_pair = fence((mid_pair, grad_far, grad_near_pair))
    proj_near_side = swapped(proj_weight, "side")
    act_near_side = swapped(activated, "side")
    grad_mine = jnp.stack(grad_far).reshape(-1, half)
    grad_pair = swapped(grad_mine, "pair")
    proj_far = [shifted(proj_weight, k) for k in hops]
    act_far = [shifted(activated, k) for k in hops]

    def pieces(*own):
        return (*own, *(swapped(p, "tp") for p in own))

    mids = pieces(mid_near, mid_mine, mid_near_pair, mid_pair)
    cots = pieces(grad_near, grad_mine, grad_near_pair, grad_pair)
    slots, hidden = (4 * wide, gate_slabs.shape[2])
    held = jax.ShapeDtypeStruct((slots, hidden), jnp.bfloat16)
    flops = 2 * slots * width * hidden
    hidden_act, gate_f, up_f = in_vmem(
        hidden_kernel,
        (held, held, held),
        2 * flops,
        (*mids, gate_slabs, up_slabs),
        (((slots, width), jnp.bfloat16),),
    )
    gate_pre, up_pre = in_vmem(
        pre_kernel,
        (held, held),
        flops,
        (*cots, down_slabs, gate_f, up_f),
        (((slots, width), jnp.bfloat16),),
    )
    summed = []
    for part in (1, 0):
        one = jax.ShapeDtypeStruct((2 * wide, half), jnp.bfloat16)
        kept, given = in_vmem(
            functools.partial(back_kernel, part),
            (one, one),
            flops,
            (gate_pre, up_pre, gate_slabs, up_slabs),
        )
        given = swapped(given, "tp")
        summed.append(kept.astype(jnp.float32) + given.astype(jnp.float32))
    proj_rest = jnp.concatenate(proj_far, axis=0)
    proj_side = swapped(proj_rest, "side")
    act_rest = jnp.concatenate(act_far, axis=0)
    act_side = swapped(act_rest, "side")
    moving = summed[0].astype(jnp.bfloat16)
    across = swapped(moving[near_rows:], "pair")
    across_near = swapped(moving[:near_rows], "pair")
    both = (summed[1][near_rows:] + across.astype(jnp.float32)).astype(jnp.bfloat16)
    both = both.reshape(planes - 1, 2, capacity, half)
    back_far = [shifted(both[k - 1], -k) for k in hops]
    back_near = (summed[1][:near_rows] + across_near.astype(jnp.float32)).astype(jnp.bfloat16)
    back = jnp.stack([back_near.reshape(2, capacity, half), *back_far])
    for_beside = jnp.dot(
        beside_table, back[:, 1].reshape(wide, half), preferred_element_type=jnp.float32
    ).astype(jnp.bfloat16)
    for_own = jnp.dot(
        own_table, back[:, 0].reshape(wide, half), preferred_element_type=jnp.float32
    )
    from_beside = swapped(for_beside, "side")
    grad_stream = (
        out_grad.astype(jnp.float32) + for_own + from_beside.astype(jnp.float32)
    ).astype(jnp.bfloat16)

    grad_gate, grad_up, grad_down = weight_grads(
        core, mids, cots, hidden_act, gate_pre, up_pre
    )

    blocks = half // (2 * out_rows)
    by_place = grad_stream.reshape(tok_rows, blocks, 2 * out_rows).transpose(1, 0, 2)
    by_pair = grad_stream.reshape(tok_rows, blocks, 2, out_rows).transpose(2, 1, 0, 3)
    stream_met = swapped(chosen(pair, by_pair[1], by_pair[0]), "pair")
    whole_stream = lax.all_gather(by_place, "tp", axis=0, tiled=True)
    columns = lax.all_to_all(whole_stream, ("far", "side"), split_axis=0, concat_axis=0, tiled=True)
    shared = jnp.concatenate([chosen(pair, by_pair[0], by_pair[1]), stream_met], axis=1)
    shared = lax.all_gather(shared, "tp", axis=0, tiled=True)
    act_kept, act_given = in_vmem(
        act_kernel,
        (
            jax.ShapeDtypeStruct((tok_rows, half), jnp.float32),
            jax.ShapeDtypeStruct((tok_rows, half), jnp.bfloat16),
        ),
        2 * tok_rows * width * half,
        (shared, proj_weight, proj_rest, proj_near_side, proj_side),
        limit=24,
    )
    act_met = swapped(act_given, "pair")
    grad_act = act_kept + act_met.astype(jnp.float32)
    grad_normed = grad_act * z_sig * (1.0 + scaled_z * (1.0 - z_sig)) * ln_gain[None, :]
    first_sum, second_sum = lax.psum(
        (jnp.sum(grad_normed, axis=1), jnp.sum(grad_normed * normed, axis=1)), "tp"
    )
    grad_conv = (
        inv_std * (grad_normed - first_sum[:, None] / width - normed * second_sum[:, None] / width)
    ).astype(jnp.bfloat16)
    reach_rows = taps.shape[0] - 1
    following = passed_along(grad_conv[:reach_rows], -1)
    extended = jnp.concatenate([grad_conv, following], axis=0).astype(jnp.float32)
    tap_values = taps.astype(jnp.float32)
    grad_input = jnp.zeros((tok_rows, grad_conv.shape[1]), jnp.float32)
    for offset in range(taps.shape[0]):
        grad_input = grad_input + tap_values[offset][None, :] * extended[offset : offset + tok_rows]

    proj_kept, proj_given = in_vmem(
        proj_kernel,
        (
            jax.ShapeDtypeStruct((out_rows, half), jnp.float32),
            jax.ShapeDtypeStruct((out_rows, half), jnp.bfloat16),
        ),
        2 * tok_rows * width * half,
        (columns, activated, act_rest, act_near_side, act_side),
        (((2 * out_rows, half), jnp.float32),),
    )
    proj_met = swapped(proj_given, "pair")
    grad_proj = proj_kept + proj_met.astype(jnp.float32)
    return (
        grad_input.astype(jnp.bfloat16),
        grad_proj,
        grad_gate,
        grad_up,
        grad_down,
    )


def solution(mesh):
    places, cores = mesh.devices.shape
    split = Mesh(mesh.devices.reshape(places // 4, 2, 2, cores), (*SP, "tp"))
    return jax.shard_map(
        on_device,
        mesh=split,
        in_specs=(
            P(SP, "tp"),
            P("tp"),
            P(None, "tp"),
            P(SP, "tp"),
            P(SP, "tp"),
            P(SP, "tp"),
            P(SP, None),
            P(SP, None),
            P(SP, None, "tp"),
            P(SP, None, "tp"),
            P(SP, "tp", None),
        ),
        out_specs=(
            P(SP, "tp"),
            P(SP, "tp"),
            P(SP, None, "tp"),
            P(SP, None, "tp"),
            P(SP, "tp", None),
        ),
        check_vma=False,
    )
```

time: 295 us -> 250 us (0.85); the launches traced: 290 us -> 249 us
  matrix products: 48.1 us -> 3.2 us
  Pallas kernels: 0 us -> 40 us
  local copies, waits for them, and re-layouts: 9.62 us -> 39.5 us
  other arithmetic: 46 us -> 16.9 us
  starting transfers between devices: 78.5 us -> 58.6 us
  waiting for transfers between devices: 96.5 us -> 78.9 us
    pallas_call x0 -> x7, Pallas kernels: none -> 40 us  [the longest x6 26.1 us: in_vmem(): pl.pallas_call(kernel, out_shape=shapes, in_specs=[pl.BlockSpec(memory_sp...]
    unnamed x98 -> x180, local copies, waits for them, and re-layouts: 0.53 us -> 30.3 us
    select_n x6 -> x2, other arithmetic: 30.5 us -> 1.97 us  [chosen(): return jnp.where(bit == 0, low, high)]
    dot_general x9 -> x4, matrix products: 26.3 us -> 1.23 us  [contract_rows(): lax.dot_general(left, right, (((0,), (0,)), ((), ())), preferred_element_...]
    ppermute x15, waiting for transfers between devices: 52.8 us -> 30 us  [shifted(): lax.ppermute(value, 'far', [(s, (s + steps) % count) for s in range(count)])]
    dot_general x7 -> x0, matrix products: 20.5 us -> none  [the longest x3 11.3 us: contract_cols(): lax.dot_general(left, right, (((1,), (1,)), ((), ())), preferred_element_...]
    ppermute x15, starting transfers between devices: 45.6 us -> 28.8 us  [shifted(): lax.ppermute(value, 'far', [(s, (s + steps) % count) for s in range(count)])]
    all_to_all x1, starting transfers between devices: 15.7 us -> 6.14 us  [on_device(): lax.all_to_all(whole_stream, ('far', 'side'), split_axis=0, concat_axis=0...]
  transfers between devices with their start and end apart: 32 -> 44, of which waited for: 13 -> 16; matrix products, arithmetic and copies ran while one was open for 24% -> 12% of each run, Pallas kernels for 0% -> 12%
where the time goes in v2:
time: 250 us; the launch traced here: 249 us
  waiting for transfers between devices  78.9 us (32%)
  starting transfers between devices  58.6 us (23%)
  Pallas kernels  40 us (16%)
  local copies, waits for them, and re-layouts  39.5 us (16%)
  other arithmetic  16.9 us (7%)
  blocking collectives  9.61 us (4%)
  matrix products  3.2 us (1%)
    ppermute x27, waiting for transfers between devices, swapped(): return lax.ppermute(value, axis, [(0, 1), (1, 0)])  48.9 us
    unnamed x180, local copies, waits for them, and re-layouts  30.3 us
    ppermute x15, waiting for transfers between devices, shifted(): lax.ppermute(value, 'far', [(s, (s + steps) % count) for s in range(count)])  30 us
    ppermute x15, starting transfers between devices, shifted(): lax.ppermute(value, 'far', [(s, (s + steps) % count) for s in range(count)])  28.8 us
    pallas_call x6, Pallas kernels, in_vmem(): pl.pallas_call(kernel, out_shape=shapes, in_specs=[pl.BlockSpec(memory_sp...  26.1 us
    ppermute x27, starting transfers between devices, swapped(): return lax.ppermute(value, axis, [(0, 1), (1, 0)])  22.4 us
    pallas_call x1, Pallas kernels, weight_grads(): pl.pallas_call(grads_kernel, grid_spec=pltpu.PrefetchScalarGridSpec(num_s...  14 us
    all_to_all x1, starting transfers between devices, on_device(): lax.all_to_all(whole_stream, ('far', 'side'), split_axis=0, concat_axis=0...  6.14 us
  transfers between devices with their start and end apart: 44, of which 16 were waited for; matrix products, arithmetic and copies ran while one was open for 12% of the time, Pallas kernels for 12%

profile of v2, /device:TPU:0, one launch (start us, length us, event | category | flops | bytes accessed | tf_op | source)
XLA Modules:
  0.0 248.7 jit_solution(11422870338265173129)
XLA Ops:
  2.1 3.0 %collective-permute-start = (f32[4,128]{1,0:T(4,128)S(1)}, f32[4,128]{1,0:T(4,128)S(1)}, u32[]{:S(2)}, u32[]{:S(2)}) collective-permute-start(f32[4,128]{1,0:T(4,128)S(1)} %pad_maximum_fusion.12), channel_id=1, source_target_pairs={{0,4},{4,0},{1,5},{5,1},{2,6},{6,2},{3,7},{7,3},{8,12},{12,8},{9,1... | collective-permute-start | bytes 6152 | tf_op jit(solution)/shard_map/ppermute | solution.py:17
  5.1 2.0 collective-permute-start.1
  7.9 1.1 fusion.3
  9.0 2.5 all-reduce.1
  11.5 1.2 fusion.14.near
  14.8 3.9 %collective-permute-done.1 = bf16[128,1024]{1,0:T(8,128)(2,1)S(1)} collective-permute-done((bf16[128,1024]{1,0:T(8,128)(2,1)}, bf16[128,1024]{1,0:T(8,128)(2,1)S(1)}, u32[]{:S(2)}, u32[]{:S(2)}) %collective-permute-start.1) | collective-permute-done | bytes 262176 | tf_op jit(solution)/shard_map/ppermute | solution.py:17
  19.1 2.7 %collective-permute-start.3 = (bf16[2,48,1024]{2,1,0:T(8,128)(2,1)S(1)}, bf16[2,48,1024]{2,1,0:T(8,128)(2,1)S(1)}, u32[]{:S(2)}, u32[]{:S(2)}) collective-permute-start(bf16[2,48,1024]{2,1,0:T(8,128)(2,1)S(1)} %pad_maximum_fusion.5), channel_id=1, source_target_pairs={{0,16},{8,24},{16,0},{24,8},{1,17},{9,25},{17,1},{25,9},{2,18},{10... | collective-permute-start | bytes 589832 | tf_op jit(solution)/shard_map/ppermute | solution.py:22
  21.7 1.4 collective-permute-start.4
  24.0 11.0 %collective-permute-done.3 = bf16[2,48,1024]{2,1,0:T(8,128)(2,1)S(1)} collective-permute-done((bf16[2,48,1024]{2,1,0:T(8,128)(2,1)S(1)}, bf16[2,48,1024]{2,1,0:T(8,128)(2,1)S(1)}, u32[]{:S(2)}, u32[]{:S(2)}) %collective-permute-start.3) | collective-permute-done | bytes 196640 | tf_op jit(solution)/shard_map/ppermute | solution.py:22
  35.1 1.6 collective-permute-start.6
  37.2 3.8 %collective-permute-start.7 = (bf16[2,48,1024]{2,1,0:T(8,128)(2,1)S(1)}, bf16[2,48,1024]{2,1,0:T(8,128)(2,1)S(1)}, u32[]{:S(2)}, u32[]{:S(2)}) collective-permute-start(bf16[2,48,1024]{2,1,0:T(8,128)(2,1)S(1)} %pad_maximum_fusion.8), channel_id=1, source_target_pairs={{0,8},{8,16},{16,24},{24,0},{1,9},{9,17},{17,25},{25,1},{2,10},{10... | collective-permute-start | bytes 589832 | tf_op jit(solution)/shard_map/ppermute | solution.py:22
  41.0 1.9 collective-permute-start.8
  42.9 2.9 %collective-permute-start.9 = (bf16[2,48,1024]{2,1,0:T(8,128)(2,1)S(1)}, bf16[2,48,1024]{2,1,0:T(8,128)(2,1)S(1)}, u32[]{:S(2)}, u32[]{:S(2)}) collective-permute-start(bf16[2,48,1024]{2,1,0:T(8,128)(2,1)S(1)} %pad_maximum_fusion.10), channel_id=1, source_target_pairs={{0,24},{8,0},{16,8},{24,16},{1,25},{9,1},{17,9},{25,17},{2,26},{10... | collective-permute-start | bytes 589832 | tf_op jit(solution)/shard_map/ppermute | solution.py:22
  45.8 6.3 %collective-permute-done.10.refs_2_.refs_10_ = bf16[96,1024]{1,0:T(8,128)(2,1)S(1)} collective-permute-done((bf16[96,1024]{1,0:T(8,128)(2,1)S(1)}, bf16[96,1024]{1,0:T(8,128)(2,1)S(1)}, u32[]{:S(2)}, u32[]{:S(2)}) %collective-permute-start.10) | collective-permute-done | bytes 196640 | tf_op jit(solution)/shard_map/ppermute | solution.py:17
  52.2 1.7 collective-permute-done.8
  54.0 1.6 collective-permute-start.11
  56.7 15.4 %collective-permute-done.16.refs_2_ = bf16[96,1024]{1,0:T(8,128)(2,1)S(1)} collective-permute-done((bf16[96,1024]{1,0:T(8,128)(2,1)S(1)}, bf16[96,1024]{1,0:T(8,128)(2,1)S(1)}, u32[]{:S(2)}, u32[]{:S(2)}) %collective-permute-start.16) | collective-permute-done | bytes 196640 | tf_op jit(solution)/shard_map/ppermute | solution.py:17
  74.1 7.3 %shard_map.146 = (bf16[768,896]{1,0:T(8,128)(2,1)S(1)}, bf16[768,896]{1,0:T(8,128)(2,1)S(1)}, bf16[768,896]{1,0:T(8,128)(2,1)S(1)}) custom-call(bf16[96,1024]{1,0:T(8,128)(2,1)S(1)} %bitcast.144, bf16[288,1024]{1,0:T(8,128)(2,1)S(1)} %bitcast.132, bf16[96,1024]{1,0:T(8,128)(2,1)S(1)} %collective-permute-done.16.refs_2_, ...), custom_call_target="tpu_custom_call" | custom-call | flops 5637144576 | bytes 10485760 | tf_op jit(solution)/shard_map/pallas_call | solution.py:80
  81.4 1.1 copy-done.44
  82.6 4.2 %shard_map.147 = (bf16[768,896]{1,0:T(8,128)(2,1)S(1)}, bf16[768,896]{1,0:T(8,128)(2,1)S(1)}) custom-call(bf16[96,1024]{1,0:T(8,128)(2,1)S(1)} %bitcast.140, bf16[288,1024]{1,0:T(8,128)(2,1)S(1)} %bitcast.136, bf16[96,1024]{1,0:T(8,128)(2,1)S(1)} %collective-permute-done.10.refs_2_.refs_10_, bf16[288,1024]{1,0:T(8,128)(2,1)S(1)} %collective-permute-done.11.refs_3_.refs_11_, ...), custom_call_target="tpu_custom_call" | custom-call | flops 2818572288 | bytes 9568256 | tf_op jit(solution)/shard_map/pallas_call | solution.py:80
  86.9 4.6 %shard_map.149 = (bf16[384,1024]{1,0:T(8,128)(2,1)S(1)}, bf16[384,1024]{1,0:T(8,128)(2,1)S(1)}) custom-call(bf16[768,896]{1,0:T(8,128)(2,1)S(1)} %get-tuple-element.48.gate_pre.refs_17_, bf16[768,896]{1,0:T(8,128)(2,1)S(1)} %get-tuple-element.49.up_pre.refs_18_, bf16[1,2048,896]{2,1,0:T(8,128)(2,1)S(1)} %copy-done.10, bf16[1,2048,896]{2,1,0:T(8,128)(2,1)S(1)} %copy-done.12), custom_call_target="tpu_custom_call" | custom-call | flops 2818572288 | bytes 10092544 | tf_op jit(solution)/shard_map/pallas_call | solution.py:80
  91.8 6.0 %collective-permute-start.30 = (bf16[128,1024]{1,0:T(8,128)(2,1)S(1)}, bf16[128,1024]{1,0:T(8,128)(2,1)}, u32[]{:S(2)}, u32[]{:S(2)}) collective-permute-start(bf16[128,1024]{1,0:T(8,128)(2,1)S(1)} %copy-done.4), channel_id=1, source_target_pairs={{0,8},{8,16},{16,24},{24,0},{1,9},{9,17},{17,25},{25,1},{2,10},{10... | collective-permute-start | bytes 786440 | tf_op jit(solution)/shard_map/ppermute | solution.py:22
  97.8 3.4 %collective-permute-start.31 = (bf16[128,1024]{1,0:T(8,128)(2,1)S(1)}, bf16[128,1024]{1,0:T(8,128)(2,1)}, u32[]{:S(2)}, u32[]{:S(2)}) collective-permute-start(bf16[128,1024]{1,0:T(8,128)(2,1)S(1)} %copy-done.4), channel_id=1, source_target_pairs={{0,16},{8,24},{16,0},{24,8},{1,17},{9,25},{17,1},{25,9},{2,18},{10... | collective-permute-start | bytes 786440 | tf_op jit(solution)/shard_map/ppermute | solution.py:22
  101.8 2.0 copy-done.11
  103.9 2.0 copy-done.13
  105.9 1.3 copy-done.39
  107.2 1.3 copy-done.42
  108.6 4.6 %shard_map.148 = (bf16[384,1024]{1,0:T(8,128)(2,1)S(1)}, bf16[384,1024]{1,0:T(8,128)(2,1)S(1)}) custom-call(bf16[768,896]{1,0:T(8,128)(2,1)S(1)} %copy-done.39, bf16[768,896]{1,0:T(8,128)(2,1)S(1)} %copy-done.42, bf16[1,2048,896]{2,1,0:T(8,128)(2,1)S(1)} %copy-done.11, bf16[1,2048,896]{2,1,0:T(8,128)(2,1)S(1)} %copy-done.13), custom_call_target="tpu_custom_call" | custom-call | flops 2818572288 | bytes 10092544 | tf_op jit(solution)/shard_map/pallas_call | solution.py:80
  114.0 1.4 add_convert_fusion
  115.5 1.6 collective-permute-start.24
  119.6 12.2 %collective-permute-done.24 = bf16[288,1024]{1,0:T(8,128)(2,1)S(1)} collective-permute-done((bf16[288,1024]{1,0:T(8,128)(2,1)S(1)}, bf16[288,1024]{1,0:T(8,128)(2,1)S(1)}, u32[]{:S(2)}, u32[]{:S(2)}) %collective-permute-start.24) | collective-permute-done | bytes 589856 | tf_op jit(solution)/shard_map/ppermute | solution.py:17
  132.9 2.0 collective-permute-start.26
  135.5 1.4 collective-permute-start.27
  137.0 1.3 collective-permute-done.25
  138.8 12.7 %collective-permute-done.26 = bf16[2,48,1024]{2,1,0:T(8,128)(2,1)S(1)} collective-permute-done((bf16[2,48,1024]{2,1,0:T(8,128)(2,1)S(1)}, bf16[2,48,1024]{2,1,0:T(8,128)(2,1)S(1)}, u32[]{:S(2)}, u32[]{:S(2)}) %collective-permute-start.26) | collective-permute-done | bytes 196640 | tf_op jit(solution)/shard_map/ppermute | solution.py:22
  155.1 1.5 collective-permute-start.34
  157.6 3.3 %collective-permute-done.37 = bf16[128,1024]{1,0:T(8,128)(2,1)S(1)} collective-permute-done((bf16[128,1024]{1,0:T(8,128)(2,1)S(1)}, bf16[128,1024]{1,0:T(8,128)(2,1)S(1)}, u32[]{:S(2)}, u32[]{:S(2)}) %collective-permute-start.37) | collective-permute-done | bytes 262176 | tf_op jit(solution)/shard_map/ppermute | solution.py:22
  162.8 1.8 copy.20
  165.6 1.6 collective-permute-start.29
  168.2 2.5 %collective-permute-done.29 = bf16[4,128,128]{1,2,0:T(8,128)(2,1)S(1)} collective-permute-done((bf16[4,128,128]{1,2,0:T(8,128)(2,1)S(1)}, bf16[4,128,128]{1,2,0:T(8,128)(2,1)S(1)}, u32[]{:S(2)}, u32[]{:S(2)}) %collective-permute-start.29) | collective-permute-done | bytes 131104 | tf_op jit(solution)/shard_map/ppermute | solution.py:17
  171.7 1.8 copy.25
  173.4 2.4 all_gather.6.columns
  175.8 2.8 %collective-permute-done.34.far_side_w = bf16[384,1024]{1,0:T(8,128)(2,1)S(1)} collective-permute-done((bf16[384,1024]{1,0:T(8,128)(2,1)S(1)}, bf16[384,1024]{1,0:T(8,128)(2,1)S(1)}, u32[]{:S(2)}, u32[]{:S(2)}) %collective-permute-start.34) | collective-permute-done | bytes 786464 | tf_op jit(solution)/shard_map/ppermute | solution.py:17
  178.6 2.9 %shard_map.150 = (f32[128,1024]{1,0:T(8,128)S(1)}, bf16[128,1024]{1,0:T(8,128)(2,1)}) custom-call(bf16[8,256,128]{2,1,0:T(8,128)(2,1)S(1)} %all_gather.6.columns, bf16[128,1024]{1,0:T(8,128)(2,1)S(1)} %copy-done.4, bf16[384,1024]{1,0:T(8,128)(2,1)S(1)} %constant_dynamic-update-slice_fusion.far_w, bf16[128,1024]{1,0:T(8,128)(2,1)} %collective-permute-done.33.near_side_w, ...), custom_call_target="tpu_custom_call" | custom-call | flops 536870912 | bytes 2621440 | tf_op jit(solution)/shard_map/pallas_call | solution.py:80
  181.5 1.5 collective-permute-start.35
  185.3 1.1 copy.27
  186.5 2.3 all_gather.7
  188.8 6.1 %all-to-all-start = ((bf16[8,128,256]{2,1,0:T(8,128)(2,1)}), bf16[8,128,256]{2,1,0:T(8,128)(2,1)S(1)}, u32[]{:S(2)}, u32[]{:S(2)}) async-start(bf16[8,128,256]{2,1,0:T(8,128)(2,1)} %all_gather.7), calls=%async_computation | async-start | bytes 1048576 | tf_op jit(solution)/shard_map/all_to_all | solution.py:425
  195.0 2.2 fusion.76
  197.2 2.4 all-reduce
  199.7 1.4 fusion.22
  201.0 1.3 collective-permute-start.36
  205.3 1.1 copy-done.15
  206.3 1.1 copy-done.17
  207.4 1.1 copy-done.19
  208.4 1.1 copy-done.21
  217.2 1.3 copy-done.40
  218.5 1.3 copy-done.43
  219.9 1.3 copy-done.45
  221.2 14.0 %shard_map.152 = (bf16[1,2048,896]{2,1,0:T(8,128)(2,1)}, bf16[1,2048,896]{2,1,0:T(8,128)(2,1)}, bf16[1,896,2048]{2,1,0:T(8,128)(2,1)}) custom-call(s32[1]{0:T(128)} %bitcast.86.core_ref, bf16[96,1024]{1,0:T(8,128)(2,1)S(1)} %bitcast.145, bf16[288,1024]{1,0:T(8,128)(2,1)S(1)} %bitcast.133, bf16[96,1024]{1,0:T(8,128)(2,1)S(1)} %copy-done.29, ...), custom_call_target="tpu_custom_call" | custom-call | flops 8455716864 | bytes 11010048 | tf_op jit(solution)/shard_map/pallas_call | solution.py:257
  236.4 2.4 shard_map.151
  238.8 2.7 %collective-permute-start.42 = (bf16[128,1024]{1,0:T(8,128)(2,1)S(1)}, bf16[128,1024]{1,0:T(8,128)(2,1)S(1)}, u32[]{:S(2)}, u32[]{:S(2)}) collective-permute-start(bf16[128,1024]{1,0:T(8,128)(2,1)S(1)} %get-tuple-element.58), channel_id=1, source_target_pairs={{0,2},{2,0},{1,3},{3,1},{4,6},{6,4},{5,7},{7,5},{8,10},{10,8},{9,1... | collective-permute-start | bytes 786440 | tf_op jit(solution)/shard_map/ppermute | solution.py:17
  241.7 2.7 %fusion.24 = bf16[128,1024]{1,0:T(8,128)(2,1)} fusion(f32[158,1024]{1,0:T(8,128)S(1)} %copy-done.46, f32[1024]{0:T(1024)S(1)} %bitcast.194, f32[1024]{0:T(1024)S(1)} %bitcast.193, f32[1024]{0:T(1024)S(1)} %bitcast.192, f32[1024]{0:T(1024)S(1)} %bitcast.191, f32[1024]{0:T(1024)S(1)} %bitcast.190, f32[1024]{0:T(1024)S(1)} %bitcast.189, f32[1024]{0:T(1024)S(1)} %bitcast.188, ...), kind=kLoop, calls=%fused_computation.42 | loop fusion | flops 8126464 | bytes 16642048 | tf_op jit(solution)/shard_map/convert_element_type | solution.py:468
  244.4 3.4 %collective-permute-done.42 = bf16[128,1024]{1,0:T(8,128)(2,1)S(1)} collective-permute-done((bf16[128,1024]{1,0:T(8,128)(2,1)S(1)}, bf16[128,1024]{1,0:T(8,128)(2,1)S(1)}, u32[]{:S(2)}, u32[]{:S(2)}) %collective-permute-start.42) | collective-permute-done | bytes 262176 | tf_op jit(solution)/shard_map/ppermute | solution.py:17
  (274 shorter events, 39.9 us)
Async XLA Ops:
  0.6 13.2 %copy-start.47 = (bf16[128,1024]{1,0:T(8,128)(2,1)S(1)}, bf16[128,1024]{1,0:T(8,128)(2,1)}, u32[]{:S(2)}) copy-start(bf16[128,1024]{1,0:T(8,128)(2,1)} %param.16) | copy-start | bytes 786436
  0.6 12.9 %copy-start.49 = (bf16[128,1024]{1,0:T(8,128)(2,1)S(1)}, bf16[128,1024]{1,0:T(8,128)(2,1)}, u32[]{:S(2)}) copy-start(bf16[128,1024]{1,0:T(8,128)(2,1)} %param.15) | copy-start | bytes 786436
  2.1 10.8 %collective-permute-start = (f32[4,128]{1,0:T(4,128)S(1)}, f32[4,128]{1,0:T(4,128)S(1)}, u32[]{:S(2)}, u32[]{:S(2)}) collective-permute-start(f32[4,128]{1,0:T(4,128)S(1)} %pad_maximum_fusion.12), channel_id=1, source_target_pairs={{0,4},{4,0},{1,5},{5,1},{2,6},{6,2},{3,7},{7,3},{8,12},{12,8},{9,1... | collective-permute-start | bytes 6152 | tf_op jit(solution)/shard_map/ppermute | solution.py:17
  5.1 9.4 %collective-permute-start.5 = (bf16[128,1024]{1,0:T(8,128)(2,1)}, bf16[128,1024]{1,0:T(8,128)(2,1)S(1)}, u32[]{:S(2)}, u32[]{:S(2)}) collective-permute-start(bf16[128,1024]{1,0:T(8,128)(2,1)} %param.16), channel_id=1, source_target_pairs={{0,4},{4,0},{1,5},{5,1},{2,6},{6,2},{3,7},{7,3},{8,12},{12,8},{9,1... | collective-permute-start | bytes 786440 | tf_op jit(solution)/shard_map/ppermute | solution.py:17
  5.1 13.5 %collective-permute-start.1 = (bf16[128,1024]{1,0:T(8,128)(2,1)}, bf16[128,1024]{1,0:T(8,128)(2,1)S(1)}, u32[]{:S(2)}, u32[]{:S(2)}) collective-permute-start(bf16[128,1024]{1,0:T(8,128)(2,1)} %param.15), channel_id=1, source_target_pairs={{0,4},{4,0},{1,5},{5,1},{2,6},{6,2},{3,7},{7,3},{8,12},{12,8},{9,1... | collective-permute-start | bytes 786440 | tf_op jit(solution)/shard_map/ppermute | solution.py:17
  14.8 59.3 %copy-start.12 = (bf16[1,2048,896]{2,1,0:T(8,128)(2,1)S(1)}, bf16[1,2048,896]{2,1,0:T(8,128)(2,1)}, u32[]{:S(2)}) copy-start(bf16[1,2048,896]{2,1,0:T(8,128)(2,1)} %up_w.3) | copy-start | bytes 11010052
  19.1 16.0 %collective-permute-start.3 = (bf16[2,48,1024]{2,1,0:T(8,128)(2,1)S(1)}, bf16[2,48,1024]{2,1,0:T(8,128)(2,1)S(1)}, u32[]{:S(2)}, u32[]{:S(2)}) collective-permute-start(bf16[2,48,1024]{2,1,0:T(8,128)(2,1)S(1)} %pad_maximum_fusion.5), channel_id=1, source_target_pairs={{0,16},{8,24},{16,0},{24,8},{1,17},{9,25},{17,1},{25,9},{2,18},{10... | collective-permute-start | bytes 589832 | tf_op jit(solution)/shard_map/ppermute | solution.py:22
  21.7 13.3 %collective-permute-start.4 = (bf16[2,48,1024]{2,1,0:T(8,128)(2,1)S(1)}, bf16[2,48,1024]{2,1,0:T(8,128)(2,1)S(1)}, u32[]{:S(2)}, u32[]{:S(2)}) collective-permute-start(bf16[2,48,1024]{2,1,0:T(8,128)(2,1)S(1)} %pad_maximum_fusion.6), channel_id=1, source_target_pairs={{0,24},{8,0},{16,8},{24,16},{1,25},{9,1},{17,9},{25,17},{2,26},{10... | collective-permute-start | bytes 589832 | tf_op jit(solution)/shard_map/ppermute | solution.py:22
  23.2 11.9 %collective-permute-start.2 = (bf16[2,48,1024]{2,1,0:T(8,128)(2,1)S(1)}, bf16[2,48,1024]{2,1,0:T(8,128)(2,1)S(1)}, u32[]{:S(2)}, u32[]{:S(2)}) collective-permute-start(bf16[2,48,1024]{2,1,0:T(8,128)(2,1)S(1)} %pad_maximum_fusion.4), channel_id=1, source_target_pairs={{0,8},{8,16},{16,24},{24,0},{1,9},{9,17},{17,25},{25,1},{2,10},{10... | collective-permute-start | bytes 589832 | tf_op jit(solution)/shard_map/ppermute | solution.py:22
  23.9 50.1 %copy-start.10 = (bf16[1,2048,896]{2,1,0:T(8,128)(2,1)S(1)}, bf16[1,2048,896]{2,1,0:T(8,128)(2,1)}, u32[]{:S(2)}) copy-start(bf16[1,2048,896]{2,1,0:T(8,128)(2,1)} %gate_w.3) | copy-start | bytes 11010052
  24.0 58.6 %copy-start.5 = (bf16[2,48,1024]{2,1,0:T(8,128)(2,1)}, bf16[2,48,1024]{2,1,0:T(8,128)(2,1)S(1)}, u32[]{:S(2)}) copy-start(bf16[2,48,1024]{2,1,0:T(8,128)(2,1)S(1)} %pad_maximum_fusion.7) | copy-start | bytes 589828
  35.1 18.8 %collective-permute-start.6 = (bf16[288,1024]{1,0:T(8,128)(2,1)S(1)}, bf16[288,1024]{1,0:T(8,128)(2,1)S(1)}, u32[]{:S(2)}, u32[]{:S(2)}) collective-permute-start(bf16[288,1024]{1,0:T(8,128)(2,1)S(1)} %bitcast.130), channel_id=1, source_target_pairs={{0,2},{2,0},{1,3},{3,1},{4,6},{6,4},{5,7},{7,5},{8,10},{10,8},{9,1... | collective-permute-start | bytes 1769480 | tf_op jit(solution)/shard_map/ppermute | solution.py:17
  36.7 15.5 %collective-permute-start.10 = (bf16[96,1024]{1,0:T(8,128)(2,1)S(1)}, bf16[96,1024]{1,0:T(8,128)(2,1)S(1)}, u32[]{:S(2)}, u32[]{:S(2)}) collective-permute-start(bf16[96,1024]{1,0:T(8,128)(2,1)S(1)} %bitcast.138), channel_id=1, source_target_pairs={{0,2},{2,0},{1,3},{3,1},{4,6},{6,4},{5,7},{7,5},{8,10},{10,8},{9,1... | collective-permute-start | bytes 589832 | tf_op jit(solution)/shard_map/ppermute | solution.py:17
  37.2 15.0 %collective-permute-start.7 = (bf16[2,48,1024]{2,1,0:T(8,128)(2,1)S(1)}, bf16[2,48,1024]{2,1,0:T(8,128)(2,1)S(1)}, u32[]{:S(2)}, u32[]{:S(2)}) collective-permute-start(bf16[2,48,1024]{2,1,0:T(8,128)(2,1)S(1)} %pad_maximum_fusion.8), channel_id=1, source_target_pairs={{0,8},{8,16},{16,24},{24,0},{1,9},{9,17},{17,25},{25,1},{2,10},{10... | collective-permute-start | bytes 589832 | tf_op jit(solution)/shard_map/ppermute | solution.py:22
  41.0 12.9 %collective-permute-start.8 = (bf16[2,48,1024]{2,1,0:T(8,128)(2,1)S(1)}, bf16[2,48,1024]{2,1,0:T(8,128)(2,1)S(1)}, u32[]{:S(2)}, u32[]{:S(2)}) collective-permute-start(bf16[2,48,1024]{2,1,0:T(8,128)(2,1)S(1)} %pad_maximum_fusion.9), channel_id=1, source_target_pairs={{0,16},{8,24},{16,0},{24,8},{1,17},{9,25},{17,1},{25,9},{2,18},{10... | collective-permute-start | bytes 589832 | tf_op jit(solution)/shard_map/ppermute | solution.py:22
  42.9 11.0 %collective-permute-start.9 = (bf16[2,48,1024]{2,1,0:T(8,128)(2,1)S(1)}, bf16[2,48,1024]{2,1,0:T(8,128)(2,1)S(1)}, u32[]{:S(2)}, u32[]{:S(2)}) collective-permute-start(bf16[2,48,1024]{2,1,0:T(8,128)(2,1)S(1)} %pad_maximum_fusion.10), channel_id=1, source_target_pairs={{0,24},{8,0},{16,8},{24,16},{1,25},{9,1},{17,9},{25,17},{2,26},{10... | collective-permute-start | bytes 589832 | tf_op jit(solution)/shard_map/ppermute | solution.py:22
  52.2 30.4 %copy-start.26 = (bf16[96,1024]{1,0:T(8,128)(2,1)}, bf16[96,1024]{1,0:T(8,128)(2,1)S(1)}, u32[]{:S(2)}) copy-start(bf16[96,1024]{1,0:T(8,128)(2,1)S(1)} %collective-permute-done.10.refs_2_.refs_10_) | copy-start | bytes 589828
  53.9 27.5 %copy-start.14 = (bf16[288,1024]{1,0:T(8,128)(2,1)}, bf16[288,1024]{1,0:T(8,128)(2,1)S(1)}, u32[]{:S(2)}) copy-start(bf16[288,1024]{1,0:T(8,128)(2,1)S(1)} %collective-permute-done.6.refs_3_) | copy-start | bytes 1769476
  54.0 28.6 %copy-start = (bf16[3,2,48,1024]{3,2,1,0:T(8,128)(2,1)}, bf16[3,2,48,1024]{3,2,1,0:T(8,128)(2,1)S(1)}, u32[]{:S(2)}) copy-start(bf16[3,2,48,1024]{3,2,1,0:T(8,128)(2,1)S(1)} %pad_maximum_fusion.2) | copy-start | bytes 1769476
  54.0 18.6 %collective-permute-start.11 = (bf16[288,1024]{1,0:T(8,128)(2,1)S(1)}, bf16[288,1024]{1,0:T(8,128)(2,1)S(1)}, u32[]{:S(2)}, u32[]{:S(2)}) collective-permute-start(bf16[288,1024]{1,0:T(8,128)(2,1)S(1)} %bitcast.134), channel_id=1, source_target_pairs={{0,2},{2,0},{1,3},{3,1},{4,6},{6,4},{5,7},{7,5},{8,10},{10,8},{9,1... | collective-permute-start | bytes 1769480 | tf_op jit(solution)/shard_map/ppermute | solution.py:17
  55.5 18.1 %collective-permute-start.18 = (bf16[288,1024]{1,0:T(8,128)(2,1)S(1)}, bf16[288,1024]{1,0:T(8,128)(2,1)S(1)}, u32[]{:S(2)}, u32[]{:S(2)}) collective-permute-start(bf16[288,1024]{1,0:T(8,128)(2,1)S(1)} %bitcast.131), channel_id=1, source_target_pairs={{0,1},{1,0},{2,3},{3,2},{4,5},{5,4},{6,7},{7,6},{8,9},{9,8},{10,11... | collective-permute-start | bytes 1769480 | tf_op jit(solution)/shard_map/ppermute | solution.py:17
  55.5 18.5 %collective-permute-start.20 = (bf16[288,1024]{1,0:T(8,128)(2,1)S(1)}, bf16[288,1024]{1,0:T(8,128)(2,1)S(1)}, u32[]{:S(2)}, u32[]{:S(2)}) collective-permute-start(bf16[288,1024]{1,0:T(8,128)(2,1)S(1)} %collective-permute-done.6.refs_3_), channel_id=1, source_target_pairs={{0,1},{1,0},{2,3},{3,2},{4,5},{5,4},{6,7},{7,6},{8,9},{9,8},{10,11... | collective-permute-start | bytes 1769480 | tf_op jit(solution)/shard_map/ppermute | solution.py:17
  56.1 25.3 %copy-start.7 = (bf16[2,48,1024]{2,1,0:T(8,128)(2,1)}, bf16[2,48,1024]{2,1,0:T(8,128)(2,1)S(1)}, u32[]{:S(2)}) copy-start(bf16[2,48,1024]{2,1,0:T(8,128)(2,1)S(1)} %pad_maximum_fusion.11) | copy-start | bytes 589828
  56.1 26.5 %copy-start.9 = (bf16[1,896,2048]{2,1,0:T(8,128)(2,1)S(1)}, bf16[1,896,2048]{2,1,0:T(8,128)(2,1)}, u32[]{:S(2)}) copy-start(bf16[1,896,2048]{2,1,0:T(8,128)(2,1)} %refs_8_.3) | copy-start | bytes 11010052
  56.1 16.0 %collective-permute-start.16 = (bf16[96,1024]{1,0:T(8,128)(2,1)S(1)}, bf16[96,1024]{1,0:T(8,128)(2,1)S(1)}, u32[]{:S(2)}, u32[]{:S(2)}) collective-permute-start(bf16[96,1024]{1,0:T(8,128)(2,1)S(1)} %bitcast.142), channel_id=1, source_target_pairs={{0,2},{2,0},{1,3},{3,1},{4,6},{6,4},{5,7},{7,5},{8,10},{10,8},{9,1... | collective-permute-start | bytes 589832 | tf_op jit(solution)/shard_map/ppermute | solution.py:17
  56.7 15.4 %collective-permute-start.17 = (bf16[96,1024]{1,0:T(8,128)(2,1)S(1)}, bf16[96,1024]{1,0:T(8,128)(2,1)S(1)}, u32[]{:S(2)}, u32[]{:S(2)}) collective-permute-start(bf16[96,1024]{1,0:T(8,128)(2,1)S(1)} %bitcast.143), channel_id=1, source_target_pairs={{0,1},{1,0},{2,3},{3,2},{4,5},{5,4},{6,7},{7,6},{8,9},{9,8},{10,11... | collective-permute-start | bytes 589832 | tf_op jit(solution)/shard_map/ppermute | solution.py:17
  72.1 9.3 %copy-start.28 = (bf16[96,1024]{1,0:T(8,128)(2,1)}, bf16[96,1024]{1,0:T(8,128)(2,1)S(1)}, u32[]{:S(2)}) copy-start(bf16[96,1024]{1,0:T(8,128)(2,1)S(1)} %collective-permute-done.16.refs_2_) | copy-start | bytes 589828
  72.1 1.4 collective-permute-start.19
  72.1 9.3 %copy-start.30 = (bf16[96,1024]{1,0:T(8,128)(2,1)}, bf16[96,1024]{1,0:T(8,128)(2,1)S(1)}, u32[]{:S(2)}) copy-start(bf16[96,1024]{1,0:T(8,128)(2,1)S(1)} %collective-permute-done.17.refs_4_) | copy-start | bytes 589828
  72.1 10.4 %collective-permute-start.13 = (bf16[288,1024]{1,0:T(8,128)(2,1)S(1)}, bf16[288,1024]{1,0:T(8,128)(2,1)S(1)}, u32[]{:S(2)}, u32[]{:S(2)}) collective-permute-start(bf16[288,1024]{1,0:T(8,128)(2,1)S(1)} %bitcast.135), channel_id=1, source_target_pairs={{0,1},{1,0},{2,3},{3,2},{4,5},{5,4},{6,7},{7,6},{8,9},{9,8},{10,11... | collective-permute-start | bytes 1769480 | tf_op jit(solution)/shard_map/ppermute | solution.py:17
  72.6 10.0 %copy-start.16 = (bf16[288,1024]{1,0:T(8,128)(2,1)}, bf16[288,1024]{1,0:T(8,128)(2,1)S(1)}, u32[]{:S(2)}) copy-start(bf16[288,1024]{1,0:T(8,128)(2,1)S(1)} %collective-permute-done.11.refs_3_.refs_11_) | copy-start | bytes 1769476
  72.6 9.9 %collective-permute-start.15 = (bf16[288,1024]{1,0:T(8,128)(2,1)S(1)}, bf16[288,1024]{1,0:T(8,128)(2,1)S(1)}, u32[]{:S(2)}, u32[]{:S(2)}) collective-permute-start(bf16[288,1024]{1,0:T(8,128)(2,1)S(1)} %collective-permute-done.11.refs_3_.refs_11_), channel_id=1, source_target_pairs={{0,1},{1,0},{2,3},{3,2},{4,5},{5,4},{6,7},{7,6},{8,9},{9,8},{10,11... | collective-permute-start | bytes 1769480 | tf_op jit(solution)/shard_map/ppermute | solution.py:17
  73.5 9.0 %collective-permute-start.12 = (bf16[96,1024]{1,0:T(8,128)(2,1)S(1)}, bf16[96,1024]{1,0:T(8,128)(2,1)S(1)}, u32[]{:S(2)}, u32[]{:S(2)}) collective-permute-start(bf16[96,1024]{1,0:T(8,128)(2,1)S(1)} %bitcast.139), channel_id=1, source_target_pairs={{0,1},{1,0},{2,3},{3,2},{4,5},{5,4},{6,7},{7,6},{8,9},{9,8},{10,11... | collective-permute-start | bytes 589832 | tf_op jit(solution)/shard_map/ppermute | solution.py:17
  73.7 8.8 %collective-permute-start.14 = (bf16[96,1024]{1,0:T(8,128)(2,1)S(1)}, bf16[96,1024]{1,0:T(8,128)(2,1)S(1)}, u32[]{:S(2)}, u32[]{:S(2)}) collective-permute-start(bf16[96,1024]{1,0:T(8,128)(2,1)S(1)} %collective-permute-done.10.refs_2_.refs_10_), channel_id=1, source_target_pairs={{0,1},{1,0},{2,3},{3,2},{4,5},{5,4},{6,7},{7,6},{8,9},{9,8},{10,11... | collective-permute-start | bytes 589832 | tf_op jit(solution)/shard_map/ppermute | solution.py:17
  91.6 22.4 %collective-permute-start.22 = (bf16[384,1024]{1,0:T(8,128)(2,1)S(1)}, bf16[384,1024]{1,0:T(8,128)(2,1)}, u32[]{:S(2)}, u32[]{:S(2)}) collective-permute-start(bf16[384,1024]{1,0:T(8,128)(2,1)S(1)} %get-tuple-element.53), channel_id=1, source_target_pairs={{0,1},{1,0},{2,3},{3,2},{4,5},{5,4},{6,7},{7,6},{8,9},{9,8},{10,11... | collective-permute-start | bytes 2359304 | tf_op jit(solution)/shard_map/ppermute | solution.py:17
  91.8 25.9 %collective-permute-start.30 = (bf16[128,1024]{1,0:T(8,128)(2,1)S(1)}, bf16[128,1024]{1,0:T(8,128)(2,1)}, u32[]{:S(2)}, u32[]{:S(2)}) collective-permute-start(bf16[128,1024]{1,0:T(8,128)(2,1)S(1)} %copy-done.4), channel_id=1, source_target_pairs={{0,8},{8,16},{16,24},{24,0},{1,9},{9,17},{17,25},{25,1},{2,10},{10... | collective-permute-start | bytes 786440 | tf_op jit(solution)/shard_map/ppermute | solution.py:22
  97.8 55.3 %collective-permute-start.31 = (bf16[128,1024]{1,0:T(8,128)(2,1)S(1)}, bf16[128,1024]{1,0:T(8,128)(2,1)}, u32[]{:S(2)}, u32[]{:S(2)}) collective-permute-start(bf16[128,1024]{1,0:T(8,128)(2,1)S(1)} %copy-done.4), channel_id=1, source_target_pairs={{0,16},{8,24},{16,0},{24,8},{1,17},{9,25},{17,1},{25,9},{2,18},{10... | collective-permute-start | bytes 786440 | tf_op jit(solution)/shard_map/ppermute | solution.py:22
  101.2 52.9 %collective-permute-start.32 = (bf16[128,1024]{1,0:T(8,128)(2,1)S(1)}, bf16[128,1024]{1,0:T(8,128)(2,1)}, u32[]{:S(2)}, u32[]{:S(2)}) collective-permute-start(bf16[128,1024]{1,0:T(8,128)(2,1)S(1)} %copy-done.4), channel_id=1, source_target_pairs={{0,24},{8,0},{16,8},{24,16},{1,25},{9,1},{17,9},{25,17},{2,26},{10... | collective-permute-start | bytes 786440 | tf_op jit(solution)/shard_map/ppermute | solution.py:22
  113.2 6.1 %collective-permute-start.21 = (bf16[384,1024]{1,0:T(8,128)(2,1)S(1)}, bf16[384,1024]{1,0:T(8,128)(2,1)S(1)}, u32[]{:S(2)}, u32[]{:S(2)}) collective-permute-start(bf16[384,1024]{1,0:T(8,128)(2,1)S(1)} %get-tuple-element.51), channel_id=1, source_target_pairs={{0,1},{1,0},{2,3},{3,2},{4,5},{5,4},{6,7},{7,6},{8,9},{9,8},{10,11... | collective-permute-start | bytes 2359304 | tf_op jit(solution)/shard_map/ppermute | solution.py:17
  115.5 16.3 %collective-permute-start.24 = (bf16[288,1024]{1,0:T(8,128)(2,1)S(1)}, bf16[288,1024]{1,0:T(8,128)(2,1)S(1)}, u32[]{:S(2)}, u32[]{:S(2)}) collective-permute-start(bf16[288,1024]{1,0:T(8,128)(2,1)S(1)} %slice.487), channel_id=1, source_target_pairs={{0,2},{2,0},{1,3},{3,1},{4,6},{6,4},{5,7},{7,5},{8,10},{10,8},{9,1... | collective-permute-start | bytes 1769480 | tf_op jit(solution)/shard_map/ppermute | solution.py:17
  118.7 16.8 %collective-permute-start.23 = (bf16[96,1024]{1,0:T(8,128)(2,1)S(1)}, bf16[96,1024]{1,0:T(8,128)(2,1)S(1)}, u32[]{:S(2)}, u32[]{:S(2)}) collective-permute-start(bf16[96,1024]{1,0:T(8,128)(2,1)S(1)} %slice.485), channel_id=1, source_target_pairs={{0,2},{2,0},{1,3},{3,1},{4,6},{6,4},{5,7},{7,5},{8,10},{10,8},{9,1... | collective-permute-start | bytes 589832 | tf_op jit(solution)/shard_map/ppermute | solution.py:17
  132.0 6.3 %collective-permute-start.25 = (bf16[2,48,1024]{2,1,0:T(8,128)(2,1)S(1)}, bf16[2,48,1024]{2,1,0:T(8,128)(2,1)S(1)}, u32[]{:S(2)}, u32[]{:S(2)}) collective-permute-start(bf16[2,48,1024]{2,1,0:T(8,128)(2,1)S(1)} %bitcast.162), channel_id=1, source_target_pairs={{0,24},{8,0},{16,8},{24,16},{1,25},{9,1},{17,9},{25,17},{2,26},{10... | collective-permute-start | bytes 589832 | tf_op jit(solution)/shard_map/ppermute | solution.py:22
  132.9 18.6 %collective-permute-start.26 = (bf16[2,48,1024]{2,1,0:T(8,128)(2,1)S(1)}, bf16[2,48,1024]{2,1,0:T(8,128)(2,1)S(1)}, u32[]{:S(2)}, u32[]{:S(2)}) collective-permute-start(bf16[2,48,1024]{2,1,0:T(8,128)(2,1)S(1)} %bitcast.157), channel_id=1, source_target_pairs={{0,16},{8,24},{16,0},{24,8},{1,17},{9,25},{17,1},{25,9},{2,18},{10... | collective-permute-start | bytes 589832 | tf_op jit(solution)/shard_map/ppermute | solution.py:22
  135.5 16.0 %collective-permute-start.27 = (bf16[2,48,1024]{2,1,0:T(8,128)(2,1)S(1)}, bf16[2,48,1024]{2,1,0:T(8,128)(2,1)S(1)}, u32[]{:S(2)}, u32[]{:S(2)}) collective-permute-start(bf16[2,48,1024]{2,1,0:T(8,128)(2,1)S(1)} %bitcast.153), channel_id=1, source_target_pairs={{0,8},{8,16},{16,24},{24,0},{1,9},{9,17},{17,25},{25,1},{2,10},{10... | collective-permute-start | bytes 589832 | tf_op jit(solution)/shard_map/ppermute | solution.py:22
  138.2 37.6 %collective-permute-start.33 = (bf16[128,1024]{1,0:T(8,128)(2,1)S(1)}, bf16[128,1024]{1,0:T(8,128)(2,1)}, u32[]{:S(2)}, u32[]{:S(2)}) collective-permute-start(bf16[128,1024]{1,0:T(8,128)(2,1)S(1)} %copy-done.4), channel_id=1, source_target_pairs={{0,4},{4,0},{1,5},{5,1},{2,6},{6,2},{3,7},{7,3},{8,12},{12,8},{9,1... | collective-permute-start | bytes 786440 | tf_op jit(solution)/shard_map/ppermute | solution.py:17
  151.5 9.4 %collective-permute-start.37 = (bf16[128,1024]{1,0:T(8,128)(2,1)S(1)}, bf16[128,1024]{1,0:T(8,128)(2,1)S(1)}, u32[]{:S(2)}, u32[]{:S(2)}) collective-permute-start(bf16[128,1024]{1,0:T(8,128)(2,1)S(1)} %fusion.14.near), channel_id=1, source_target_pairs={{0,8},{8,16},{16,24},{24,0},{1,9},{9,17},{17,25},{25,1},{2,10},{10... | collective-permute-start | bytes 786440 | tf_op jit(solution)/shard_map/ppermute | solution.py:22
  151.6 10.1 %copy-start.48 = (bf16[128,1024]{1,0:T(8,128)(2,1)S(1)}, bf16[128,1024]{1,0:T(8,128)(2,1)}, u32[]{:S(2)}) copy-start(bf16[128,1024]{1,0:T(8,128)(2,1)} %param.16) | copy-start | bytes 786436
  151.6 10.1 %copy-start.81 = (f32[128]{0:T(128)S(1)}, f32[128]{0:T(128)}, u32[]{:S(2)}) copy-start(f32[128]{0:T(128)} %copy-done.80) | copy-start | bytes 1540
  151.7 10.1 %copy-start.83 = (f32[128]{0:T(128)S(1)}, f32[128]{0:T(128)}, u32[]{:S(2)}) copy-start(f32[128]{0:T(128)} %copy-done.82) | copy-start | bytes 1540
  152.5 9.2 %collective-permute-start.28 = (bf16[128,1024]{1,0:T(8,128)(2,1)S(1)}, bf16[128,1024]{1,0:T(8,128)(2,1)S(1)}, u32[]{:S(2)}, u32[]{:S(2)}) collective-permute-start(bf16[128,1024]{1,0:T(8,128)(2,1)S(1)} %convolution_convert_fusion.2), channel_id=1, source_target_pairs={{0,4},{4,0},{1,5},{5,1},{2,6},{6,2},{3,7},{7,3},{8,12},{12,8},{9,1... | collective-permute-start | bytes 786440 | tf_op jit(solution)/shard_map/ppermute | solution.py:17
  155.1 23.5 %collective-permute-start.34 = (bf16[384,1024]{1,0:T(8,128)(2,1)S(1)}, bf16[384,1024]{1,0:T(8,128)(2,1)S(1)}, u32[]{:S(2)}, u32[]{:S(2)}) collective-permute-start(bf16[384,1024]{1,0:T(8,128)(2,1)S(1)} %constant_dynamic-update-slice_fusion.far_w), channel_id=1, source_target_pairs={{0,4},{4,0},{1,5},{5,1},{2,6},{6,2},{3,7},{7,3},{8,12},{12,8},{9,1... | collective-permute-start | bytes 2359304 | tf_op jit(solution)/shard_map/ppermute | solution.py:17
  156.6 26.4 %collective-permute-start.38 = (bf16[128,1024]{1,0:T(8,128)(2,1)S(1)}, bf16[128,1024]{1,0:T(8,128)(2,1)}, u32[]{:S(2)}, u32[]{:S(2)}) collective-permute-start(bf16[128,1024]{1,0:T(8,128)(2,1)S(1)} %fusion.14.near), channel_id=1, source_target_pairs={{0,16},{8,24},{16,0},{24,8},{1,17},{9,25},{17,1},{25,9},{2,18},{10... | collective-permute-start | bytes 786440 | tf_op jit(solution)/shard_map/ppermute | solution.py:22
  160.9 23.1 %collective-permute-start.39 = (bf16[128,1024]{1,0:T(8,128)(2,1)S(1)}, bf16[128,1024]{1,0:T(8,128)(2,1)}, u32[]{:S(2)}, u32[]{:S(2)}) collective-permute-start(bf16[128,1024]{1,0:T(8,128)(2,1)S(1)} %fusion.14.near), channel_id=1, source_target_pairs={{0,24},{8,0},{16,8},{24,16},{1,25},{9,1},{17,9},{25,17},{2,26},{10... | collective-permute-start | bytes 786440 | tf_op jit(solution)/shard_map/ppermute | solution.py:22
  165.6 5.0 %collective-permute-start.29 = (bf16[4,128,128]{1,2,0:T(8,128)(2,1)S(1)}, bf16[4,128,128]{1,2,0:T(8,128)(2,1)S(1)}, u32[]{:S(2)}, u32[]{:S(2)}) collective-permute-start(bf16[4,128,128]{1,2,0:T(8,128)(2,1)S(1)} %fusion.55), channel_id=1, source_target_pairs={{0,2},{2,0},{1,3},{3,1},{4,6},{6,4},{5,7},{7,5},{8,10},{10,8},{9,1... | collective-permute-start | bytes 393224 | tf_op jit(solution)/shard_map/ppermute | solution.py:17
  170.6 65.7 %collective-permute-start.40 = (bf16[128,1024]{1,0:T(8,128)(2,1)S(1)}, bf16[128,1024]{1,0:T(8,128)(2,1)}, u32[]{:S(2)}, u32[]{:S(2)}) collective-permute-start(bf16[128,1024]{1,0:T(8,128)(2,1)S(1)} %fusion.14.near), channel_id=1, source_target_pairs={{0,4},{4,0},{1,5},{5,1},{2,6},{6,2},{3,7},{7,3},{8,12},{12,8},{9,1... | collective-permute-start | bytes 786440 | tf_op jit(solution)/shard_map/ppermute | solution.py:17
  181.5 13.4 %collective-permute-start.35 = (bf16[128,1024]{1,0:T(8,128)(2,1)}, bf16[128,1024]{1,0:T(8,128)(2,1)}, u32[]{:S(2)}, u32[]{:S(2)}) collective-permute-start(bf16[128,1024]{1,0:T(8,128)(2,1)} %get-tuple-element.55), channel_id=1, source_target_pairs={{0,2},{2,0},{1,3},{3,1},{4,6},{6,4},{5,7},{7,5},{8,10},{10,8},{9,1... | collective-permute-start | bytes 786440 | tf_op jit(solution)/shard_map/ppermute | solution.py:17
  184.0 11.0 %copy-start.51 = (f32[1024]{0:T(1024)S(1)}, f32[1024]{0:T(1024)}, u32[]{:S(2)}) copy-start(f32[1024]{0:T(1024)} %param.12) | copy-start | bytes 12292
  184.0 11.0 %copy-start.77 = (f32[128]{0:T(128)S(1)}, f32[128]{0:T(128)}, u32[]{:S(2)}) copy-start(f32[128]{0:T(128)} %copy-done.76) | copy-start | bytes 1540
  184.0 11.0 %copy-start.79 = (f32[128]{0:T(128)S(1)}, f32[128]{0:T(128)}, u32[]{:S(2)}) copy-start(f32[128]{0:T(128)} %copy-done.78) | copy-start | bytes 1540
  185.0 51.3 %collective-permute-start.41 = (bf16[384,1024]{1,0:T(8,128)(2,1)S(1)}, bf16[384,1024]{1,0:T(8,128)(2,1)S(1)}, u32[]{:S(2)}, u32[]{:S(2)}) collective-permute-start(bf16[384,1024]{1,0:T(8,128)(2,1)S(1)} %constant_dynamic-update-slice_fusion.3.far), channel_id=1, source_target_pairs={{0,4},{4,0},{1,5},{5,1},{2,6},{6,2},{3,7},{7,3},{8,12},{12,8},{9,1... | collective-permute-start | bytes 2359304 | tf_op jit(solution)/shard_map/ppermute | solution.py:17
  185.3 9.6 %copy-start.3 = (f32[128,1024]{1,0:T(8,128)S(1)}, f32[128,1024]{1,0:T(8,128)}, u32[]{:S(2)}) copy-start(f32[128,1024]{1,0:T(8,128)} %copy-done.2) | copy-start | bytes 1572868
  188.8 47.6 %all-to-all-start = ((bf16[8,128,256]{2,1,0:T(8,128)(2,1)}), bf16[8,128,256]{2,1,0:T(8,128)(2,1)S(1)}, u32[]{:S(2)}, u32[]{:S(2)}) async-start(bf16[8,128,256]{2,1,0:T(8,128)(2,1)} %all_gather.7), calls=%async_computation | async-start | bytes 1048576 | tf_op jit(solution)/shard_map/all_to_all | solution.py:425
  201.0 34.1 %collective-permute-start.36 = (bf16[30,1024]{1,0:T(8,128)(2,1)S(1)}, bf16[30,1024]{1,0:T(8,128)(2,1)S(1)}, u32[]{:S(2)}, u32[]{:S(2)}) collective-permute-start(bf16[30,1024]{1,0:T(8,128)(2,1)S(1)} %slice.495), channel_id=1, source_target_pairs={{2,0},{4,2},{6,4},{8,6},{10,8},{12,10},{14,12},{16,14},{18,16},{20... | collective-permute-start | bytes 184328 | tf_op jit(solution)/shard_map/ppermute | solution.py:28
  238.8 9.1 %collective-permute-start.42 = (bf16[128,1024]{1,0:T(8,128)(2,1)S(1)}, bf16[128,1024]{1,0:T(8,128)(2,1)S(1)}, u32[]{:S(2)}, u32[]{:S(2)}) collective-permute-start(bf16[128,1024]{1,0:T(8,128)(2,1)S(1)} %get-tuple-element.58), channel_id=1, source_target_pairs={{0,2},{2,0},{1,3},{3,1},{4,6},{6,4},{5,7},{7,5},{8,10},{10,8},{9,1... | collective-permute-start | bytes 786440 | tf_op jit(solution)/shard_map/ppermute | solution.py:17
  (68 other events, 251.7 us)

commit v3 on v2

--- a/solution.py
+++ b/solution.py
@@ -150,30 +150,35 @@
         piece(steps * 2 * LANES, count % (2 * LANES))
 
 
-def held_block(k, refs, side_refs):
-    if k == 0:
-        return (refs[0][...], side_refs[0][...])
-    rows = refs[0].shape[0]
-    at = slice((k - 1) * rows, k * rows)
-    return (refs[1][at, :], side_refs[1][at, :])
-
-
-def act_kernel(columns, near_w, far_w, near_side_w, far_side_w, kept, given):
-    blocks, rows, _ = columns.shape
+def block_of(k, stacks, refs):
+    for stack, ref in zip(stacks, refs, strict=True):
+        if k in stack:
+            rows = ref.shape[0] // len(stack)
+            at = stack.index(k) * rows
+            return ref[at : at + rows, :]
+    raise ValueError(k)
+
+
+def act_kernel(stacks, kept_cols, met_cols, *refs):
+    weights, (kept, given) = (refs[:-2], refs[-2:])
+    count = len(stacks)
+    blocks, rows, _ = kept_cols.shape
     planes = blocks // 2
     plane = lax.axis_index("far")
     side = lax.axis_index("side")
-    total = jnp.zeros((rows, near_w.shape[1]), jnp.float32)
+    total = jnp.zeros((2 * rows, kept.shape[1]), jnp.float32)
     for k in range(planes):
         r = lax.rem(plane + planes - k, planes)
-        here, beside = held_block(k, (near_w, far_w), (near_side_w, far_side_w))
-        total = total + dotted(columns[2 * r + side], here)
-        total = total + dotted(columns[2 * r + 1 - side], beside)
-    kept[...] = total[: rows // 2]
-    given[...] = total[rows // 2 :].astype(given.dtype)
-
-
-def proj_kernel(columns, near, far, near_side, far_side, kept, given, total):
+        for at, held in ((2 * r + side, weights[:count]), (2 * r + 1 - side, weights[count:])):
+            both = jnp.concatenate([kept_cols[at], met_cols[at]], axis=0)
+            total = total + dotted(both, block_of(k, stacks, held))
+    kept[...] = total[:rows]
+    given[...] = total[rows:].astype(given.dtype)
+
+
+def proj_kernel(stacks, columns, *refs):
+    acts, (kept, given, total) = (refs[:-3], refs[-3:])
+    count = len(stacks)
     planes = columns.shape[0] // 2
     plane = lax.axis_index("far")
     side = lax.axis_index("side")
@@ -182,9 +187,8 @@
     value = jnp.zeros(total.shape, jnp.float32)
     for k in range(planes):
         r = lax.rem(plane + planes - k, planes)
-        here, beside = held_block(k, (near, far), (near_side, far_side))
-        value = value + contract_rows(columns[2 * r + side], here)
-        value = value + contract_rows(columns[2 * r + 1 - side], beside)
+        for at, held in ((2 * r + side, acts[:count]), (2 * r + 1 - side, acts[count:])):
+            value = value + contract_rows(columns[at], block_of(k, stacks, held))
     total[...] = value
     kept[...] = total[pl.ds(pl.multiple_of(pair * out, out), out), :]
     given[...] = total[pl.ds(pl.multiple_of((1 - pair) * out, out), out), :].astype(given.dtype)
@@ -351,7 +355,6 @@
     grad_near_pair = swapped(grad_near, "pair")
     mid_pair, grad_far, grad_near_pair = fence((mid_pair, grad_far, grad_near_pair))
     proj_near_side = swapped(proj_weight, "side")
-    act_near_side = swapped(activated, "side")
     grad_mine = jnp.stack(grad_far).reshape(-1, half)
     grad_pair = swapped(grad_mine, "pair")
     proj_far = [shifted(proj_weight, k) for k in hops]
@@ -392,8 +395,15 @@
         summed.append(kept.astype(jnp.float32) + given.astype(jnp.float32))
     proj_rest = jnp.concatenate(proj_far, axis=0)
     proj_side = swapped(proj_rest, "side")
-    act_rest = jnp.concatenate(act_far, axis=0)
-    act_side = swapped(act_rest, "side")
+    proj_stacks = ((0,), tuple(hops))
+    late = planes // 2
+    first = tuple(k for k in range(planes) if k != late)
+    act_stacks = (first, (late,))
+    act_all = [activated, *act_far]
+    act_first = jnp.concatenate([act_all[k] for k in first], axis=0)
+    act_first_side = swapped(act_first, "side")
+    act_late = act_all[late]
+    act_late_side = swapped(act_late, "side")
     moving = summed[0].astype(jnp.bfloat16)
     across = swapped(moving[near_rows:], "pair")
     across_near = swapped(moving[:near_rows], "pair")
@@ -405,13 +415,12 @@
     for_beside = jnp.dot(
         beside_table, back[:, 1].reshape(wide, half), preferred_element_type=jnp.float32
     ).astype(jnp.bfloat16)
-    for_own = jnp.dot(
+    for_own = out_grad.astype(jnp.float32) + jnp.dot(
         own_table, back[:, 0].reshape(wide, half), preferred_element_type=jnp.float32
     )
+    for_own = fence(for_own)
     from_beside = swapped(for_beside, "side")
-    grad_stream = (
-        out_grad.astype(jnp.float32) + for_own + from_beside.astype(jnp.float32)
-    ).astype(jnp.bfloat16)
+    grad_stream = (for_own + from_beside.astype(jnp.float32)).astype(jnp.bfloat16)
 
     grad_gate, grad_up, grad_down = weight_grads(
         core, mids, cots, hidden_act, gate_pre, up_pre
@@ -423,16 +432,18 @@
     stream_met = swapped(chosen(pair, by_pair[1], by_pair[0]), "pair")
     whole_stream = lax.all_gather(by_place, "tp", axis=0, tiled=True)
     columns = lax.all_to_all(whole_stream, ("far", "side"), split_axis=0, concat_axis=0, tiled=True)
-    shared = jnp.concatenate([chosen(pair, by_pair[0], by_pair[1]), stream_met], axis=1)
-    shared = lax.all_gather(shared, "tp", axis=0, tiled=True)
+    kept_cols = lax.all_gather(
+        chosen(pair, by_pair[0], by_pair[1]), "tp", axis=0, tiled=True
+    )
+    met_cols = lax.all_gather(stream_met, "tp", axis=0, tiled=True)
     act_kept, act_given = in_vmem(
-        act_kernel,
+        functools.partial(act_kernel, proj_stacks),
         (
             jax.ShapeDtypeStruct((tok_rows, half), jnp.float32),
             jax.ShapeDtypeStruct((tok_rows, half), jnp.bfloat16),
         ),
         2 * tok_rows * width * half,
-        (shared, proj_weight, proj_rest, proj_near_side, proj_side),
+        (kept_cols, met_cols, proj_weight, proj_rest, proj_near_side, proj_side),
         limit=24,
     )
     act_met = swapped(act_given, "pair")
@@ -453,13 +464,13 @@
         grad_input = grad_input + tap_values[offset][None, :] * extended[offset : offset + tok_rows]
 
     proj_kept, proj_given = in_vmem(
-        proj_kernel,
+        functools.partial(proj_kernel, act_stacks),
         (
             jax.ShapeDtypeStruct((out_rows, half), jnp.float32),
             jax.ShapeDtypeStruct((out_rows, half), jnp.bfloat16),
         ),
         2 * tok_rows * width * half,
-        (columns, activated, act_rest, act_near_side, act_side),
+        (columns, act_first, act_late, act_first_side, act_late_side),
         (((2 * out_rows, half), jnp.float32),),
     )
     proj_met = swapped(proj_given, "pair")

time: 250 us -> 245 us (0.980)
  waiting for transfers between devices: 78.9 us -> 67.6 us
  starting transfers between devices: 58.6 us -> 65.9 us
  local copies, waits for them, and re-layouts: 39.5 us -> 33.8 us
  blocking collectives: 9.61 us -> 12.2 us
    ppermute x27, waiting for transfers between devices: 48.9 us -> 34.4 us  [swapped(): return lax.ppermute(value, axis, [(0, 1), (1, 0)])]
    ppermute x15, starting transfers between devices: 28.8 us -> 35.9 us  [shifted(): lax.ppermute(value, 'far', [(s, (s + steps) % count) for s in range(count)])]
    unnamed x180 -> x160, local copies, waits for them, and re-layouts: 30.3 us -> 23.9 us
    ppermute x15, waiting for transfers between devices: 30 us -> 33.1 us  [shifted(): lax.ppermute(value, 'far', [(s, (s + steps) % count) for s in range(count)])]
  transfers between devices with their start and end apart: 44 -> 44, of which waited for: 16 -> 13; matrix products, arithmetic and copies ran while one was open for 12% -> 13% of each run, Pallas kernels for 12% -> 12%
where the time goes in v3:
time: 245 us; the launch traced here: 242 us
  waiting for transfers between devices  67.6 us (28%)
  starting transfers between devices  65.9 us (27%)
  Pallas kernels  40 us (16%)
  local copies, waits for them, and re-layouts  33.8 us (14%)
  other arithmetic  18.1 us (7%)
  blocking collectives  12.2 us (5%)
  matrix products  2.48 us (1%)
    ppermute x15, starting transfers between devices, shifted(): lax.ppermute(value, 'far', [(s, (s + steps) % count) for s in range(count)])  35.9 us
    ppermute x27, waiting for transfers between devices, swapped(): return lax.ppermute(value, axis, [(0, 1), (1, 0)])  34.4 us
    ppermute x15, waiting for transfers between devices, shifted(): lax.ppermute(value, 'far', [(s, (s + steps) % count) for s in range(count)])  33.1 us
    pallas_call x6, Pallas kernels, in_vmem(): pl.pallas_call(kernel, out_shape=shapes, in_specs=[pl.BlockSpec(memory_sp...  26.1 us
    ppermute x27, starting transfers between devices, swapped(): return lax.ppermute(value, axis, [(0, 1), (1, 0)])  24.6 us
    unnamed x160, local copies, waits for them, and re-layouts  23.9 us
    pallas_call x1, Pallas kernels, weight_grads(): pl.pallas_call(grads_kernel, grid_spec=pltpu.PrefetchScalarGridSpec(num_s...  14 us
  transfers between devices with their start and end apart: 44, of which 13 were waited for; matrix products, arithmetic and copies ran while one was open for 13% of the time, Pallas kernels for 12%

profile of v3, /device:TPU:0, one launch (start us, length us, event | category | flops | bytes accessed | tf_op | source)
XLA Modules:
  0.0 242.1 jit_solution(5564488687904480760)
XLA Ops:
  2.1 3.0 %collective-permute-start = (f32[4,128]{1,0:T(4,128)S(1)}, f32[4,128]{1,0:T(4,128)S(1)}, u32[]{:S(2)}, u32[]{:S(2)}) collective-permute-start(f32[4,128]{1,0:T(4,128)S(1)} %pad_maximum_fusion.11), channel_id=1, source_target_pairs={{0,4},{4,0},{1,5},{5,1},{2,6},{6,2},{3,7},{7,3},{8,12},{12,8},{9,1... | collective-permute-start | bytes 6152 | tf_op jit(solution)/shard_map/ppermute | solution.py:17
  5.1 2.0 collective-permute-start.1
  7.9 1.1 fusion.3
  9.0 2.5 %all-reduce.1 = (f32[128]{0:T(128)S(1)}, f32[128]{0:T(128)S(1)}) all-reduce(f32[128]{0:T(128)S(1)} %get-tuple-element.66, f32[128]{0:T(128)S(1)} %get-tuple-element.65), channel_id=1, replica_groups=mesh['far'=4,'side'=2,'pair'=2,'tp'=2] {'tp'}, use_global_device_ids=true, to_apply=%region_3.0 | all-reduce | flops 256 | bytes 2048 | tf_op jit(solution)/shard_map/psum | solution.py:320
  11.5 2.0 fusion.14
  15.3 3.4 %collective-permute-done.1 = bf16[128,1024]{1,0:T(8,128)(2,1)S(1)} collective-permute-done((bf16[128,1024]{1,0:T(8,128)(2,1)}, bf16[128,1024]{1,0:T(8,128)(2,1)S(1)}, u32[]{:S(2)}, u32[]{:S(2)}) %collective-permute-start.1) | collective-permute-done | bytes 262176 | tf_op jit(solution)/shard_map/ppermute | solution.py:17
  19.0 2.7 %collective-permute-start.3 = (bf16[2,48,1024]{2,1,0:T(8,128)(2,1)S(1)}, bf16[2,48,1024]{2,1,0:T(8,128)(2,1)S(1)}, u32[]{:S(2)}, u32[]{:S(2)}) collective-permute-start(bf16[2,48,1024]{2,1,0:T(8,128)(2,1)S(1)} %pad_maximum_fusion.4), channel_id=1, source_target_pairs={{0,16},{8,24},{16,0},{24,8},{1,17},{9,25},{17,1},{25,9},{2,18},{10... | collective-permute-start | bytes 589832 | tf_op jit(solution)/shard_map/ppermute | solution.py:22
  21.7 1.4 collective-permute-start.4
  24.0 11.0 %collective-permute-done.3 = bf16[2,48,1024]{2,1,0:T(8,128)(2,1)S(1)} collective-permute-done((bf16[2,48,1024]{2,1,0:T(8,128)(2,1)S(1)}, bf16[2,48,1024]{2,1,0:T(8,128)(2,1)S(1)}, u32[]{:S(2)}, u32[]{:S(2)}) %collective-permute-start.3) | collective-permute-done | bytes 196640 | tf_op jit(solution)/shard_map/ppermute | solution.py:22
  35.1 1.6 collective-permute-start.6
  37.2 3.8 %collective-permute-start.7 = (bf16[2,48,1024]{2,1,0:T(8,128)(2,1)S(1)}, bf16[2,48,1024]{2,1,0:T(8,128)(2,1)S(1)}, u32[]{:S(2)}, u32[]{:S(2)}) collective-permute-start(bf16[2,48,1024]{2,1,0:T(8,128)(2,1)S(1)} %pad_maximum_fusion.7), channel_id=1, source_target_pairs={{0,8},{8,16},{16,24},{24,0},{1,9},{9,17},{17,25},{25,1},{2,10},{10... | collective-permute-start | bytes 589832 | tf_op jit(solution)/shard_map/ppermute | solution.py:22
  41.0 1.9 collective-permute-start.8
  42.9 2.9 %collective-permute-start.9 = (bf16[2,48,1024]{2,1,0:T(8,128)(2,1)S(1)}, bf16[2,48,1024]{2,1,0:T(8,128)(2,1)S(1)}, u32[]{:S(2)}, u32[]{:S(2)}) collective-permute-start(bf16[2,48,1024]{2,1,0:T(8,128)(2,1)S(1)} %pad_maximum_fusion.9), channel_id=1, source_target_pairs={{0,24},{8,0},{16,8},{24,16},{1,25},{9,1},{17,9},{25,17},{2,26},{10... | collective-permute-start | bytes 589832 | tf_op jit(solution)/shard_map/ppermute | solution.py:22
  45.8 6.3 %collective-permute-done.10.refs_2_.refs_10_ = bf16[96,1024]{1,0:T(8,128)(2,1)S(1)} collective-permute-done((bf16[96,1024]{1,0:T(8,128)(2,1)S(1)}, bf16[96,1024]{1,0:T(8,128)(2,1)S(1)}, u32[]{:S(2)}, u32[]{:S(2)}) %collective-permute-start.10) | collective-permute-done | bytes 196640 | tf_op jit(solution)/shard_map/ppermute | solution.py:17
  52.2 1.7 collective-permute-done.8
  54.0 1.6 collective-permute-start.11
  56.7 15.4 %collective-permute-done.16.refs_2_ = bf16[96,1024]{1,0:T(8,128)(2,1)S(1)} collective-permute-done((bf16[96,1024]{1,0:T(8,128)(2,1)S(1)}, bf16[96,1024]{1,0:T(8,128)(2,1)S(1)}, u32[]{:S(2)}, u32[]{:S(2)}) %collective-permute-start.16) | collective-permute-done | bytes 196640 | tf_op jit(solution)/shard_map/ppermute | solution.py:17
  74.1 7.3 %shard_map.146 = (bf16[768,896]{1,0:T(8,128)(2,1)S(1)}, bf16[768,896]{1,0:T(8,128)(2,1)S(1)}, bf16[768,896]{1,0:T(8,128)(2,1)S(1)}) custom-call(bf16[96,1024]{1,0:T(8,128)(2,1)S(1)} %bitcast.132, bf16[288,1024]{1,0:T(8,128)(2,1)S(1)} %bitcast.120, bf16[96,1024]{1,0:T(8,128)(2,1)S(1)} %collective-permute-done.16.refs_2_, ...), custom_call_target="tpu_custom_call" | custom-call | flops 5637144576 | bytes 10485760 | tf_op jit(solution)/shard_map/pallas_call | solution.py:80
  81.4 1.1 copy-done.39
  82.6 4.2 %shard_map.147 = (bf16[768,896]{1,0:T(8,128)(2,1)S(1)}, bf16[768,896]{1,0:T(8,128)(2,1)S(1)}) custom-call(bf16[96,1024]{1,0:T(8,128)(2,1)S(1)} %bitcast.128, bf16[288,1024]{1,0:T(8,128)(2,1)S(1)} %bitcast.124, bf16[96,1024]{1,0:T(8,128)(2,1)S(1)} %collective-permute-done.10.refs_2_.refs_10_, bf16[288,1024]{1,0:T(8,128)(2,1)S(1)} %collective-permute-done.11.refs_3_.refs_11_, ...), custom_call_target="tpu_custom_call" | custom-call | flops 2818572288 | bytes 9568256 | tf_op jit(solution)/shard_map/pallas_call | solution.py:80
  86.9 4.6 %shard_map.149 = (bf16[384,1024]{1,0:T(8,128)(2,1)S(1)}, bf16[384,1024]{1,0:T(8,128)(2,1)S(1)}) custom-call(bf16[768,896]{1,0:T(8,128)(2,1)S(1)} %get-tuple-element.48.gate_pre.refs_17_, bf16[768,896]{1,0:T(8,128)(2,1)S(1)} %get-tuple-element.49.up_pre.refs_18_, bf16[1,2048,896]{2,1,0:T(8,128)(2,1)S(1)} %copy-done.9, bf16[1,2048,896]{2,1,0:T(8,128)(2,1)S(1)} %copy-done.10), custom_call_target="tpu_custom_call" | custom-call | flops 2818572288 | bytes 10092544 | tf_op jit(solution)/shard_map/pallas_call | solution.py:80
  91.8 6.0 %collective-permute-start.30 = (bf16[128,1024]{1,0:T(8,128)(2,1)S(1)}, bf16[128,1024]{1,0:T(8,128)(2,1)}, u32[]{:S(2)}, u32[]{:S(2)}) collective-permute-start(bf16[128,1024]{1,0:T(8,128)(2,1)S(1)} %copy-done.3), channel_id=1, source_target_pairs={{0,8},{8,16},{16,24},{24,0},{1,9},{9,17},{17,25},{25,1},{2,10},{10... | collective-permute-start | bytes 786440 | tf_op jit(solution)/shard_map/ppermute | solution.py:22
  97.8 3.4 %collective-permute-start.31 = (bf16[128,1024]{1,0:T(8,128)(2,1)S(1)}, bf16[128,1024]{1,0:T(8,128)(2,1)}, u32[]{:S(2)}, u32[]{:S(2)}) collective-permute-start(bf16[128,1024]{1,0:T(8,128)(2,1)S(1)} %copy-done.3), channel_id=1, source_target_pairs={{0,16},{8,24},{16,0},{24,8},{1,17},{9,25},{17,1},{25,9},{2,18},{10... | collective-permute-start | bytes 786440 | tf_op jit(solution)/shard_map/ppermute | solution.py:22
  101.8 4.6 %shard_map.148 = (bf16[384,1024]{1,0:T(8,128)(2,1)S(1)}, bf16[384,1024]{1,0:T(8,128)(2,1)S(1)}) custom-call(bf16[768,896]{1,0:T(8,128)(2,1)S(1)} %get-tuple-element.48.gate_pre.refs_17_, bf16[768,896]{1,0:T(8,128)(2,1)S(1)} %get-tuple-element.49.up_pre.refs_18_, bf16[1,2048,896]{2,1,0:T(8,128)(2,1)S(1)} %copy-done.9, bf16[1,2048,896]{2,1,0:T(8,128)(2,1)S(1)} %copy-done.10), custom_call_target="tpu_custom_call" | custom-call | flops 2818572288 | bytes 10092544 | tf_op jit(solution)/shard_map/pallas_call | solution.py:80
  109.3 1.5 collective-permute-start.24
  113.0 5.9 %collective-permute-done.31 = bf16[128,1024]{1,0:T(8,128)(2,1)} collective-permute-done((bf16[128,1024]{1,0:T(8,128)(2,1)S(1)}, bf16[128,1024]{1,0:T(8,128)(2,1)}, u32[]{:S(2)}, u32[]{:S(2)}) %collective-permute-start.31) | collective-permute-done | bytes 262176 | tf_op jit(solution)/shard_map/ppermute | solution.py:22
  120.8 1.6 collective-permute-start.23
  122.4 1.4 convert_add_fusion
  123.8 2.0 collective-permute-done.24
  125.8 1.2 fusion.2
  127.1 4.4 %collective-permute-start.25 = (bf16[2,48,1024]{2,1,0:T(8,128)(2,1)S(1)}, bf16[2,48,1024]{2,1,0:T(8,128)(2,1)S(1)}, u32[]{:S(2)}, u32[]{:S(2)}) collective-permute-start(bf16[2,48,1024]{2,1,0:T(8,128)(2,1)S(1)} %bitcast.148), channel_id=1, source_target_pairs={{0,24},{8,0},{16,8},{24,16},{1,25},{9,1},{17,9},{25,17},{2,26},{10... | collective-permute-start | bytes 589832 | tf_op jit(solution)/shard_map/ppermute | solution.py:22
  132.2 4.6 %collective-permute-done.25 = bf16[2,48,1024]{2,1,0:T(8,128)(2,1)S(1)} collective-permute-done((bf16[2,48,1024]{2,1,0:T(8,128)(2,1)S(1)}, bf16[2,48,1024]{2,1,0:T(8,128)(2,1)S(1)}, u32[]{:S(2)}, u32[]{:S(2)}) %collective-permute-start.25) | collective-permute-done | bytes 196640 | tf_op jit(solution)/shard_map/ppermute | solution.py:22
  136.9 9.9 %collective-permute-done.26 = bf16[2,48,1024]{2,1,0:T(8,128)(2,1)S(1)} collective-permute-done((bf16[2,48,1024]{2,1,0:T(8,128)(2,1)S(1)}, bf16[2,48,1024]{2,1,0:T(8,128)(2,1)S(1)}, u32[]{:S(2)}, u32[]{:S(2)}) %collective-permute-start.26) | collective-permute-done | bytes 196640 | tf_op jit(solution)/shard_map/ppermute | solution.py:22
  148.8 1.5 collective-permute-start.34
  150.4 1.7 collective-permute-start.37
  152.1 2.1 collective-permute-start.38
  154.6 1.9 collective-permute-done.28
  157.5 1.4 collective-permute-start.29
  160.6 2.2 all-gather
  162.8 3.6 %collective-permute-start.39 = (bf16[128,1024]{1,0:T(8,128)(2,1)}, bf16[128,1024]{1,0:T(8,128)(2,1)}, u32[]{:S(2)}, u32[]{:S(2)}) collective-permute-start(bf16[128,1024]{1,0:T(8,128)(2,1)} %fusion.14), channel_id=1, source_target_pairs={{0,16},{8,24},{16,0},{24,8},{1,17},{9,25},{17,1},{25,9},{2,18},{10... | collective-permute-start | bytes 786440 | tf_op jit(solution)/shard_map/ppermute | solution.py:22
  166.4 1.7 copy.22
  168.1 2.2 all_gather.10.met_cols
  170.3 1.1 collective-permute-done.34.refs_3_
  171.4 2.9 %shard_map.150 = (f32[128,1024]{1,0:T(8,128)S(1)}, bf16[128,1024]{1,0:T(8,128)(2,1)}) custom-call(bf16[8,128,128]{2,1,0:T(8,128)(2,1)S(1)} %bitcast.117, bf16[8,128,128]{2,1,0:T(8,128)(2,1)S(1)} %all_gather.10.met_cols, bf16[128,1024]{1,0:T(8,128)(2,1)S(1)} %copy-done.3, bf16[384,1024]{1,0:T(8,128)(2,1)S(1)} %constant_dynamic-update-slice_fusion.refs_1_, ...), custom_call_target="tpu_custom_call" | custom-call | flops 536870912 | bytes 2621440 | tf_op jit(solution)/shard_map/pallas_call | solution.py:80
  174.3 1.5 collective-permute-start.35
  178.4 1.5 collective-permute-start.41
  179.9 1.1 copy.24
  181.0 2.3 all_gather.11
  183.3 4.1 %all-to-all-start = ((bf16[8,128,256]{2,1,0:T(8,128)(2,1)}), bf16[8,128,256]{2,1,0:T(8,128)(2,1)S(1)}, u32[]{:S(2)}, u32[]{:S(2)}) async-start(bf16[8,128,256]{2,1,0:T(8,128)(2,1)} %all_gather.11), calls=%async_computation | async-start | bytes 1048576 | tf_op jit(solution)/shard_map/all_to_all | solution.py:434
  187.4 3.0 %fusion.74 = (f32[128]{0:T(128)}, f32[128]{0:T(128)}, f32[128,1024]{1,0:T(8,128)}) fusion(f32[128]{0:T(128)} %copy-done.77, f32[128]{0:T(128)} %copy-done.76, bf16[128,1024]{1,0:T(8,128)(2,1)} %param.11, f32[1024]{0:T(1024)S(1)} %copy-done.47, f32[128,1024]{1,0:T(8,128)} %copy-done.2, bf16[128,1024]{1,0:T(8,128)(2,1)} %collective-permute-done.35), kind=kLoop, calls=%fused_computation.178 | loop fusion | flops 2359040 | bytes 1579008 | tf_op jit(solution)/shard_map/reduce_sum | solution.py:453
  190.3 3.1 %all-reduce = (f32[128]{0:T(128)S(1)}, f32[128]{0:T(128)}) all-reduce(f32[128]{0:T(128)} %get-tuple-element.64, f32[128]{0:T(128)} %get-tuple-element.63), channel_id=1, replica_groups=mesh['far'=4,'side'=2,'pair'=2,'tp'=2] {'tp'}, use_global_device_ids=true, to_apply=%region_9.10 | all-reduce | flops 256 | bytes 2048 | tf_op jit(solution)/shard_map/psum | solution.py:452
  194.1 1.3 fusion.22
  195.4 1.3 collective-permute-start.36
  198.6 1.1 copy-done.12
  199.7 1.1 copy-done.14
  200.7 1.1 copy-done.16
  210.6 1.3 copy-done.36
  211.9 1.3 copy-done.38
  213.2 1.3 copy-done.40
  214.6 14.0 %shard_map.152 = (bf16[1,2048,896]{2,1,0:T(8,128)(2,1)}, bf16[1,2048,896]{2,1,0:T(8,128)(2,1)}, bf16[1,896,2048]{2,1,0:T(8,128)(2,1)}) custom-call(s32[1]{0:T(128)} %bitcast.83.core_ref, bf16[96,1024]{1,0:T(8,128)(2,1)S(1)} %bitcast.133, bf16[288,1024]{1,0:T(8,128)(2,1)S(1)} %bitcast.121, bf16[96,1024]{1,0:T(8,128)(2,1)S(1)} %copy-done.26, ...), custom_call_target="tpu_custom_call" | custom-call | flops 8455716864 | bytes 11010048 | tf_op jit(solution)/shard_map/pallas_call | solution.py:261
  229.7 2.4 shard_map.151
  232.1 2.7 %collective-permute-start.42 = (bf16[128,1024]{1,0:T(8,128)(2,1)S(1)}, bf16[128,1024]{1,0:T(8,128)(2,1)S(1)}, u32[]{:S(2)}, u32[]{:S(2)}) collective-permute-start(bf16[128,1024]{1,0:T(8,128)(2,1)S(1)} %get-tuple-element.58), channel_id=1, source_target_pairs={{0,2},{2,0},{1,3},{3,1},{4,6},{6,4},{5,7},{7,5},{8,10},{10,8},{9,1... | collective-permute-start | bytes 786440 | tf_op jit(solution)/shard_map/ppermute | solution.py:17
  235.1 2.7 %fusion.24 = bf16[128,1024]{1,0:T(8,128)(2,1)} fusion(f32[158,1024]{1,0:T(8,128)S(1)} %copy-done.41, f32[1024]{0:T(1024)S(1)} %bitcast.181, f32[1024]{0:T(1024)S(1)} %bitcast.180, f32[1024]{0:T(1024)S(1)} %bitcast.179, f32[1024]{0:T(1024)S(1)} %bitcast.178, f32[1024]{0:T(1024)S(1)} %bitcast.177, f32[1024]{0:T(1024)S(1)} %bitcast.176, f32[1024]{0:T(1024)S(1)} %bitcast.175, ...), kind=kLoop, calls=%fused_computation.42 | loop fusion | flops 8126464 | bytes 16642048 | tf_op jit(solution)/shard_map/convert_element_type | solution.py:479
  237.8 3.4 %collective-permute-done.42 = bf16[128,1024]{1,0:T(8,128)(2,1)S(1)} collective-permute-done((bf16[128,1024]{1,0:T(8,128)(2,1)S(1)}, bf16[128,1024]{1,0:T(8,128)(2,1)S(1)}, u32[]{:S(2)}, u32[]{:S(2)}) %collective-permute-start.42) | collective-permute-done | bytes 262176 | tf_op jit(solution)/shard_map/ppermute | solution.py:17
  (255 shorter events, 38.5 us)
Async XLA Ops:
  0.6 13.9 %copy-start.44 = (bf16[128,1024]{1,0:T(8,128)(2,1)S(1)}, bf16[128,1024]{1,0:T(8,128)(2,1)}, u32[]{:S(2)}) copy-start(bf16[128,1024]{1,0:T(8,128)(2,1)} %param.16) | copy-start | bytes 786436
  0.6 13.5 %copy-start.45 = (bf16[128,1024]{1,0:T(8,128)(2,1)S(1)}, bf16[128,1024]{1,0:T(8,128)(2,1)}, u32[]{:S(2)}) copy-start(bf16[128,1024]{1,0:T(8,128)(2,1)} %param.15) | copy-start | bytes 786436
  2.1 11.5 %collective-permute-start = (f32[4,128]{1,0:T(4,128)S(1)}, f32[4,128]{1,0:T(4,128)S(1)}, u32[]{:S(2)}, u32[]{:S(2)}) collective-permute-start(f32[4,128]{1,0:T(4,128)S(1)} %pad_maximum_fusion.11), channel_id=1, source_target_pairs={{0,4},{4,0},{1,5},{5,1},{2,6},{6,2},{3,7},{7,3},{8,12},{12,8},{9,1... | collective-permute-start | bytes 6152 | tf_op jit(solution)/shard_map/ppermute | solution.py:17
  5.1 9.8 %collective-permute-start.5 = (bf16[128,1024]{1,0:T(8,128)(2,1)}, bf16[128,1024]{1,0:T(8,128)(2,1)S(1)}, u32[]{:S(2)}, u32[]{:S(2)}) collective-permute-start(bf16[128,1024]{1,0:T(8,128)(2,1)} %param.16), channel_id=1, source_target_pairs={{0,4},{4,0},{1,5},{5,1},{2,6},{6,2},{3,7},{7,3},{8,12},{12,8},{9,1... | collective-permute-start | bytes 786440 | tf_op jit(solution)/shard_map/ppermute | solution.py:17
  5.1 13.5 %collective-permute-start.1 = (bf16[128,1024]{1,0:T(8,128)(2,1)}, bf16[128,1024]{1,0:T(8,128)(2,1)S(1)}, u32[]{:S(2)}, u32[]{:S(2)}) collective-permute-start(bf16[128,1024]{1,0:T(8,128)(2,1)} %param.15), channel_id=1, source_target_pairs={{0,4},{4,0},{1,5},{5,1},{2,6},{6,2},{3,7},{7,3},{8,12},{12,8},{9,1... | collective-permute-start | bytes 786440 | tf_op jit(solution)/shard_map/ppermute | solution.py:17
  15.2 58.8 %copy-start.10 = (bf16[1,2048,896]{2,1,0:T(8,128)(2,1)S(1)}, bf16[1,2048,896]{2,1,0:T(8,128)(2,1)}, u32[]{:S(2)}) copy-start(bf16[1,2048,896]{2,1,0:T(8,128)(2,1)} %up_w.3) | copy-start | bytes 11010052
  19.0 16.0 %collective-permute-start.3 = (bf16[2,48,1024]{2,1,0:T(8,128)(2,1)S(1)}, bf16[2,48,1024]{2,1,0:T(8,128)(2,1)S(1)}, u32[]{:S(2)}, u32[]{:S(2)}) collective-permute-start(bf16[2,48,1024]{2,1,0:T(8,128)(2,1)S(1)} %pad_maximum_fusion.4), channel_id=1, source_target_pairs={{0,16},{8,24},{16,0},{24,8},{1,17},{9,25},{17,1},{25,9},{2,18},{10... | collective-permute-start | bytes 589832 | tf_op jit(solution)/shard_map/ppermute | solution.py:22
  21.7 13.3 %collective-permute-start.4 = (bf16[2,48,1024]{2,1,0:T(8,128)(2,1)S(1)}, bf16[2,48,1024]{2,1,0:T(8,128)(2,1)S(1)}, u32[]{:S(2)}, u32[]{:S(2)}) collective-permute-start(bf16[2,48,1024]{2,1,0:T(8,128)(2,1)S(1)} %pad_maximum_fusion.5), channel_id=1, source_target_pairs={{0,24},{8,0},{16,8},{24,16},{1,25},{9,1},{17,9},{25,17},{2,26},{10... | collective-permute-start | bytes 589832 | tf_op jit(solution)/shard_map/ppermute | solution.py:22
  23.1 11.9 %collective-permute-start.2 = (bf16[2,48,1024]{2,1,0:T(8,128)(2,1)S(1)}, bf16[2,48,1024]{2,1,0:T(8,128)(2,1)S(1)}, u32[]{:S(2)}, u32[]{:S(2)}) collective-permute-start(bf16[2,48,1024]{2,1,0:T(8,128)(2,1)S(1)} %pad_maximum_fusion.3), channel_id=1, source_target_pairs={{0,8},{8,16},{16,24},{24,0},{1,9},{9,17},{17,25},{25,1},{2,10},{10... | collective-permute-start | bytes 589832 | tf_op jit(solution)/shard_map/ppermute | solution.py:22
  23.9 58.6 %copy-start.4 = (bf16[2,48,1024]{2,1,0:T(8,128)(2,1)}, bf16[2,48,1024]{2,1,0:T(8,128)(2,1)S(1)}, u32[]{:S(2)}) copy-start(bf16[2,48,1024]{2,1,0:T(8,128)(2,1)S(1)} %pad_maximum_fusion.6) | copy-start | bytes 589828
  23.9 50.1 %copy-start.9 = (bf16[1,2048,896]{2,1,0:T(8,128)(2,1)S(1)}, bf16[1,2048,896]{2,1,0:T(8,128)(2,1)}, u32[]{:S(2)}) copy-start(bf16[1,2048,896]{2,1,0:T(8,128)(2,1)} %gate_w.3) | copy-start | bytes 11010052
  35.1 18.8 %collective-permute-start.6 = (bf16[288,1024]{1,0:T(8,128)(2,1)S(1)}, bf16[288,1024]{1,0:T(8,128)(2,1)S(1)}, u32[]{:S(2)}, u32[]{:S(2)}) collective-permute-start(bf16[288,1024]{1,0:T(8,128)(2,1)S(1)} %bitcast.118), channel_id=1, source_target_pairs={{0,2},{2,0},{1,3},{3,1},{4,6},{6,4},{5,7},{7,5},{8,10},{10,8},{9,1... | collective-permute-start | bytes 1769480 | tf_op jit(solution)/shard_map/ppermute | solution.py:17
  36.7 15.5 %collective-permute-start.10 = (bf16[96,1024]{1,0:T(8,128)(2,1)S(1)}, bf16[96,1024]{1,0:T(8,128)(2,1)S(1)}, u32[]{:S(2)}, u32[]{:S(2)}) collective-permute-start(bf16[96,1024]{1,0:T(8,128)(2,1)S(1)} %bitcast.126), channel_id=1, source_target_pairs={{0,2},{2,0},{1,3},{3,1},{4,6},{6,4},{5,7},{7,5},{8,10},{10,8},{9,1... | collective-permute-start | bytes 589832 | tf_op jit(solution)/shard_map/ppermute | solution.py:17
  37.2 15.0 %collective-permute-start.7 = (bf16[2,48,1024]{2,1,0:T(8,128)(2,1)S(1)}, bf16[2,48,1024]{2,1,0:T(8,128)(2,1)S(1)}, u32[]{:S(2)}, u32[]{:S(2)}) collective-permute-start(bf16[2,48,1024]{2,1,0:T(8,128)(2,1)S(1)} %pad_maximum_fusion.7), channel_id=1, source_target_pairs={{0,8},{8,16},{16,24},{24,0},{1,9},{9,17},{17,25},{25,1},{2,10},{10... | collective-permute-start | bytes 589832 | tf_op jit(solution)/shard_map/ppermute | solution.py:22
  41.0 12.9 %collective-permute-start.8 = (bf16[2,48,1024]{2,1,0:T(8,128)(2,1)S(1)}, bf16[2,48,1024]{2,1,0:T(8,128)(2,1)S(1)}, u32[]{:S(2)}, u32[]{:S(2)}) collective-permute-start(bf16[2,48,1024]{2,1,0:T(8,128)(2,1)S(1)} %pad_maximum_fusion.8), channel_id=1, source_target_pairs={{0,16},{8,24},{16,0},{24,8},{1,17},{9,25},{17,1},{25,9},{2,18},{10... | collective-permute-start | bytes 589832 | tf_op jit(solution)/shard_map/ppermute | solution.py:22
  42.9 11.0 %collective-permute-start.9 = (bf16[2,48,1024]{2,1,0:T(8,128)(2,1)S(1)}, bf16[2,48,1024]{2,1,0:T(8,128)(2,1)S(1)}, u32[]{:S(2)}, u32[]{:S(2)}) collective-permute-start(bf16[2,48,1024]{2,1,0:T(8,128)(2,1)S(1)} %pad_maximum_fusion.9), channel_id=1, source_target_pairs={{0,24},{8,0},{16,8},{24,16},{1,25},{9,1},{17,9},{25,17},{2,26},{10... | collective-permute-start | bytes 589832 | tf_op jit(solution)/shard_map/ppermute | solution.py:22
  52.2 30.4 %copy-start.23 = (bf16[96,1024]{1,0:T(8,128)(2,1)}, bf16[96,1024]{1,0:T(8,128)(2,1)S(1)}, u32[]{:S(2)}) copy-start(bf16[96,1024]{1,0:T(8,128)(2,1)S(1)} %collective-permute-done.10.refs_2_.refs_10_) | copy-start | bytes 589828
  53.9 27.4 %copy-start.11 = (bf16[288,1024]{1,0:T(8,128)(2,1)}, bf16[288,1024]{1,0:T(8,128)(2,1)S(1)}, u32[]{:S(2)}) copy-start(bf16[288,1024]{1,0:T(8,128)(2,1)S(1)} %collective-permute-done.6.refs_3_) | copy-start | bytes 1769476
  54.0 28.6 %copy-start = (bf16[3,2,48,1024]{3,2,1,0:T(8,128)(2,1)}, bf16[3,2,48,1024]{3,2,1,0:T(8,128)(2,1)S(1)}, u32[]{:S(2)}) copy-start(bf16[3,2,48,1024]{3,2,1,0:T(8,128)(2,1)S(1)} %pad_maximum_fusion.2) | copy-start | bytes 1769476
  54.0 18.6 %collective-permute-start.11 = (bf16[288,1024]{1,0:T(8,128)(2,1)S(1)}, bf16[288,1024]{1,0:T(8,128)(2,1)S(1)}, u32[]{:S(2)}, u32[]{:S(2)}) collective-permute-start(bf16[288,1024]{1,0:T(8,128)(2,1)S(1)} %bitcast.122), channel_id=1, source_target_pairs={{0,2},{2,0},{1,3},{3,1},{4,6},{6,4},{5,7},{7,5},{8,10},{10,8},{9,1... | collective-permute-start | bytes 1769480 | tf_op jit(solution)/shard_map/ppermute | solution.py:17
  55.5 18.1 %collective-permute-start.18 = (bf16[288,1024]{1,0:T(8,128)(2,1)S(1)}, bf16[288,1024]{1,0:T(8,128)(2,1)S(1)}, u32[]{:S(2)}, u32[]{:S(2)}) collective-permute-start(bf16[288,1024]{1,0:T(8,128)(2,1)S(1)} %bitcast.119), channel_id=1, source_target_pairs={{0,1},{1,0},{2,3},{3,2},{4,5},{5,4},{6,7},{7,6},{8,9},{9,8},{10,11... | collective-permute-start | bytes 1769480 | tf_op jit(solution)/shard_map/ppermute | solution.py:17
  55.5 18.5 %collective-permute-start.20 = (bf16[288,1024]{1,0:T(8,128)(2,1)S(1)}, bf16[288,1024]{1,0:T(8,128)(2,1)S(1)}, u32[]{:S(2)}, u32[]{:S(2)}) collective-permute-start(bf16[288,1024]{1,0:T(8,128)(2,1)S(1)} %collective-permute-done.6.refs_3_), channel_id=1, source_target_pairs={{0,1},{1,0},{2,3},{3,2},{4,5},{5,4},{6,7},{7,6},{8,9},{9,8},{10,11... | collective-permute-start | bytes 1769480 | tf_op jit(solution)/shard_map/ppermute | solution.py:17
  56.1 25.3 %copy-start.6 = (bf16[2,48,1024]{2,1,0:T(8,128)(2,1)}, bf16[2,48,1024]{2,1,0:T(8,128)(2,1)S(1)}, u32[]{:S(2)}) copy-start(bf16[2,48,1024]{2,1,0:T(8,128)(2,1)S(1)} %pad_maximum_fusion.10) | copy-start | bytes 589828
  56.1 26.5 %copy-start.8 = (bf16[1,896,2048]{2,1,0:T(8,128)(2,1)S(1)}, bf16[1,896,2048]{2,1,0:T(8,128)(2,1)}, u32[]{:S(2)}) copy-start(bf16[1,896,2048]{2,1,0:T(8,128)(2,1)} %refs_8_.3) | copy-start | bytes 11010052
  56.1 16.0 %collective-permute-start.16 = (bf16[96,1024]{1,0:T(8,128)(2,1)S(1)}, bf16[96,1024]{1,0:T(8,128)(2,1)S(1)}, u32[]{:S(2)}, u32[]{:S(2)}) collective-permute-start(bf16[96,1024]{1,0:T(8,128)(2,1)S(1)} %bitcast.130), channel_id=1, source_target_pairs={{0,2},{2,0},{1,3},{3,1},{4,6},{6,4},{5,7},{7,5},{8,10},{10,8},{9,1... | collective-permute-start | bytes 589832 | tf_op jit(solution)/shard_map/ppermute | solution.py:17
  56.7 15.4 %collective-permute-start.17 = (bf16[96,1024]{1,0:T(8,128)(2,1)S(1)}, bf16[96,1024]{1,0:T(8,128)(2,1)S(1)}, u32[]{:S(2)}, u32[]{:S(2)}) collective-permute-start(bf16[96,1024]{1,0:T(8,128)(2,1)S(1)} %bitcast.131), channel_id=1, source_target_pairs={{0,1},{1,0},{2,3},{3,2},{4,5},{5,4},{6,7},{7,6},{8,9},{9,8},{10,11... | collective-permute-start | bytes 589832 | tf_op jit(solution)/shard_map/ppermute | solution.py:17
  72.1 9.3 %copy-start.25 = (bf16[96,1024]{1,0:T(8,128)(2,1)}, bf16[96,1024]{1,0:T(8,128)(2,1)S(1)}, u32[]{:S(2)}) copy-start(bf16[96,1024]{1,0:T(8,128)(2,1)S(1)} %collective-permute-done.16.refs_2_) | copy-start | bytes 589828
  72.1 1.4 collective-permute-start.19
  72.1 9.3 %copy-start.27 = (bf16[96,1024]{1,0:T(8,128)(2,1)}, bf16[96,1024]{1,0:T(8,128)(2,1)S(1)}, u32[]{:S(2)}) copy-start(bf16[96,1024]{1,0:T(8,128)(2,1)S(1)} %collective-permute-done.17.refs_4_) | copy-start | bytes 589828
  72.1 10.4 %collective-permute-start.13 = (bf16[288,1024]{1,0:T(8,128)(2,1)S(1)}, bf16[288,1024]{1,0:T(8,128)(2,1)S(1)}, u32[]{:S(2)}, u32[]{:S(2)}) collective-permute-start(bf16[288,1024]{1,0:T(8,128)(2,1)S(1)} %bitcast.123), channel_id=1, source_target_pairs={{0,1},{1,0},{2,3},{3,2},{4,5},{5,4},{6,7},{7,6},{8,9},{9,8},{10,11... | collective-permute-start | bytes 1769480 | tf_op jit(solution)/shard_map/ppermute | solution.py:17
  72.6 10.0 %copy-start.13 = (bf16[288,1024]{1,0:T(8,128)(2,1)}, bf16[288,1024]{1,0:T(8,128)(2,1)S(1)}, u32[]{:S(2)}) copy-start(bf16[288,1024]{1,0:T(8,128)(2,1)S(1)} %collective-permute-done.11.refs_3_.refs_11_) | copy-start | bytes 1769476
  72.6 9.9 %collective-permute-start.15 = (bf16[288,1024]{1,0:T(8,128)(2,1)S(1)}, bf16[288,1024]{1,0:T(8,128)(2,1)S(1)}, u32[]{:S(2)}, u32[]{:S(2)}) collective-permute-start(bf16[288,1024]{1,0:T(8,128)(2,1)S(1)} %collective-permute-done.11.refs_3_.refs_11_), channel_id=1, source_target_pairs={{0,1},{1,0},{2,3},{3,2},{4,5},{5,4},{6,7},{7,6},{8,9},{9,8},{10,11... | collective-permute-start | bytes 1769480 | tf_op jit(solution)/shard_map/ppermute | solution.py:17
  73.5 7.9 %copy-start.29 = (bf16[96,1024]{1,0:T(8,128)(2,1)}, bf16[96,1024]{1,0:T(8,128)(2,1)S(1)}, u32[]{:S(2)}) copy-start(bf16[96,1024]{1,0:T(8,128)(2,1)S(1)} %collective-permute-done.19.refs_6_) | copy-start | bytes 589828
  73.5 9.0 %collective-permute-start.12 = (bf16[96,1024]{1,0:T(8,128)(2,1)S(1)}, bf16[96,1024]{1,0:T(8,128)(2,1)S(1)}, u32[]{:S(2)}, u32[]{:S(2)}) collective-permute-start(bf16[96,1024]{1,0:T(8,128)(2,1)S(1)} %bitcast.127), channel_id=1, source_target_pairs={{0,1},{1,0},{2,3},{3,2},{4,5},{5,4},{6,7},{7,6},{8,9},{9,8},{10,11... | collective-permute-start | bytes 589832 | tf_op jit(solution)/shard_map/ppermute | solution.py:17
  73.7 7.7 %copy-start.15 = (bf16[288,1024]{1,0:T(8,128)(2,1)}, bf16[288,1024]{1,0:T(8,128)(2,1)S(1)}, u32[]{:S(2)}) copy-start(bf16[288,1024]{1,0:T(8,128)(2,1)S(1)} %collective-permute-done.18.refs_5_) | copy-start | bytes 1769476
  73.7 8.8 %collective-permute-start.14 = (bf16[96,1024]{1,0:T(8,128)(2,1)S(1)}, bf16[96,1024]{1,0:T(8,128)(2,1)S(1)}, u32[]{:S(2)}, u32[]{:S(2)}) collective-permute-start(bf16[96,1024]{1,0:T(8,128)(2,1)S(1)} %collective-permute-done.10.refs_2_.refs_10_), channel_id=1, source_target_pairs={{0,1},{1,0},{2,3},{3,2},{4,5},{5,4},{6,7},{7,6},{8,9},{9,8},{10,11... | collective-permute-start | bytes 589832 | tf_op jit(solution)/shard_map/ppermute | solution.py:17
  86.9 14.9 %copy-start.35 = (bf16[768,896]{1,0:T(8,128)(2,1)}, bf16[768,896]{1,0:T(8,128)(2,1)S(1)}, u32[]{:S(2)}) copy-start(bf16[768,896]{1,0:T(8,128)(2,1)S(1)} %get-tuple-element.48.gate_pre.refs_17_) | copy-start | bytes 4128772
  86.9 14.9 %copy-start.37 = (bf16[768,896]{1,0:T(8,128)(2,1)}, bf16[768,896]{1,0:T(8,128)(2,1)S(1)}, u32[]{:S(2)}) copy-start(bf16[768,896]{1,0:T(8,128)(2,1)S(1)} %get-tuple-element.49.up_pre.refs_18_) | copy-start | bytes 4128772
  91.6 15.0 %copy-start.46 = (bf16[31,1024]{1,0:T(8,128)(2,1)S(1)}, bf16[31,1024]{1,0:T(8,128)(2,1)}, u32[]{:S(2)}) copy-start(bf16[31,1024]{1,0:T(8,128)(2,1)} %param.13) | copy-start | bytes 190468
  91.6 15.6 %collective-permute-start.22 = (bf16[384,1024]{1,0:T(8,128)(2,1)S(1)}, bf16[384,1024]{1,0:T(8,128)(2,1)S(1)}, u32[]{:S(2)}, u32[]{:S(2)}) collective-permute-start(bf16[384,1024]{1,0:T(8,128)(2,1)S(1)} %get-tuple-element.53), channel_id=1, source_target_pairs={{0,1},{1,0},{2,3},{3,2},{4,5},{5,4},{6,7},{7,6},{8,9},{9,8},{10,11... | collective-permute-start | bytes 2359304 | tf_op jit(solution)/shard_map/ppermute | solution.py:17
  91.8 19.7 %collective-permute-start.30 = (bf16[128,1024]{1,0:T(8,128)(2,1)S(1)}, bf16[128,1024]{1,0:T(8,128)(2,1)}, u32[]{:S(2)}, u32[]{:S(2)}) collective-permute-start(bf16[128,1024]{1,0:T(8,128)(2,1)S(1)} %copy-done.3), channel_id=1, source_target_pairs={{0,8},{8,16},{16,24},{24,0},{1,9},{9,17},{17,25},{25,1},{2,10},{10... | collective-permute-start | bytes 786440 | tf_op jit(solution)/shard_map/ppermute | solution.py:22
  97.8 21.1 %collective-permute-start.31 = (bf16[128,1024]{1,0:T(8,128)(2,1)S(1)}, bf16[128,1024]{1,0:T(8,128)(2,1)}, u32[]{:S(2)}, u32[]{:S(2)}) collective-permute-start(bf16[128,1024]{1,0:T(8,128)(2,1)S(1)} %copy-done.3), channel_id=1, source_target_pairs={{0,16},{8,24},{16,0},{24,8},{1,17},{9,25},{17,1},{25,9},{2,18},{10... | collective-permute-start | bytes 786440 | tf_op jit(solution)/shard_map/ppermute | solution.py:22
  101.2 46.7 %collective-permute-start.32 = (bf16[128,1024]{1,0:T(8,128)(2,1)S(1)}, bf16[128,1024]{1,0:T(8,128)(2,1)}, u32[]{:S(2)}, u32[]{:S(2)}) collective-permute-start(bf16[128,1024]{1,0:T(8,128)(2,1)S(1)} %copy-done.3), channel_id=1, source_target_pairs={{0,24},{8,0},{16,8},{24,16},{1,25},{9,1},{17,9},{25,17},{2,26},{10... | collective-permute-start | bytes 786440 | tf_op jit(solution)/shard_map/ppermute | solution.py:22
  106.5 15.9 %collective-permute-start.21 = (bf16[384,1024]{1,0:T(8,128)(2,1)S(1)}, bf16[384,1024]{1,0:T(8,128)(2,1)}, u32[]{:S(2)}, u32[]{:S(2)}) collective-permute-start(bf16[384,1024]{1,0:T(8,128)(2,1)S(1)} %get-tuple-element.51), channel_id=1, source_target_pairs={{0,1},{1,0},{2,3},{3,2},{4,5},{5,4},{6,7},{7,6},{8,9},{9,8},{10,11... | collective-permute-start | bytes 2359304 | tf_op jit(solution)/shard_map/ppermute | solution.py:17
  109.3 16.5 %collective-permute-start.24 = (bf16[288,1024]{1,0:T(8,128)(2,1)}, bf16[288,1024]{1,0:T(8,128)(2,1)}, u32[]{:S(2)}, u32[]{:S(2)}) collective-permute-start(bf16[288,1024]{1,0:T(8,128)(2,1)} %slice.487), channel_id=1, source_target_pairs={{0,2},{2,0},{1,3},{3,1},{4,6},{6,4},{5,7},{7,5},{8,10},{10,8},{9,1... | collective-permute-start | bytes 1769480 | tf_op jit(solution)/shard_map/ppermute | solution.py:17
  111.5 58.8 %collective-permute-start.33 = (bf16[128,1024]{1,0:T(8,128)(2,1)S(1)}, bf16[128,1024]{1,0:T(8,128)(2,1)}, u32[]{:S(2)}, u32[]{:S(2)}) collective-permute-start(bf16[128,1024]{1,0:T(8,128)(2,1)S(1)} %copy-done.3), channel_id=1, source_target_pairs={{0,4},{4,0},{1,5},{5,1},{2,6},{6,2},{3,7},{7,3},{8,12},{12,8},{9,1... | collective-permute-start | bytes 786440 | tf_op jit(solution)/shard_map/ppermute | solution.py:17
  120.8 10.7 %collective-permute-start.23 = (bf16[96,1024]{1,0:T(8,128)(2,1)S(1)}, bf16[96,1024]{1,0:T(8,128)(2,1)S(1)}, u32[]{:S(2)}, u32[]{:S(2)}) collective-permute-start(bf16[96,1024]{1,0:T(8,128)(2,1)S(1)} %slice.485), channel_id=1, source_target_pairs={{0,2},{2,0},{1,3},{3,1},{4,6},{6,4},{5,7},{7,5},{8,10},{10,8},{9,1... | collective-permute-start | bytes 589832 | tf_op jit(solution)/shard_map/ppermute | solution.py:17
  127.1 9.8 %collective-permute-start.25 = (bf16[2,48,1024]{2,1,0:T(8,128)(2,1)S(1)}, bf16[2,48,1024]{2,1,0:T(8,128)(2,1)S(1)}, u32[]{:S(2)}, u32[]{:S(2)}) collective-permute-start(bf16[2,48,1024]{2,1,0:T(8,128)(2,1)S(1)} %bitcast.148), channel_id=1, source_target_pairs={{0,24},{8,0},{16,8},{24,16},{1,25},{9,1},{17,9},{25,17},{2,26},{10... | collective-permute-start | bytes 589832 | tf_op jit(solution)/shard_map/ppermute | solution.py:22
  131.6 15.2 %collective-permute-start.26 = (bf16[2,48,1024]{2,1,0:T(8,128)(2,1)S(1)}, bf16[2,48,1024]{2,1,0:T(8,128)(2,1)S(1)}, u32[]{:S(2)}, u32[]{:S(2)}) collective-permute-start(bf16[2,48,1024]{2,1,0:T(8,128)(2,1)S(1)} %bitcast.145), channel_id=1, source_target_pairs={{0,16},{8,24},{16,0},{24,8},{1,17},{9,25},{17,1},{25,9},{2,18},{10... | collective-permute-start | bytes 589832 | tf_op jit(solution)/shard_map/ppermute | solution.py:22
  131.6 15.2 %collective-permute-start.27 = (bf16[2,48,1024]{2,1,0:T(8,128)(2,1)S(1)}, bf16[2,48,1024]{2,1,0:T(8,128)(2,1)S(1)}, u32[]{:S(2)}, u32[]{:S(2)}) collective-permute-start(bf16[2,48,1024]{2,1,0:T(8,128)(2,1)S(1)} %bitcast.142), channel_id=1, source_target_pairs={{0,8},{8,16},{16,24},{24,0},{1,9},{9,17},{17,25},{25,1},{2,10},{10... | collective-permute-start | bytes 589832 | tf_op jit(solution)/shard_map/ppermute | solution.py:22
  147.3 9.2 %collective-permute-start.28 = (bf16[128,1024]{1,0:T(8,128)(2,1)S(1)}, bf16[128,1024]{1,0:T(8,128)(2,1)S(1)}, u32[]{:S(2)}, u32[]{:S(2)}) collective-permute-start(bf16[128,1024]{1,0:T(8,128)(2,1)S(1)} %convolution_convert_fusion.2), channel_id=1, source_target_pairs={{0,4},{4,0},{1,5},{5,1},{2,6},{6,2},{3,7},{7,3},{8,12},{12,8},{9,1... | collective-permute-start | bytes 786440 | tf_op jit(solution)/shard_map/ppermute | solution.py:17
  148.8 22.6 %collective-permute-start.34 = (bf16[384,1024]{1,0:T(8,128)(2,1)S(1)}, bf16[384,1024]{1,0:T(8,128)(2,1)S(1)}, u32[]{:S(2)}, u32[]{:S(2)}) collective-permute-start(bf16[384,1024]{1,0:T(8,128)(2,1)S(1)} %constant_dynamic-update-slice_fusion.refs_1_), channel_id=1, source_target_pairs={{0,4},{4,0},{1,5},{5,1},{2,6},{6,2},{3,7},{7,3},{8,12},{12,8},{9,1... | collective-permute-start | bytes 2359304 | tf_op jit(solution)/shard_map/ppermute | solution.py:17
  150.4 25.4 %collective-permute-start.37 = (bf16[128,1024]{1,0:T(8,128)(2,1)}, bf16[128,1024]{1,0:T(8,128)(2,1)}, u32[]{:S(2)}, u32[]{:S(2)}) collective-permute-start(bf16[128,1024]{1,0:T(8,128)(2,1)} %fusion.14), channel_id=1, source_target_pairs={{0,8},{8,16},{16,24},{24,0},{1,9},{9,17},{17,25},{25,1},{2,10},{10... | collective-permute-start | bytes 786440 | tf_op jit(solution)/shard_map/ppermute | solution.py:22
  152.1 24.7 %collective-permute-start.38 = (bf16[128,1024]{1,0:T(8,128)(2,1)}, bf16[128,1024]{1,0:T(8,128)(2,1)}, u32[]{:S(2)}, u32[]{:S(2)}) collective-permute-start(bf16[128,1024]{1,0:T(8,128)(2,1)} %fusion.14), channel_id=1, source_target_pairs={{0,24},{8,0},{16,8},{24,16},{1,25},{9,1},{17,9},{25,17},{2,26},{10... | collective-permute-start | bytes 786440 | tf_op jit(solution)/shard_map/ppermute | solution.py:22
  157.5 5.3 %collective-permute-start.29 = (bf16[4,128,128]{1,2,0:T(8,128)(2,1)}, bf16[4,128,128]{1,2,0:T(8,128)(2,1)}, u32[]{:S(2)}, u32[]{:S(2)}) collective-permute-start(bf16[4,128,128]{1,2,0:T(8,128)(2,1)} %get-tuple-element.95), channel_id=1, source_target_pairs={{0,2},{2,0},{1,3},{3,1},{4,6},{6,4},{5,7},{7,5},{8,10},{10,8},{9,1... | collective-permute-start | bytes 393224 | tf_op jit(solution)/shard_map/ppermute | solution.py:17
  162.8 15.6 %collective-permute-start.39 = (bf16[128,1024]{1,0:T(8,128)(2,1)}, bf16[128,1024]{1,0:T(8,128)(2,1)}, u32[]{:S(2)}, u32[]{:S(2)}) collective-permute-start(bf16[128,1024]{1,0:T(8,128)(2,1)} %fusion.14), channel_id=1, source_target_pairs={{0,16},{8,24},{16,0},{24,8},{1,17},{9,25},{17,1},{25,9},{2,18},{10... | collective-permute-start | bytes 786440 | tf_op jit(solution)/shard_map/ppermute | solution.py:22
  174.3 13.1 %collective-permute-start.35 = (bf16[128,1024]{1,0:T(8,128)(2,1)}, bf16[128,1024]{1,0:T(8,128)(2,1)}, u32[]{:S(2)}, u32[]{:S(2)}) collective-permute-start(bf16[128,1024]{1,0:T(8,128)(2,1)} %get-tuple-element.55), channel_id=1, source_target_pairs={{0,2},{2,0},{1,3},{3,1},{4,6},{6,4},{5,7},{7,5},{8,10},{10,8},{9,1... | collective-permute-start | bytes 786440 | tf_op jit(solution)/shard_map/ppermute | solution.py:17
  176.8 10.6 %copy-start.47 = (f32[1024]{0:T(1024)S(1)}, f32[1024]{0:T(1024)}, u32[]{:S(2)}) copy-start(f32[1024]{0:T(1024)} %param.12) | copy-start | bytes 12292
  177.8 51.9 %collective-permute-start.40 = (bf16[384,1024]{1,0:T(8,128)(2,1)S(1)}, bf16[384,1024]{1,0:T(8,128)(2,1)S(1)}, u32[]{:S(2)}, u32[]{:S(2)}) collective-permute-start(bf16[384,1024]{1,0:T(8,128)(2,1)S(1)} %constant_dynamic-update-slice_fusion.3.refs_0_), channel_id=1, source_target_pairs={{0,4},{4,0},{1,5},{5,1},{2,6},{6,2},{3,7},{7,3},{8,12},{12,8},{9,1... | collective-permute-start | bytes 2359304 | tf_op jit(solution)/shard_map/ppermute | solution.py:17
  178.4 51.3 %collective-permute-start.41 = (bf16[128,1024]{1,0:T(8,128)(2,1)}, bf16[128,1024]{1,0:T(8,128)(2,1)S(1)}, u32[]{:S(2)}, u32[]{:S(2)}) collective-permute-start(bf16[128,1024]{1,0:T(8,128)(2,1)} %collective-permute-done.39.refs_1_), channel_id=1, source_target_pairs={{0,4},{4,0},{1,5},{5,1},{2,6},{6,2},{3,7},{7,3},{8,12},{12,8},{9,1... | collective-permute-start | bytes 786440 | tf_op jit(solution)/shard_map/ppermute | solution.py:17
  183.3 46.4 %all-to-all-start = ((bf16[8,128,256]{2,1,0:T(8,128)(2,1)}), bf16[8,128,256]{2,1,0:T(8,128)(2,1)S(1)}, u32[]{:S(2)}, u32[]{:S(2)}) async-start(bf16[8,128,256]{2,1,0:T(8,128)(2,1)} %all_gather.11), calls=%async_computation | async-start | bytes 1048576 | tf_op jit(solution)/shard_map/all_to_all | solution.py:434
  187.4 9.4 %copy-start.1 = (bf16[3,2,48,1024]{3,2,1,0:T(8,128)(2,1)S(1)}, bf16[3,2,48,1024]{3,2,1,0:T(8,128)(2,1)}, u32[]{:S(2)}) copy-start(bf16[3,2,48,1024]{3,2,1,0:T(8,128)(2,1)} %copy-done) | copy-start | bytes 1769476
  195.4 33.1 %collective-permute-start.36 = (bf16[30,1024]{1,0:T(8,128)(2,1)S(1)}, bf16[30,1024]{1,0:T(8,128)(2,1)S(1)}, u32[]{:S(2)}, u32[]{:S(2)}) collective-permute-start(bf16[30,1024]{1,0:T(8,128)(2,1)S(1)} %slice.495), channel_id=1, source_target_pairs={{2,0},{4,2},{6,4},{8,6},{10,8},{12,10},{14,12},{16,14},{18,16},{20... | collective-permute-start | bytes 184328 | tf_op jit(solution)/shard_map/ppermute | solution.py:28
  232.1 9.1 %collective-permute-start.42 = (bf16[128,1024]{1,0:T(8,128)(2,1)S(1)}, bf16[128,1024]{1,0:T(8,128)(2,1)S(1)}, u32[]{:S(2)}, u32[]{:S(2)}) collective-permute-start(bf16[128,1024]{1,0:T(8,128)(2,1)S(1)} %get-tuple-element.58), channel_id=1, source_target_pairs={{0,2},{2,0},{1,3},{3,1},{4,6},{6,4},{5,7},{7,5},{8,10},{10,8},{9,1... | collective-permute-start | bytes 786440 | tf_op jit(solution)/shard_map/ppermute | solution.py:17
  (58 other events, 217.0 us)
